TPU v7x, 512 devices: a whole 4x4x16 slice. The times are simulated.
512 devices in a mesh: sp: 16 (over z), fs: 4 (over y), tp: 8 (over x, core).
Axes of the slice: x: 4, y: 4, z: 16, core: 2. Of those that a mesh axis runs over, the one named last changes fastest.
Arguments:
- tokens: bfloat16 [16384, 2048], P(('fs', 'sp', 'tp')), parts along dimension 0, may hold values from -6 to 6
- norm_gain: bfloat16 [2048], replicated, may hold values from 0.099609375 to 1.8984375
- w_pool_in: bfloat16 [2048, 1024], P('sp', 'tp'), may hold values from -0.125 to 0.125
- w_query: bfloat16 [2048, 1024], P('sp', 'tp'), may hold values from -0.125 to 0.125
- w_key: bfloat16 [2048, 1024], P('sp', 'tp'), may hold values from -0.125 to 0.125
- w_value: bfloat16 [2048, 1024], P('sp', 'tp'), may hold values from -0.125 to 0.125
- w_gate: bfloat16 [2048, 1024], P('sp', 'tp'), may hold values from -0.125 to 0.125
- w_beta: bfloat16 [2048, 8], replicated, may hold values from -0.125 to 0.125
- w_decay: bfloat16 [2048, 8], replicated, may hold values from -0.5 to 0.5
- conv_weight: float32 [3, 4, 1024], P(None, None, 'tp'), may hold values from -3 to 3
- a_log: float32 [8], P('tp'), may hold values from -20 to -1.7, as said below
- decay_extra: float32 [16384, 8], P(('fs', 'sp'), 'tp'), parts along dimension 0, may hold values from -1.4 to 0
- w_mix: bfloat16 [8, 128, 128], P('tp'), may hold values from -0.5 to 0.5
- pool_scale: float32 [1024], P('tp'), may hold values from 0.1 to 1.9
- delta_gain: float32 [128], replicated, may hold values from 0.1 to 1.9
- w_out_pool: bfloat16 [1024, 2048], P('tp', 'sp'), may hold values from -0.125 to 0.125
- w_out_delta: bfloat16 [1024, 2048], P('tp', 'sp'), may hold values from -0.125 to 0.125
Outputs:
- mixed: bfloat16 [16384, 2048], P(('fs', 'sp', 'tp')), parts along dimension 0
There are 4 independent parts, one for each index of `fs`. A program takes and returns all parts, laid end to end along the dimension named above; an argument that names none is the same for every part. Nothing has to cross between parts.
Inputs may be any that keep to these rules, and one draw needn't show every extreme that they name: `a_log`: logarithm of each head's base decay rate.
All inputs are finite; a program needn't handle non-finite values.
Results may differ from a plain program's by a relative error of at most 0.018.
Values may be sent and summed in bfloat16 or wider, within the bound.
No kernel may reach another device: no remote copies, remote signals or barrier semaphores. Data moves between devices by JAX's collectives and lax.ppermute only.
A program may use at most 64 MiB of HBM per device.

v0:
```python
import jax
import jax.numpy as jnp
from jax import lax
from jax.sharding import PartitionSpec as P

BLOCK = 64


eps = 1e-06
windows = (2, 4, 8, 16)
tail_rows = 15


def turned_gather(arrays, axis, dims):
    turned = [jnp.moveaxis(a, dim, 0) for a, dim in zip(arrays, dims)]
    both = jnp.concatenate([t.reshape(len(t), -1) for t in turned], axis=1)
    out, at, finished = (lax.all_gather(both, axis, axis=0, tiled=True), 0, [])
    for t, dim in zip(turned, dims):
        slab = out[:, at : at + t[0].size].reshape(-1, *t.shape[1:])
        finished.append(jnp.moveaxis(slab, 0, dim))
        at += t[0].size
    return tuple(finished)


def copy_for_each(x, axis):
    copies = jnp.broadcast_to(x, (lax.axis_size(axis), *x.shape))
    return lax.all_to_all(copies, axis, split_axis=0, concat_axis=0, tiled=True)


def laid_out(blocks, dim):
    lengths = list(blocks.shape[1:])
    lengths[dim] *= blocks.shape[0]
    return jnp.moveaxis(blocks, 0, dim).reshape(lengths)


def gather_directly(x, axis, dim):
    blocks = copy_for_each(x, axis)
    return laid_out(blocks, dim)


def from_behind(block, axis, distance):
    devices = range(lax.axis_size(axis))
    route = [(i - distance, i) for i in devices if i - distance in devices]
    return lax.ppermute(block, axis, route)


def entering(x, axis, join, neutral):
    place = lax.axis_index(axis)
    gathered = jax.tree.map(
        lambda a, kind: lax.all_gather(a.astype(kind), axis), x, (jnp.bfloat16, jnp.bfloat16)
    )
    state = jax.tree.map(lambda a, e: jnp.zeros_like(a) + jnp.asarray(e, a.dtype), x, neutral)

    def one(hop, state):
        return join(
            state,
            jax.tree.map(
                lambda a, own: lax.dynamic_index_in_dim(a, hop, 0, False).astype(own.dtype),
                gathered,
                x,
            ),
        )

    return lax.fori_loop(0, place, one, state)


def side_by_side(arrays, axis, dim, along):
    ends, at = ([], 0)
    for a in arrays[:-1]:
        at += a.shape[along]
        ends.append(at)
    both = jnp.concatenate(arrays, axis=along)
    return tuple(jnp.split(lax.all_gather(both, axis, axis=dim, tiled=True), ends, axis=along))


def rms_rows(values, gain):
    floats = values.astype(jnp.float32)
    scale = lax.rsqrt(jnp.mean(floats * floats, axis=-1, keepdims=True) + eps)
    return (floats * scale * gain.astype(jnp.float32)).astype(jnp.bfloat16)


def unit_rows(values):
    return values * lax.rsqrt(jnp.sum(values * values, axis=-1, keepdims=True) + eps)


def block_terms(query, keys, values, log_gate, strength, block):
    heads, length, width = keys.shape
    count = length // block

    def split(tensor):
        return tensor.reshape(heads, count, block, tensor.shape[-1])

    query_part, key_part, value_part = (split(query), split(keys), split(values))
    gate_cum = jnp.cumsum(log_gate.reshape(heads, count, block), axis=-1)
    beta_part = strength.reshape(heads, count, block)[..., None]
    lower_mask = jnp.tril(jnp.ones((block, block), dtype=bool))
    strict_mask = jnp.tril(jnp.ones((block, block), dtype=bool), k=-1)
    gaps = gate_cum[..., :, None] - gate_cum[..., None, :]
    decay_tab = jnp.where(lower_mask, jnp.exp(jnp.where(lower_mask, gaps, 0.0)), 0.0)
    key_scaled_beta = key_part * beta_part
    value_beta = value_part * beta_part
    corr_lower = jnp.where(
        strict_mask, jnp.einsum("hnid,hnjd->hnij", key_scaled_beta, key_part) * decay_tab, 0.0
    )
    identity = jnp.eye(block, dtype=jnp.float32)
    inverse = lax.linalg.triangular_solve(
        identity + corr_lower,
        jnp.broadcast_to(identity, corr_lower.shape),
        left_side=True,
        lower=True,
    )
    fixed_values = jnp.einsum("hnij,hnjd->hnid", inverse, value_beta)
    key_weights = jnp.einsum(
        "hnij,hnjd->hnid", inverse, key_scaled_beta * jnp.exp(gate_cum)[..., None]
    )
    scores = jnp.where(
        lower_mask, jnp.einsum("hnid,hnjd->hnij", query_part, key_part) * decay_tab, 0.0
    )
    key_decayed = key_part * jnp.exp(gate_cum[..., -1:] - gate_cum)[..., None]
    query_gated = query_part * jnp.exp(gate_cum)[..., None]
    terms = (query_gated, key_decayed, fixed_values, key_weights, scores, gate_cum[..., -1])
    return tuple((jnp.moveaxis(tensor, 1, 0) for tensor in terms))


def carry_step(state, inputs):
    query_gated, key_decayed, fixed_values, key_weights, scores, last_gate = inputs
    fresh = fixed_values - jnp.einsum("hcd,hde->hce", key_weights, state)
    output = jnp.einsum("hcd,hde->hce", query_gated, state) + jnp.einsum(
        "hij,hje->hie", scores, fresh
    )
    state = state * jnp.exp(last_gate)[:, None, None] + jnp.einsum(
        "hcd,hce->hde", key_decayed, fresh
    )
    return (state, output)


def compose_step(carry, inputs):
    linear, offset = carry
    query_gated, key_decayed, fixed_values, key_weights, scores, last_gate = inputs
    fade = jnp.exp(last_gate)[:, None, None]
    moved = jnp.einsum("hcd,hde->hce", key_weights, linear)
    linear = fade * linear - jnp.einsum("hcd,hce->hde", key_decayed, moved)
    fresh = fixed_values - jnp.einsum("hcd,hde->hce", key_weights, offset)
    offset = fade * offset + jnp.einsum("hcd,hce->hde", key_decayed, fresh)
    return ((linear, offset), None)


def apply_map(linear, state):
    return jnp.einsum("hij,hjk->hik", linear, state)


def combine_maps(earlier, later):
    return (apply_map(later[0], earlier[0]), apply_map(later[0], earlier[1]) + later[1])


def per_device(
    tokens,
    norm_gain,
    w_pool_in,
    w_query,
    w_key,
    w_value,
    w_gate,
    w_beta,
    w_decay,
    conv_weight,
    a_log,
    decay_extra,
    w_mix,
    pool_scale,
    delta_gain,
    w_out_pool,
    w_out_delta,
):
    pool_w, query_w, key_w, value_w, gate_w, outp_w, outd_w = turned_gather(
        (w_pool_in, w_query, w_key, w_value, w_gate, w_out_pool, w_out_delta),
        "sp",
        (0, 0, 0, 0, 0, 1, 1),
    )
    rows_all = gather_directly(tokens, "tp", 0)
    norm_result = rms_rows(rows_all, norm_gain)
    length = norm_result.shape[0]

    def project(weight):
        return jnp.dot(norm_result, weight, preferred_element_type=jnp.float32).astype(jnp.bfloat16)

    pool_in = project(pool_w)
    query_raw = project(query_w)
    key_raw = project(key_w)
    value_raw = project(value_w)
    gate_raw = project(gate_w)
    heads_dev = a_log.shape[0]
    head_dim = query_raw.shape[1] // heads_dev
    width_dev = heads_dev * head_dim
    all_heads = w_beta.shape[1]
    lane = lax.axis_index("tp")
    both_pre = jnp.dot(
        norm_result, jnp.concatenate([w_beta, w_decay], axis=1), preferred_element_type=jnp.float32
    )
    beta_pre = lax.dynamic_slice_in_dim(both_pre[:, :all_heads], lane * heads_dev, heads_dev, 1)
    forget_logits = lax.dynamic_slice_in_dim(
        both_pre[:, all_heads:], lane * heads_dev, heads_dev, 1
    )
    raw_three = jnp.concatenate([query_raw, key_raw, value_raw], axis=1)
    tails = jnp.concatenate(
        [pool_in[length - tail_rows :], raw_three[length - tail_rows :]], axis=1
    )
    prior_state = from_behind(tails, "sp", 1)
    pool_width_dev = pool_in.shape[1]
    source_rows = pool_in.astype(jnp.float32)
    extended = jnp.concatenate(
        [prior_state[:, :pool_width_dev].astype(jnp.float32), source_rows], axis=0
    )
    running = jnp.concatenate(
        [jnp.zeros((1, pool_width_dev), jnp.float32), jnp.cumsum(extended, axis=0)], axis=0
    )
    groups_dev = w_mix.shape[0]
    group_dim = w_mix.shape[1]
    group = lane * groups_dev + jnp.arange(pool_width_dev) // group_dim
    span = (2 ** (1 + group % 4)).astype(jnp.int32)
    ending = running[tail_rows + 1 : tail_rows + 1 + length]
    window_sum = jnp.zeros((length, pool_width_dev), jnp.float32)
    for width in windows:
        lagged = running[tail_rows + 1 - width : tail_rows + 1 - width + length]
        window_sum = window_sum + jnp.where(span[None, :] == width, ending - lagged, 0.0)
    positions = lax.axis_index("sp") * length + jnp.arange(length)
    counts = jnp.minimum(positions[:, None] + 1, span[None, :]).astype(jnp.float32)
    pooled = (window_sum / counts - source_rows).astype(jnp.bfloat16)
    mixed_pool = jnp.einsum(
        "sgc,gcd->sgd",
        pooled.reshape(length, groups_dev, group_dim),
        w_mix,
        preferred_element_type=jnp.float32,
    )
    pool_out = (mixed_pool.reshape(length, pool_width_dev) * pool_scale).astype(jnp.bfloat16)
    taps = conv_weight.shape[1]
    kernel = jnp.transpose(conv_weight, (1, 0, 2)).reshape(taps, 3 * width_dev)
    stacked = jnp.concatenate(
        [prior_state[tail_rows - (taps - 1) :, pool_width_dev:], raw_three], axis=0
    ).astype(jnp.float32)
    conv = jnp.zeros((length, 3 * width_dev), jnp.float32)
    for tap in range(taps):
        conv = conv + stacked[tap : tap + length] * kernel[tap]
    after_silu = jax.nn.silu(conv)

    def heads_first(tensor):
        return jnp.transpose(tensor.reshape(length, heads_dev, head_dim), (1, 0, 2))

    query = unit_rows(heads_first(after_silu[:, :width_dev])) * head_dim ** (-0.5)
    keys = unit_rows(heads_first(after_silu[:, width_dev : 2 * width_dev]))
    values = heads_first(after_silu[:, 2 * width_dev :])
    strength = jax.nn.sigmoid(beta_pre).T
    log_gate = (-jnp.exp(a_log)[None, :] * jax.nn.softplus(forget_logits) + decay_extra).T
    terms = block_terms(query, keys, values, log_gate, strength, BLOCK)
    identity = jnp.broadcast_to(
        jnp.eye(head_dim, dtype=jnp.float32), (heads_dev, head_dim, head_dim)
    )
    empty = jnp.zeros((heads_dev, head_dim, head_dim), jnp.float32)
    (linear, offset), _ = lax.scan(compose_step, (identity, empty), terms)
    prefix = entering((linear, offset), "sp", combine_maps, (identity, empty))
    incoming = prefix[1]
    _, outputs = lax.scan(carry_step, incoming, terms)
    attended = jnp.transpose(outputs, (1, 0, 2, 3)).reshape(heads_dev, length, head_dim)
    normal_out = (
        attended
        * lax.rsqrt(jnp.mean(attended * attended, axis=-1, keepdims=True) + eps)
        * delta_gain
    )
    gated = normal_out * jax.nn.silu(heads_first(gate_raw.astype(jnp.float32)))
    delta_out = jnp.transpose(gated, (1, 0, 2)).reshape(length, width_dev).astype(jnp.bfloat16)
    groups = lax.axis_size("tp")
    rows = length // groups
    both = jnp.concatenate([pool_out, delta_out], axis=1)
    arrived = lax.all_to_all(both, "tp", split_axis=0, concat_axis=0, tiled=True).reshape(
        groups, rows, pool_width_dev + width_dev
    )
    pool_rows, delta_rows = side_by_side((outp_w, outd_w), "tp", 0, 1)
    part_pool = jnp.einsum(
        "jrp,jpd->jrd",
        arrived[..., :pool_width_dev],
        pool_rows.reshape(groups, pool_width_dev, -1),
        preferred_element_type=jnp.float32,
    )
    part_delta = jnp.einsum(
        "jrp,jpd->jrd",
        arrived[..., pool_width_dev:],
        delta_rows.reshape(groups, width_dev, -1),
        preferred_element_type=jnp.float32,
    )
    value_partial_rows = lax.optimization_barrier(
        (part_pool + part_delta).astype(jnp.bfloat16)
    ).astype(jnp.float32)
    result = jnp.sum(value_partial_rows, axis=0)
    return result.astype(jnp.bfloat16)


def solution(mesh):
    placed = (
        P(("fs", "sp", "tp"), None),
        P(),
        P("sp", "tp"),
        P("sp", "tp"),
        P("sp", "tp"),
        P("sp", "tp"),
        P("sp", "tp"),
        P(),
        P(),
        P(None, None, "tp"),
        P("tp"),
        P(("fs", "sp"), "tp"),
        P("tp", None, None),
        P("tp"),
        P(),
        P("tp", "sp"),
        P("tp", "sp"),
    )
    return jax.shard_map(
        per_device,
        mesh=mesh,
        in_specs=placed,
        out_specs=P(("fs", "sp", "tp"), None),
        check_vma=False,
    )
```

profile of v0, /device:TPU:1, one launch (start us, length us, event | category | flops | bytes accessed | tf_op | source)
XLA Modules:
  0.0 249.7 jit_solution(6866411914422944330)
XLA Ops:
  6.5 0.9 copy.78
  13.3 2.0 broadcast_in_dim.91
  15.3 10.4 %all-to-all-start = ((bf16[8,32,2048]{2,1,0:T(8,128)(2,1)}), bf16[8,32,2048]{2,1,0:T(8,128)(2,1)S(1)}, u32[]{:S(2)}, u32[]{:S(2)}) async-start(bf16[8,32,2048]{2,1,0:T(8,128)(2,1)} %broadcast_in_dim.91), calls=%async_computation | async-start | bytes 2097152 | tf_op jit(solution)/shard_map/all_to_all | solution.py:27
  26.5 71.0 %all-gather.5.cloned.1.call-done = bf16[2048,896]{0,1:T(8,128)(2,1)} async-done(((bf16[128,896]{0,1:T(8,128)(2,1)}), bf16[2048,896]{0,1:T(8,128)(2,1)}) %all-gather.5.cloned.1.call-update) | async-done | bytes 3670032 | tf_op jit(solution)/shard_map/all_gather | solution.py:17
  97.5 1.3 slice_bitcast_fusion.1
  98.8 1.1 pad_maximum_fusion
  101.8 1.5 fusion.131
  103.3 1.5 convolution_convert_fusion.1
  104.8 1.5 convolution_convert_fusion.2
  106.3 1.5 convolution_convert_fusion.3
  107.8 3.3 %collective-permute-start = (bf16[15,512]{1,0:T(8,128)(2,1)S(1)}, bf16[15,512]{1,0:T(8,128)(2,1)S(1)}, u32[]{:S(2)}, u32[]{:S(2)}) collective-permute-start(bf16[15,512]{1,0:T(8,128)(2,1)S(1)} %fusion.115), channel_id=1, source_target_pairs={{0,32},{32,64},{64,96},{96,128},{128,160},{160,192},{192,224},{224... | collective-permute-start | bytes 46088 | tf_op jit(solution)/shard_map/ppermute | solution.py:44
  113.1 19.7 %custom-call.3 = f32[1,4,1,64,64]{3,4,2,1,0:T(8,128)S(1)} custom-call(f32[1,4,1,64,64]{4,3,2,1,0:T(8,128)S(1)} %fusion.65), custom_call_target="InvertDiagBlocksLowerTriangular" | custom-call | tf_op jit(solution)/shard_map/triangular_solve | solution.py:106
  133.8 9.7 %while.39 = (s32[]{:T(128)}, f32[1,128,128]{2,1,0:T(8,128)S(1)}, f32[1,128,128]{2,1,0:T(8,128)S(1)}, f32[4,1]{0,1:T(1,128)S(1)}, bf16[4,1,64,128]{3,2,1,0:T(8,12...) while((s32[]{:T(128)}, f32[1,128,128]{2,1,0:T(8,128)S(1)}, ...), condition=%wide.region_6.7_spmd.clone, body=%wide.region_5.6_spmd.clone.sunk | while | flops 8503299 | bytes 757378 | solution.py:259
  134.5 0.9 fusion.208
  136.9 0.9 fusion.208
  139.3 0.9 fusion.208
  141.7 0.9 fusion.208
  143.8 26.1 %all-gather = bf16[16,128,128]{2,1,0:T(8,128)(2,1)S(1)} all-gather(bf16[1,128,128]{2,1,0:T(8,128)(2,1)S(1)} %convert_element_type.116), channel_id=2, replica_groups=mesh['sp'=16,'fs'=4,'tp'=8] {'sp'}, dimensions={0}, use_global_device_ids=true | all-gather | bytes 557056 | tf_op jit(solution)/shard_map/all_gather | solution.py:50
  169.9 24.1 %all-gather.1 = bf16[16,128,128]{2,1,0:T(8,128)(2,1)S(1)} all-gather(bf16[1,128,128]{2,1,0:T(8,128)(2,1)S(1)} %convert_element_type.117), channel_id=3, replica_groups=mesh['sp'=16,'fs'=4,'tp'=8] {'sp'}, dimensions={0}, use_global_device_ids=true | all-gather | bytes 557056 | tf_op jit(solution)/shard_map/all_gather | solution.py:50
  194.0 7.4 %while.38 = (s32[]{:T(128)}, f32[1,128,128]{2,1,0:T(8,128)S(1)}, f32[4,1,64,128]{3,2,1,0:T(8,128)S(1)}, f32[4,1]{0,1:T(1,128)S(1)}, bf16[4,1,64,128]{3,2,1,0:T(8...) while((s32[]{:T(128)}, f32[1,128,128]{2,1,0:T(8,128)S(1)}, ...), condition=%wide.region_11.12_spmd, body=%wide.region_10.11_spmd.sunk | while | flops 7397378 | bytes 510085 | solution.py:262
  201.9 1.5 fusion.90
  204.1 27.8 %all-to-all-start.1 = ((bf16[8,32,256]{2,1,0:T(8,128)(2,1)}), bf16[8,32,256]{2,1,0:T(8,128)(2,1)S(1)}, u32[]{:S(2)}, u32[]{:S(2)}) async-start(bf16[8,32,256]{2,1,0:T(8,128)(2,1)} %pad_maximum_fusion.1), calls=%async_computation.1 | async-start | bytes 262144 | tf_op jit(solution)/shard_map/all_to_all | solution.py:274
  231.9 6.0 %fusion.129 = (bf16[1024,2048]{1,0:T(8,128)(2,1)}, bf16[1024,2048]{1,0:T(8,128)(2,1)}) fusion(bf16[1024,4096]{1,0:T(8,128)(2,1)} %all-gather.7.cloned.1.call-done), kind=kLoop, calls=%fused_computation.205 | loop fusion | bytes 16777216 | tf_op jit(solution)/shard_map/split | solution.py:73
  237.9 3.0 %fusion.98 = f32[8,32,2048]{2,1,0:T(8,128)S(1)} fusion(bf16[8,128,2048]{2,1,0:T(8,128)(2,1)} %bitcast.262, bf16[8,32,256]{2,1,0:T(8,128)(2,1)S(1)} %all-to-all-done.1), kind=kOutput, calls=%fused_computation.129 | convolution fusion | flops 134217728 | bytes 6356992 | tf_op jit(solution)/shard_map/jrp,jpd->jrd/dot_general | solution.py:278
  (135 shorter events, 27.4 us)
Async XLA Ops:
  6.5 195.1 %copy-start = (bf16[1,128,128]{2,1,0:T(8,128)(2,1)S(1)}, bf16[1,128,128]{2,1,0:T(8,128)(2,1)}, u32[]{:S(2)}) copy-start(bf16[1,128,128]{2,1,0:T(8,128)(2,1)} %param.35) | copy-start | bytes 98308
  6.5 19.9 %copy-start.6 = (bf16[2048]{0:T(1024)(128)(2,1)S(1)}, bf16[2048]{0:T(1024)(128)(2,1)}, u32[]{:S(2)}) copy-start(bf16[2048]{0:T(1024)(128)(2,1)} %param.24) | copy-start | bytes 12292
  6.5 90.9 %all-gather.5.cloned.1.call-start = ((), (), s32[]{:S(2)}) async-start(), calls=%async_computation.2 | async-start | bytes 3899392 | tf_op jit(solution)/shard_map/all_gather | solution.py:17
  12.5 0.7 copy-start.2
  15.3 84.7 %copy-start.5 = (f32[3,4,128]{2,1,0:T(4,128)S(1)}, f32[3,4,128]{2,1,0:T(4,128)}, u32[]{:S(2)}) copy-start(f32[3,4,128]{2,1,0:T(4,128)} %param.32) | copy-start | bytes 18436
  15.3 84.9 %all-to-all-start = ((bf16[8,32,2048]{2,1,0:T(8,128)(2,1)}), bf16[8,32,2048]{2,1,0:T(8,128)(2,1)S(1)}, u32[]{:S(2)}, u32[]{:S(2)}) async-start(bf16[8,32,2048]{2,1,0:T(8,128)(2,1)} %broadcast_in_dim.91), calls=%async_computation | async-start | bytes 2097152 | tf_op jit(solution)/shard_map/all_to_all | solution.py:27
  25.7 206.2 %all-gather.7.cloned.1.call-start = ((), (), s32[]{:S(2)}) async-start(), calls=%async_computation.3 | async-start | bytes 9437184 | tf_op jit(solution)/shard_map/all_gather | solution.py:73
  98.8 2.1 copy-start.3
  98.8 2.1 copy-start.4
  98.8 2.4 copy-start.7
  107.8 4.2 %collective-permute-start = (bf16[15,512]{1,0:T(8,128)(2,1)S(1)}, bf16[15,512]{1,0:T(8,128)(2,1)S(1)}, u32[]{:S(2)}, u32[]{:S(2)}) collective-permute-start(bf16[15,512]{1,0:T(8,128)(2,1)S(1)} %fusion.115), channel_id=1, source_target_pairs={{0,32},{32,64},{64,96},{96,128},{128,160},{160,192},{192,224},{224... | collective-permute-start | bytes 46088 | tf_op jit(solution)/shard_map/ppermute | solution.py:44
  169.9 31.9 %copy-start.8 = (f32[128]{0:T(128)S(1)}, f32[128]{0:T(128)}, u32[]{:S(2)}) copy-start(f32[128]{0:T(128)} %param.36) | copy-start | bytes 1540
  169.9 32.0 %copy-start.9 = (f32[128]{0:T(128)S(1)}, f32[128]{0:T(128)}, u32[]{:S(2)}) copy-start(f32[128]{0:T(128)} %param.37) | copy-start | bytes 1540
  204.1 33.9 %all-to-all-start.1 = ((bf16[8,32,256]{2,1,0:T(8,128)(2,1)}), bf16[8,32,256]{2,1,0:T(8,128)(2,1)S(1)}, u32[]{:S(2)}, u32[]{:S(2)}) async-start(bf16[8,32,256]{2,1,0:T(8,128)(2,1)} %pad_maximum_fusion.1), calls=%async_computation.1 | async-start | bytes 262144 | tf_op jit(solution)/shard_map/all_to_all | solution.py:274
  237.9 3.5 %copy-start.1 = (bf16[1024,2048]{1,0:T(8,128)(2,1)S(1)}, bf16[1024,2048]{1,0:T(8,128)(2,1)}, u32[]{:S(2)}) copy-start(bf16[1024,2048]{1,0:T(8,128)(2,1)} %get-tuple-element.294) | copy-start | bytes 12582916
Sparse Core Ops, SparseCore 0:
  13.4 84.0 all-gather.4
  100.0 65.0 all-gather.6
where the time goes:
time: 251 us; the launch traced here: 250 us
  waiting for transfers between devices  71.7 us (29%)
  blocking collectives  50.2 us (20%)
  starting transfers between devices  41.6 us (17%)
  matrix products  24.9 us (10%)
  other arithmetic  24.6 us (10%)
  local copies, waits for them, and re-layouts  22.1 us (9%)
  between operations  14.5 us (6%)
    all_gather x1, waiting for transfers between devices, turned_gather(): out, at, finished = (lax.all_gather(both, axis, axis=0, tiled=True), 0, [])  71 us
    all_gather x2, blocking collectives, entering(): lax.all_gather(a.astype(kind), axis)  50.2 us
    all_to_all x1, starting transfers between devices, per_device(): lax.all_to_all(both, 'tp', split_axis=0, concat_axis=0, tiled=True)  27.8 us
    another operation x1, other arithmetic, block_terms(): lax.linalg.triangular_solve(identity + corr_lower, jnp.broadcast_to(ident...  19.7 us
    all_to_all x1, starting transfers between devices, copy_for_each(): return lax.all_to_all(copies, axis, split_axis=0, concat_axis=0, tiled=True)  10.4 us
    dot_general x5, matrix products, project(): jnp.dot(norm_result, weight, preferred_element_type=jnp.float32)  7.41 us
    unnamed x31, local copies, waits for them, and re-layouts  6.34 us
    split x1, local copies, waits for them, and re-layouts, side_by_side(): jnp.split(lax.all_gather(both, axis, axis=dim, tiled=True), ends, axis=al...  6.02 us
  transfers between devices with their start and end apart: 5, of which 2 were waited for; matrix products, arithmetic and copies ran while one was open for 24% of the time, Pallas kernels for 0%

commit v1 on v0

v1 whole, which is shorter than its diff:
```python
import functools

import jax
import jax.numpy as jnp
from jax import lax
from jax.experimental import pallas as pl
from jax.experimental.pallas import tpu as pltpu
from jax.sharding import PartitionSpec as P

EPS = 1e-06
HALO = 16
F32 = jnp.float32
BF16 = jnp.bfloat16


def call(kernel, outs, *args, smem=0, scratch=(), flops=0):
    in_specs = [pl.BlockSpec(memory_space=pltpu.SMEM)] * smem + [
        pl.BlockSpec(memory_space=pltpu.VMEM)
    ] * (len(args) - smem)
    many = isinstance(outs, (list, tuple))
    out_specs = pl.BlockSpec(memory_space=pltpu.VMEM)
    return pl.pallas_call(
        kernel,
        out_shape=list(outs) if many else outs,
        in_specs=in_specs,
        out_specs=[out_specs] * len(outs) if many else out_specs,
        scratch_shapes=list(scratch),
        cost_estimate=pl.CostEstimate(flops=flops, bytes_accessed=0, transcendentals=0),
        name=kernel.__name__ if hasattr(kernel, "__name__") else kernel.func.__name__,
    )(*args)


def shape(*dims, dtype=F32):
    return jax.ShapeDtypeStruct(dims, dtype)


def dot(a, b, dims=((1,), (0,))):
    return lax.dot_general(a, b, (dims, ((), ())), preferred_element_type=F32)


def split(a):
    high = a.astype(BF16)
    return high, (a - high.astype(F32)).astype(BF16)


def dot3(a, b, dims=((1,), (0,))):
    ah, al = split(a)
    bh, bl = split(b)
    return dot(ah, bh, dims) + (dot(ah, bl, dims) + dot(al, bh, dims))


def pack_first(f_ref, a_ref, b_ref, out_ref):
    half = a_ref.shape[0] // 2
    rows = pl.ds(pl.multiple_of((f_ref[0] % 2) * half, half), half)
    piece = jnp.where(f_ref[0] < 2, a_ref[rows, :], b_ref[rows, :])
    for i in range(out_ref.shape[0]):
        out_ref[i] = piece


def pack_rest(f_ref, q_ref, g_ref, p_ref, op_ref, od_ref, qg_ref, poo_ref, stacked):
    pack_first(f_ref, q_ref, g_ref, qg_ref)
    n = p_ref.shape[0]
    stacked[0:n] = p_ref[...]
    stacked[n : 2 * n] = op_ref[...]
    stacked[2 * n : 3 * n] = od_ref[...]
    part = 3 * n // 4
    piece = stacked[pl.ds(pl.multiple_of(f_ref[0] * part, 32), part), :]
    for i in range(poo_ref.shape[0]):
        poo_ref[i] = piece


def everyone(x, axis):
    return jnp.broadcast_to(x, (lax.axis_size(axis), *x.shape))


def exchange(copies, axis, groups=None):
    return lax.all_to_all(
        copies, axis, split_axis=0, concat_axis=0, tiled=True, axis_index_groups=groups
    )


def norm_kernel(
    ids_ref, a_log_ref, tok_ref, tail_ref, gain_ref, wbd_ref, extra_ref,
    xn_ref, beta_ref, gc_ref, decay_ref,
):
    length = tok_ref.shape[0]
    gain = gain_ref[...].astype(F32)

    def rms(rows):
        x = rows.astype(F32)
        scale = lax.rsqrt(jnp.mean(x * x, axis=-1, keepdims=True) + EPS)
        return (x * scale * gain).astype(BF16)

    tail = rms(tail_ref[...])
    xn_ref[0:HALO] = jnp.where(ids_ref[0] > 0, tail, jnp.zeros_like(tail))
    step = 64
    for i in range(length // step):
        xn_ref[HALO + i * step : HALO + (i + 1) * step] = rms(tok_ref[i * step : (i + 1) * step])
    pre = dot(xn_ref[HALO:], wbd_ref[...], ((1,), (1,)))
    heads = pre.shape[1] // 2
    col = lax.broadcasted_iota(jnp.int32, pre.shape, 1)
    lane = ids_ref[1]
    beta_pre = jnp.sum(jnp.where(col == lane, pre, 0.0), axis=1, keepdims=True)
    decay_pre = jnp.sum(jnp.where(col == lane + heads, pre, 0.0), axis=1, keepdims=True)
    wide = (length, 128)
    beta_ref[...] = jax.nn.sigmoid(jnp.broadcast_to(beta_pre, wide))
    rate = jnp.exp(jnp.full(wide, a_log_ref[0], F32))
    soft = jax.nn.softplus(jnp.broadcast_to(decay_pre, wide))
    log_gate = -rate * soft + jnp.broadcast_to(extra_ref[...], wide)
    r = lax.broadcasted_iota(jnp.int32, (length, length), 0)
    c = lax.broadcasted_iota(jnp.int32, (length, length), 1)
    lower = jnp.where(r >= c, 1.0, 0.0).astype(BF16)
    g1 = log_gate.astype(BF16)
    rest = log_gate - g1.astype(F32)
    g2 = rest.astype(BF16)
    g3 = (rest - g2.astype(F32)).astype(BF16)
    gc = dot(lower, g1) + (dot(lower, g2) + dot(lower, g3))
    gc_ref[...] = gc
    across = jnp.transpose(gc)
    across = jnp.concatenate([across] * (length // 128), axis=0)
    along = jnp.concatenate([gc] * (length // 128), axis=1)
    gaps = along - across
    decay_ref[...] = jnp.where(r >= c, jnp.exp(jnp.where(r >= c, gaps, 0.0)), 0.0)


def gather_two(w_ref, w_scr):
    _, count, half, width = w_ref.shape
    for m in range(2):
        for s in range(count):
            for h in range(2):
                at = (2 * s + h) * half
                w_scr[at : at + half, m * width : (m + 1) * width] = w_ref[2 * m + h, s]


def short_conv(raw, taps, length, x_scr):
    x_scr[...] = raw.astype(BF16).astype(F32)
    conv = jnp.zeros((length, raw.shape[1]), F32)
    for j in range(4):
        conv = conv + x_scr[HALO - 3 + j : HALO - 3 + j + length, :] * taps[j : j + 1, :]
    return jax.nn.silu(conv)


def unit_rows(x):
    return x * lax.rsqrt(jnp.sum(x * x, axis=-1, keepdims=True) + EPS)


def inverse_unit_lower(low, size):
    r = lax.broadcasted_iota(jnp.int32, (size, size), 0)
    c = lax.broadcasted_iota(jnp.int32, (size, size), 1)
    inv = [jnp.where(r == c, 1.0, 0.0) - jnp.where((r // 2 == c // 2) & (r > c), x, 0.0) for x in low]
    b = 2
    while b < size:
        mask = (r // (2 * b) == c // (2 * b)) & (r % (2 * b) >= b) & (c % (2 * b) < b)
        mid = [dot3(x, jnp.where(mask, y, 0.0)) for x, y in zip(inv, low)]
        inv = [x - dot3(y, x) for x, y in zip(inv, mid)]
        b *= 2
    return inv


def local_kernel(
    xn_ref, w_ref, taps_ref, beta_ref, gc_ref, decay_ref,
    ab_ref, k_ref, uw_ref,
    w_scr, k_scr, v_scr,
):
    length, width = k_ref.shape
    gather_two(w_ref, w_scr)
    raw = dot(xn_ref[...], w_scr[...])
    keys = unit_rows(short_conv(raw[:, :width], taps_ref[0], length, k_scr))
    values = short_conv(raw[:, width:], taps_ref[1], length, v_scr)
    k_ref[...] = keys
    beta = beta_ref[...]
    gc = gc_ref[...]
    kb = keys * beta
    r = lax.broadcasted_iota(jnp.int32, (length, length), 0)
    c = lax.broadcasted_iota(jnp.int32, (length, length), 1)
    corr = jnp.where(r > c, dot3(kb, keys, ((1,), (1,))) * decay_ref[...], 0.0)
    half = length // 2
    first, second = inverse_unit_lower(
        [corr[:half, :half], corr[half:, half:]], half
    )
    rhs = jnp.concatenate([values * beta, kb * jnp.exp(gc)], axis=1)
    top = dot3(first, rhs[:half])
    bottom = dot3(second, rhs[half:] - dot3(corr[half:, :half], top))
    uw_ref[0:half] = top
    uw_ref[half:] = bottom
    last = gc[length - 1 : length, :]
    kd = keys * jnp.exp(last - gc)
    made = dot3(kd, uw_ref[...], ((0,), (0,)))
    ri = lax.broadcasted_iota(jnp.int32, (width, width), 0)
    ci = lax.broadcasted_iota(jnp.int32, (width, width), 1)
    linear = jnp.where(ri == ci, jnp.exp(last), 0.0) - made[:, width:]
    ab_ref[:, :width] = linear.astype(BF16)
    ab_ref[:, width:] = made[:, :width].astype(BF16)


def query_kernel(
    xn_ref, w_ref, taps_ref, gc_ref, decay_ref, k_ref, uw_ref,
    own_ref, eff_ref, silu_ref,
    w_scr, q_scr,
):
    length, width = k_ref.shape
    gather_two(w_ref, w_scr)
    raw = dot(xn_ref[...], w_scr[...])
    query = unit_rows(short_conv(raw[:, :width], taps_ref[0], length, q_scr)) * width ** (-0.5)
    silu_ref[...] = jax.nn.silu(raw[HALO:, width:].astype(BF16).astype(F32))
    scores = dot3(query, k_ref[...], ((1,), (1,))) * decay_ref[...]
    both = dot3(scores, uw_ref[...])
    own_ref[...] = both[:, :width]
    eff_ref[...] = query * jnp.exp(gc_ref[...]) - both[:, width:]


def pool_kernel(
    ids_ref, xn_ref, w_ref, mix_ref, scale_ref, out_ref, wo_ref, w_scr, a_scr, b_scr
):
    _, count, part, width = w_ref.shape
    length = xn_ref.shape[0] - HALO
    for s in range(count):
        at = s * width
        w_scr[at : at + 96, :] = w_ref[0, s]
        w_scr[at + 96 : at + 128, :] = w_ref[1, s, 0:32]
        wo_ref[0:64, at : at + width] = w_ref[1, s, 32:96]
        wo_ref[64:128, at : at + width] = w_ref[2, s, 0:64]
        wo_ref[128:160, at : at + width] = w_ref[2, s, 64:96]
        wo_ref[160:256, at : at + width] = w_ref[3, s]
    x = dot(xn_ref[...], w_scr[...]).astype(BF16).astype(F32)
    kind = ids_ref[1] % 4
    total = HALO + length
    a_scr[0:HALO] = jnp.zeros((HALO, width), F32)
    b_scr[0:HALO] = jnp.zeros((HALO, width), F32)
    a_scr[HALO:] = x
    two = x + a_scr[HALO - 1 : HALO - 1 + total]
    b_scr[HALO:] = two
    four = two + b_scr[HALO - 2 : HALO - 2 + total]
    a_scr[HALO:] = four
    eight = four + a_scr[HALO - 4 : HALO - 4 + total]
    b_scr[HALO:] = eight
    sixteen = eight + b_scr[HALO - 8 : HALO - 8 + total]
    window = jnp.where(kind == 0, two, jnp.where(kind == 1, four, jnp.where(kind == 2, eight, sixteen)))
    window = window[HALO:]
    place = ids_ref[0] * length + lax.broadcasted_iota(jnp.int32, (length, width), 0)
    span = jnp.where(kind == 0, 2, jnp.where(kind == 1, 4, jnp.where(kind == 2, 8, 16)))
    counts = jnp.minimum(place + 1, span).astype(F32)
    pooled = (window / counts - x[HALO:]).astype(BF16)
    out_ref[...] = (dot(pooled, mix_ref[...]) * scale_ref[...]).astype(BF16)


def step_map(later, carry, width):
    ch, cl = split(carry)
    linear = later[:, :width]
    moved = dot(linear, ch) + dot(linear, cl)
    offset = later[:, width:].astype(F32)
    return jnp.concatenate([moved[:, :width], moved[:, width:] + offset], axis=1)


def group_kernel(ids_ref, maps_ref, total_ref, before_ref):
    count, width, _ = maps_ref.shape
    place = ids_ref[0] % count
    r = lax.broadcasted_iota(jnp.int32, (width, width), 0)
    c = lax.broadcasted_iota(jnp.int32, (width, width), 1)
    eye = jnp.where(r == c, 1.0, 0.0)
    carry = jnp.concatenate([eye, jnp.zeros((width, width), F32)], axis=1)
    before = carry
    carry = maps_ref[0].astype(F32)
    for i in range(1, count):
        before = jnp.where(place == i, carry, before)
        carry = step_map(maps_ref[i], carry, width)
    before_ref[...] = before
    total_ref[...] = carry.astype(BF16)


def final_kernel(
    ids_ref, maps_ref, before_ref, own_ref, eff_ref, silu_ref, gain_ref, pool_ref, wo_ref, out_ref
):
    count, width, _ = maps_ref.shape
    group = ids_ref[0] // count
    state = jnp.where(group > 0, maps_ref[0, :, width:].astype(F32), 0.0)
    for i in range(1, count - 1):
        sh, sl = split(state)
        linear = maps_ref[i, :, :width]
        later = dot(linear, sh) + dot(linear, sl) + maps_ref[i, :, width:].astype(F32)
        state = jnp.where(group > i, later, state)
    state = dot3(before_ref[:, :width], state) + before_ref[:, width:]
    attended = own_ref[...] + dot3(eff_ref[...], state)
    scale = lax.rsqrt(jnp.mean(attended * attended, axis=-1, keepdims=True) + EPS)
    delta = (attended * scale * gain_ref[...] * silu_ref[...]).astype(BF16)
    both = jnp.concatenate([pool_ref[...], delta], axis=1)
    groups, rows, cols = out_ref.shape
    step = 512
    for at in range(0, cols, step):
        part = dot(both, wo_ref[:, at : at + step]).astype(BF16)
        for j in range(groups):
            out_ref[j, :, at : at + step] = part[j * rows : (j + 1) * rows]


def sum_kernel(in_ref, out_ref):
    total = in_ref[0].astype(F32)
    for j in range(1, in_ref.shape[0]):
        total = total + in_ref[j].astype(F32)
    out_ref[...] = total.astype(BF16)


def per_device(
    tokens,
    norm_gain,
    w_pool_in,
    w_query,
    w_key,
    w_value,
    w_gate,
    w_beta,
    w_decay,
    conv_weight,
    a_log,
    decay_extra,
    w_mix,
    pool_scale,
    delta_gain,
    w_out_pool,
    w_out_delta,
):
    n_sp = lax.axis_size("sp")
    n_tp = lax.axis_size("tp")
    sp_id = lax.axis_index("sp").astype(jnp.int32)
    tp_id = lax.axis_index("tp").astype(jnp.int32)
    fs_id = lax.axis_index("fs").astype(jnp.int32)
    ids = jnp.stack([sp_id, tp_id])
    f = fs_id[None]
    depth, width = w_key.shape
    rows, model = tokens.shape
    length = rows * n_tp
    half = depth // 2

    kv_copies = call(pack_first, shape(n_sp, half, width, dtype=BF16), f, w_key, w_value, smem=1)
    kv_part = exchange(kv_copies, "sp")
    all_rows = exchange(everyone(tokens, "tp"), "tp").reshape(length, model)
    qg_copies, poo_copies = call(
        pack_rest,
        (shape(n_sp, half, width, dtype=BF16), shape(n_sp, 3 * depth // 4, width, dtype=BF16)),
        f, w_query, w_gate, w_pool_in, w_out_pool, w_out_delta,
        smem=1, scratch=[pltpu.VMEM((3 * depth, width), BF16)],
    )
    tail = lax.ppermute(
        all_rows[length - HALO :], "sp", [(i, i + 1) for i in range(n_sp - 1)]
    )
    kv = exchange(everyone(kv_part, "fs"), "fs").reshape(4, n_sp, half, width)
    qg_copies, poo_copies, _ = lax.optimization_barrier((qg_copies, poo_copies, kv_part))
    qg_part = exchange(qg_copies, "sp")
    qg = exchange(everyone(qg_part, "fs"), "fs").reshape(4, n_sp, half, width)
    poo_part = exchange(poo_copies, "sp")
    poo = exchange(everyone(poo_part, "fs"), "fs").reshape(4, n_sp, 3 * depth // 4, width)

    wbd = jnp.concatenate([w_beta.T, w_decay.T], axis=0)
    xn, beta, gc, decay = call(
        norm_kernel,
        (
            shape(HALO + length, model, dtype=BF16),
            shape(length, 128),
            shape(length, 128),
            shape(length, length),
        ),
        ids, a_log, all_rows, tail, norm_gain.reshape(1, model), wbd, decay_extra,
        smem=2, flops=2 * length * model * 128,
    )
    ab, keys, uw = call(
        local_kernel,
        (shape(width, 2 * width, dtype=BF16), shape(length, width), shape(length, 2 * width)),
        xn, kv, conv_weight[1:], beta, gc, decay,
        scratch=[
            pltpu.VMEM((model, 2 * width), BF16),
            pltpu.VMEM((HALO + length, width), F32),
            pltpu.VMEM((HALO + length, width), F32),
        ],
        flops=20 * length * model * width,
    )
    quad = 4
    near = [[quad * g + r for r in range(quad)] for g in range(n_sp // quad)]
    far = [[quad * g + r for g in range(n_sp // quad)] for r in range(quad)]
    near_maps = exchange(jnp.broadcast_to(ab, (quad, *ab.shape)), "sp", near)
    total, before = call(
        group_kernel,
        (shape(width, 2 * width, dtype=BF16), shape(width, 2 * width)),
        ids, near_maps,
        smem=1, flops=20 * width**3,
    )
    far_maps = lax.all_gather(total, "sp", axis=0, axis_index_groups=far)

    own, eff, silu_gate = call(
        query_kernel,
        (shape(length, width), shape(length, width), shape(length, width)),
        xn, qg, conv_weight[:1], gc, decay, keys, uw,
        scratch=[
            pltpu.VMEM((model, 2 * width), BF16),
            pltpu.VMEM((HALO + length, width), F32),
        ],
        flops=8 * length * model * width,
    )
    pool_out, w_out = call(
        pool_kernel,
        (shape(length, width, dtype=BF16), shape(2 * width, model, dtype=BF16)),
        ids, xn, poo, w_mix[0], pool_scale.reshape(1, width),
        smem=1,
        scratch=[
            pltpu.VMEM((model, width), BF16),
            pltpu.VMEM((2 * HALO + length, width), F32),
            pltpu.VMEM((2 * HALO + length, width), F32),
        ],
        flops=4 * length * model * width,
    )
    partial = call(
        final_kernel,
        shape(n_tp, rows, model, dtype=BF16),
        ids, far_maps, before, own, eff, silu_gate, delta_gain.reshape(1, width), pool_out, w_out,
        smem=1, flops=4 * length * model * width,
    )
    arrived = exchange(partial, "tp")
    return call(sum_kernel, shape(rows, model, dtype=BF16), arrived, flops=1000000)


def solution(mesh):
    placed = (
        P(("fs", "sp", "tp"), None),
        P(),
        P("sp", "tp"),
        P("sp", "tp"),
        P("sp", "tp"),
        P("sp", "tp"),
        P("sp", "tp"),
        P(),
        P(),
        P(None, None, "tp"),
        P("tp"),
        P(("fs", "sp"), "tp"),
        P("tp", None, None),
        P("tp"),
        P(),
        P("tp", "sp"),
        P("tp", "sp"),
    )
    return jax.shard_map(
        per_device,
        mesh=mesh,
        in_specs=placed,
        out_specs=P(("fs", "sp", "tp"), None),
        check_vma=False,
    )
```

time: 251 us -> 230 us (0.916)
  blocking collectives: 50.2 us -> 129 us
  waiting for transfers between devices: 71.7 us -> 27.4 us
  Pallas kernels: 0 us -> 28.2 us
  matrix products: 24.9 us -> 0 us
  other arithmetic: 24.6 us -> 1.21 us
  between operations: 14.5 us -> 0.75 us
  local copies, waits for them, and re-layouts: 22.1 us -> 10.1 us
  starting transfers between devices: 41.6 us -> 31.5 us
    all_to_all x0 -> x5, blocking collectives: none -> 107 us  [exchange(): lax.all_to_all(copies, axis, split_axis=0, concat_axis=0, tiled=True, axi...]
    all_gather x2 -> x0, waiting for transfers between devices: 71 us -> none  [the longest x1 71 us: turned_gather(): out, at, finished = (lax.all_gather(both, axis, axis=0, tiled=True), 0, [])]
    pallas_call x0 -> x9, Pallas kernels: none -> 28.2 us  [call(): pl.pallas_call(kernel, out_shape=list(outs) if many else outs, in_specs=i...]
    all_gather x2 -> x1, blocking collectives: 50.2 us -> 22.4 us  [per_device(): far_maps = lax.all_gather(total, 'sp', axis=0, axis_index_groups=far)]
    dot_general x37 -> x0, matrix products: 24.5 us -> none  [the longest x5 7.41 us: project(): jnp.dot(norm_result, weight, preferred_element_type=jnp.float32)]
    all_to_all x2 -> x4, waiting for transfers between devices: 0.01 us -> 21.5 us  [exchange(): lax.all_to_all(copies, axis, split_axis=0, concat_axis=0, tiled=True, axi...]
    another operation x6 -> x1, other arithmetic: 20.1 us -> 0.59 us  [per_device(): ids = jnp.stack([sp_id, tp_id])]
    all_to_all x2 -> x4, starting transfers between devices: 38.2 us -> 28.2 us  [exchange(): lax.all_to_all(copies, axis, split_axis=0, concat_axis=0, tiled=True, axi...]
  transfers between devices with their start and end apart: 5 -> 5, of which waited for: 2 -> 3; matrix products, arithmetic and copies ran while one was open for 24% -> 2% of each run, Pallas kernels for 0% -> 8%
where the time goes in v1:
time: 230 us; the launch traced here: 229 us
  blocking collectives  129 us (56%)
  starting transfers between devices  31.5 us (14%)
  Pallas kernels  28.2 us (12%)
  waiting for transfers between devices  27.4 us (12%)
  local copies, waits for them, and re-layouts  10.1 us (4%)
    all_to_all x5, blocking collectives, exchange(): lax.all_to_all(copies, axis, split_axis=0, concat_axis=0, tiled=True, axi...  107 us
    all_to_all x4, starting transfers between devices, exchange(): lax.all_to_all(copies, axis, split_axis=0, concat_axis=0, tiled=True, axi...  28.2 us
    pallas_call x9, Pallas kernels, call(): pl.pallas_call(kernel, out_shape=list(outs) if many else outs, in_specs=i...  28.2 us
    all_gather x1, blocking collectives, per_device(): far_maps = lax.all_gather(total, 'sp', axis=0, axis_index_groups=far)  22.4 us
    all_to_all x4, waiting for transfers between devices, exchange(): lax.all_to_all(copies, axis, split_axis=0, concat_axis=0, tiled=True, axi...  21.5 us
    ppermute x1, waiting for transfers between devices, per_device(): lax.ppermute(all_rows[length - HALO:], 'sp', [(i, i + 1) for i in range(n...  5.88 us
    broadcast_in_dim x4, local copies, waits for them, and re-layouts, everyone(): return jnp.broadcast_to(x, (lax.axis_size(axis), *x.shape))  4.89 us
  transfers between devices with their start and end apart: 5, of which 3 were waited for; matrix products, arithmetic and copies ran while one was open for 2% of the time, Pallas kernels for 8%

profile of v1, /device:TPU:1, one launch (start us, length us, event | category | flops | bytes accessed | tf_op | source)
XLA Modules:
  0.0 228.6 jit_solution(3784800947206981470)
XLA Ops:
  0.0 2.0 broadcast_in_dim.18
  2.0 10.3 %all-to-all-start = ((bf16[8,32,2048]{2,1,0:T(8,128)(2,1)}), bf16[8,32,2048]{2,1,0:T(8,128)(2,1)S(1)}, u32[]{:S(2)}, u32[]{:S(2)}) async-start(bf16[8,32,2048]{2,1,0:T(8,128)(2,1)} %broadcast_in_dim.18), calls=%async_computation | async-start | bytes 2097152 | tf_op jit(solution)/shard_map/all_to_all | solution.py:77
  12.3 1.5 pack_first.1
  13.8 13.5 %all-to-all-done = bf16[8,32,2048]{2,1,0:T(8,128)(2,1)S(1)} async-done(((bf16[8,32,2048]{2,1,0:T(8,128)(2,1)}), bf16[8,32,2048]{2,1,0:T(8,128)(2,1)S(1)}, u32[]{:S(2)}, u32[]{:S(2)}) %all-to-all-start) | async-done | bytes 1048608 | tf_op jit(solution)/shard_map/all_to_all | solution.py:77
  27.3 23.3 %all_to_all.45 = bf16[16,64,128]{2,1,0:T(8,128)(2,1)S(1)} all-to-all(bf16[16,64,128]{2,1,0:T(8,128)(2,1)} %pack_first.1), channel_id=1, replica_groups=mesh['sp'=16,'fs'=4,'tp'=8] {'sp'}, dimensions={0} | all-to-all | bytes 524288 | tf_op jit(solution)/shard_map/all_to_all | solution.py:77
  51.8 4.3 %all-to-all-start.2 = ((bf16[4,16,64,128]{3,2,1,0:T(8,128)(2,1)}), bf16[4,16,64,128]{3,2,1,0:T(8,128)(2,1)S(1)}, u32[]{:S(2)}, u32[]{:S(2)}) async-start(bf16[4,16,64,128]{3,2,1,0:T(8,128)(2,1)} %broadcast_in_dim.20), calls=%async_computation.2 | async-start | bytes 2097152 | tf_op jit(solution)/shard_map/all_to_all | solution.py:77
  56.2 1.7 pack_rest.1
  57.9 8.0 %all-to-all-done.2.w_ref = bf16[4,16,64,128]{3,2,1,0:T(8,128)(2,1)S(1)} async-done(((bf16[4,16,64,128]{3,2,1,0:T(8,128)(2,1)}), bf16[4,16,64,128]{3,2,1,0:T(8,128)(2,1)S(1)}, u32[]{:S(2)}, u32[]{:S(2)}) %all-to-all-start.2) | async-done | bytes 1048608 | tf_op jit(solution)/shard_map/all_to_all | solution.py:77
  65.9 28.3 %all_to_all.46 = bf16[16,64,128]{2,1,0:T(8,128)(2,1)S(1)} all-to-all(bf16[16,64,128]{2,1,0:T(8,128)(2,1)} %get-tuple-element.32), channel_id=1, replica_groups=mesh['sp'=16,'fs'=4,'tp'=8] {'sp'}, dimensions={0} | all-to-all | bytes 524288 | tf_op jit(solution)/shard_map/all_to_all | solution.py:77
  94.2 10.0 %all-to-all-start.6 = ((bf16[16,96,128]{2,1,0:T(8,128)(2,1)}), bf16[16,96,128]{2,1,0:T(8,128)(2,1)S(1)}, u32[]{:S(2)}, u32[]{:S(2)}) async-start(bf16[16,96,128]{2,1,0:T(8,128)(2,1)} %get-tuple-element.38), calls=%async_computation.6 | async-start | bytes 786432 | tf_op jit(solution)/shard_map/all_to_all | solution.py:77
  107.6 3.3 %collective-permute-start = (bf16[16,2048]{1,0:T(8,128)(2,1)S(1)}, bf16[16,2048]{1,0:T(8,128)(2,1)S(1)}, u32[]{:S(2)}, u32[]{:S(2)}) collective-permute-start(bf16[16,2048]{1,0:T(8,128)(2,1)S(1)} %slice.12), channel_id=1, source_target_pairs={{0,32},{32,64},{64,96},{96,128},{128,160},{160,192},{192,224},{224... | collective-permute-start | bytes 196616 | tf_op jit(solution)/shard_map/ppermute | solution.py:342
  111.4 5.9 %collective-permute-done.tail_ref = bf16[16,2048]{1,0:T(8,128)(2,1)S(1)} collective-permute-done((bf16[16,2048]{1,0:T(8,128)(2,1)S(1)}, bf16[16,2048]{1,0:T(8,128)(2,1)S(1)}, u32[]{:S(2)}, u32[]{:S(2)}) %collective-permute-start) | collective-permute-done | bytes 65568 | tf_op jit(solution)/shard_map/ppermute | solution.py:342
  117.9 3.4 %norm_kernel.1 = (bf16[272,2048]{1,0:T(8,128)(2,1)}, f32[256,128]{1,0:T(8,128)}, f32[256,128]{1,0:T(8,128)}, f32[256,256]{1,0:T(8,128)}) custom-call(s32[2]{0:T(128)} %pad_add_fusion.ids_ref, f32[1]{0:T(128)S(6)} %copy.19.a_log_ref, bf16[256,2048]{1,0:T(8,128)(2,1)} %bitcast.11, bf16[16,2048]{1,0:T(8,128)(2,1)} %copy-done.3, ...), custom_call_target="tpu_custom_call" | custom-call | flops 134217728 | tf_op jit(solution)/shard_map/norm_kernel/pallas_call | solution.py:22
  121.4 6.3 %local_kernel.1 = (bf16[128,256]{1,0:T(8,128)(2,1)}, f32[256,128]{1,0:T(8,128)}, f32[256,256]{1,0:T(8,128)}) custom-call(bf16[272,2048]{1,0:T(8,128)(2,1)} %get-tuple-element.23.xn_ref, bf16[4,16,64,128]{3,2,1,0:T(8,128)(2,1)} %copy-done.2, f32[2,4,128]{2,1,0:T(4,128)} %slice.10.taps_ref, f32[256,128]{1,0:T(8,128)} %get-tuple-element.24.beta_ref, ...), custom_call_target="tpu_custom_call" | custom-call | flops 1342177280 | tf_op jit(solution)/shard_map/local_kernel/pallas_call | solution.py:22
  128.5 16.0 %all_to_all.47.maps_ref = bf16[4,128,256]{2,1,0:T(8,128)(2,1)} all-to-all(bf16[4,128,256]{2,1,0:T(8,128)(2,1)S(1)} %broadcast_in_dim.21), channel_id=1, replica_groups={{0,32,64,96},{128,160,192,224},{256,288,320,352},{384,416,448,480},{1,3..., dimensions={0} | all-to-all | bytes 524288 | tf_op jit(solution)/shard_map/all_to_all | solution.py:77
  144.7 14.5 %all_to_all.48.w_ref = bf16[4,16,64,128]{3,2,1,0:T(8,128)(2,1)} all-to-all(bf16[4,16,64,128]{3,2,1,0:T(8,128)(2,1)S(1)} %broadcast_in_dim.22), channel_id=1, replica_groups=mesh['sp'=16,'fs'=4,'tp'=8] {'fs'}, dimensions={0} | all-to-all | bytes 2097152 | tf_op jit(solution)/shard_map/all_to_all | solution.py:77
  160.7 3.6 %all-to-all-start.7 = ((bf16[4,16,96,128]{3,2,1,0:T(8,128)(2,1)}), bf16[4,16,96,128]{3,2,1,0:T(8,128)(2,1)S(1)}, u32[]{:S(2)}, u32[]{:S(2)}) async-start(bf16[4,16,96,128]{3,2,1,0:T(8,128)(2,1)} %broadcast_in_dim.23), calls=%async_computation.7 | async-start | bytes 3145728 | tf_op jit(solution)/shard_map/all_to_all | solution.py:77
  164.8 2.1 group_kernel.1
  167.0 22.4 %all-gather = bf16[512,256]{1,0:T(8,128)(2,1)} all-gather(bf16[128,256]{1,0:T(8,128)(2,1)} %get-tuple-element.28), channel_id=2, replica_groups={{0,128,256,384},{32,160,288,416},{64,192,320,448},{96,224,352,480},{1,1..., dimensions={0}, use_global_device_ids=true | all-gather | bytes 327680 | tf_op jit(solution)/shard_map/all_gather | solution.py:385
  189.3 3.9 %query_kernel.1 = (f32[256,128]{1,0:T(8,128)}, f32[256,128]{1,0:T(8,128)}, f32[256,128]{1,0:T(8,128)}) custom-call(bf16[272,2048]{1,0:T(8,128)(2,1)} %get-tuple-element.23.xn_ref, bf16[4,16,64,128]{3,2,1,0:T(8,128)(2,1)} %all_to_all.48.w_ref, f32[1,4,128]{2,1,0:T(4,128)} %slice.11.taps_ref, f32[256,128]{1,0:T(8,128)} %get-tuple-element.25.gc_ref, ...), custom_call_target="tpu_custom_call" | custom-call | flops 536870912 | tf_op jit(solution)/shard_map/query_kernel/pallas_call | solution.py:22
  194.4 3.5 %pool_kernel.1 = (bf16[256,128]{1,0:T(8,128)(2,1)}, bf16[256,2048]{1,0:T(8,128)(2,1)}) custom-call(s32[2]{0:T(128)} %pad_add_fusion.ids_ref, bf16[272,2048]{1,0:T(8,128)(2,1)} %get-tuple-element.23.xn_ref, bf16[4,16,96,128]{3,2,1,0:T(8,128)(2,1)} %copy-done, bf16[128,128]{1,0:T(8,128)(2,1)} %bitcast.13, f32[1,128]{1,0:T(1,128)} %bitcast.16), custom_call_target="tpu_custom_call" | custom-call | flops 268435456 | tf_op jit(solution)/shard_map/pool_kernel/pallas_call | solution.py:22
  197.9 3.7 %final_kernel.1 = bf16[8,32,2048]{2,1,0:T(8,128)(2,1)} custom-call(s32[2]{0:T(128)} %pad_add_fusion.ids_ref, bf16[4,128,256]{2,1,0:T(8,128)(2,1)} %bitcast.12, f32[128,256]{1,0:T(8,128)} %get-tuple-element.29.before_ref, f32[256,128]{1,0:T(8,128)} %get-tuple-element.35.own_ref, f32[256,128]{1,0:T(8,128)} %get-tuple-element.36.eff_ref, ...), custom_call_target="tpu_custom_call" | custom-call | flops 268435456 | tf_op jit(solution)/shard_map/final_kernel/pallas_call | solution.py:22
  201.6 25.0 %all_to_all.49.in_ref = bf16[8,32,2048]{2,1,0:T(8,128)(2,1)} all-to-all(bf16[8,32,2048]{2,1,0:T(8,128)(2,1)} %final_kernel.1), channel_id=1, replica_groups=mesh['sp'=16,'fs'=4,'tp'=8] {'tp'}, dimensions={0} | all-to-all | bytes 2097152 | tf_op jit(solution)/shard_map/all_to_all | solution.py:77
  226.6 2.0 sum_kernel.1
  (31 shorter events, 9.3 us)
Async XLA Ops:
  2.0 25.3 %all-to-all-start = ((bf16[8,32,2048]{2,1,0:T(8,128)(2,1)}), bf16[8,32,2048]{2,1,0:T(8,128)(2,1)S(1)}, u32[]{:S(2)}, u32[]{:S(2)}) async-start(bf16[8,32,2048]{2,1,0:T(8,128)(2,1)} %broadcast_in_dim.18), calls=%async_computation | async-start | bytes 2097152 | tf_op jit(solution)/shard_map/all_to_all | solution.py:77
  27.3 80.3 %copy-start.1 = (bf16[8,32,2048]{2,1,0:T(8,128)(2,1)}, bf16[8,32,2048]{2,1,0:T(8,128)(2,1)S(1)}, u32[]{:S(2)}) copy-start(bf16[8,32,2048]{2,1,0:T(8,128)(2,1)S(1)} %all-to-all-done) | copy-start | bytes 3145732
  51.8 52.5 %copy-start.8 = (f32[256,1]{0,1:T(1,128)S(1)}, f32[256,1]{0,1:T(1,128)}, u32[]{:S(2)}) copy-start(f32[256,1]{0,1:T(1,128)} %param.28) | copy-start | bytes 3076
  51.8 53.3 %copy-start.7 = (bf16[2048]{0:T(1024)(128)(2,1)S(1)}, bf16[2048]{0:T(1024)(128)(2,1)}, u32[]{:S(2)}) copy-start(bf16[2048]{0:T(1024)(128)(2,1)} %param.18) | copy-start | bytes 12292
  51.8 54.5 %copy-start.6 = (f32[3,4,128]{2,1,0:T(4,128)S(1)}, f32[3,4,128]{2,1,0:T(4,128)}, u32[]{:S(2)}) copy-start(f32[3,4,128]{2,1,0:T(4,128)} %param.26) | copy-start | bytes 18436
  51.8 55.1 %copy-start.4 = (bf16[2048,8]{0,1:T(8,128)(2,1)S(1)}, bf16[2048,8]{0,1:T(8,128)(2,1)}, u32[]{:S(2)}) copy-start(bf16[2048,8]{0,1:T(8,128)(2,1)} %param.25) | copy-start | bytes 98308
  51.8 55.1 %copy-start.5 = (bf16[2048,8]{0,1:T(8,128)(2,1)S(1)}, bf16[2048,8]{0,1:T(8,128)(2,1)}, u32[]{:S(2)}) copy-start(bf16[2048,8]{0,1:T(8,128)(2,1)} %param.24) | copy-start | bytes 98308
  51.8 14.1 %all-to-all-start.2 = ((bf16[4,16,64,128]{3,2,1,0:T(8,128)(2,1)}), bf16[4,16,64,128]{3,2,1,0:T(8,128)(2,1)S(1)}, u32[]{:S(2)}, u32[]{:S(2)}) async-start(bf16[4,16,64,128]{3,2,1,0:T(8,128)(2,1)} %broadcast_in_dim.20), calls=%async_computation.2 | async-start | bytes 2097152 | tf_op jit(solution)/shard_map/all_to_all | solution.py:77
  65.9 55.5 %copy-start.2 = (bf16[4,16,64,128]{3,2,1,0:T(8,128)(2,1)}, bf16[4,16,64,128]{3,2,1,0:T(8,128)(2,1)S(1)}, u32[]{:S(2)}) copy-start(bf16[4,16,64,128]{3,2,1,0:T(8,128)(2,1)S(1)} %all-to-all-done.2.w_ref) | copy-start | bytes 3145732
  94.2 33.4 %all-to-all-start.6 = ((bf16[16,96,128]{2,1,0:T(8,128)(2,1)}), bf16[16,96,128]{2,1,0:T(8,128)(2,1)S(1)}, u32[]{:S(2)}, u32[]{:S(2)}) async-start(bf16[16,96,128]{2,1,0:T(8,128)(2,1)} %get-tuple-element.38), calls=%async_computation.6 | async-start | bytes 786432 | tf_op jit(solution)/shard_map/all_to_all | solution.py:77
  107.6 9.7 %collective-permute-start = (bf16[16,2048]{1,0:T(8,128)(2,1)S(1)}, bf16[16,2048]{1,0:T(8,128)(2,1)S(1)}, u32[]{:S(2)}, u32[]{:S(2)}) collective-permute-start(bf16[16,2048]{1,0:T(8,128)(2,1)S(1)} %slice.12), channel_id=1, source_target_pairs={{0,32},{32,64},{64,96},{96,128},{128,160},{160,192},{192,224},{224... | collective-permute-start | bytes 196616 | tf_op jit(solution)/shard_map/ppermute | solution.py:342
  117.3 0.6 copy-start.3
  160.7 32.5 %all-to-all-start.7 = ((bf16[4,16,96,128]{3,2,1,0:T(8,128)(2,1)}), bf16[4,16,96,128]{3,2,1,0:T(8,128)(2,1)S(1)}, u32[]{:S(2)}, u32[]{:S(2)}) async-start(bf16[4,16,96,128]{3,2,1,0:T(8,128)(2,1)} %broadcast_in_dim.23), calls=%async_computation.7 | async-start | bytes 3145728 | tf_op jit(solution)/shard_map/all_to_all | solution.py:77
  193.2 1.2 copy-start

commit v2 on v1

v2 whole, which is shorter than its diff:
```python
import jax
import jax.numpy as jnp
from jax import lax
from jax.experimental import pallas as pl
from jax.experimental.pallas import tpu as pltpu
from jax.sharding import PartitionSpec as P


EPS = 1e-06
HALO = 16
F32 = jnp.float32
BF16 = jnp.bfloat16


def call(kernel, outs, *args, smem=0, scratch=(), flops=0, vmem=16):
    in_specs = [pl.BlockSpec(memory_space=pltpu.SMEM)] * smem + [
        pl.BlockSpec(memory_space=pltpu.VMEM)
    ] * (len(args) - smem)
    many = isinstance(outs, (list, tuple))
    out_specs = pl.BlockSpec(memory_space=pltpu.VMEM)
    return pl.pallas_call(
        kernel,
        out_shape=list(outs) if many else outs,
        in_specs=in_specs,
        out_specs=[out_specs] * len(outs) if many else out_specs,
        scratch_shapes=list(scratch),
        compiler_params=pltpu.CompilerParams(vmem_limit_bytes=vmem and vmem * 1024 * 1024),
        cost_estimate=pl.CostEstimate(flops=flops, bytes_accessed=0, transcendentals=0),
    )(*args)


def shape(*dims, dtype=F32):
    return jax.ShapeDtypeStruct(dims, dtype)


def dot(a, b, dims=((1,), (0,))):
    return lax.dot_general(a, b, (dims, ((), ())), preferred_element_type=F32)


def split(a):
    high = a.astype(BF16)
    return high, (a - high.astype(F32)).astype(BF16)


def dot3(a, b, dims=((1,), (0,))):
    ah, al = split(a)
    bh, bl = split(b)
    return dot(ah, bh, dims) + (dot(ah, bl, dims) + dot(al, bh, dims))


def start_kernel(
    f_ref, tok_ref, gain_ref, k_ref, v_ref, q_ref, g_ref, p_ref, op_ref, od_ref,
    copies_ref, part_ref, stacked,
):
    x = tok_ref[...].astype(F32)
    scale = lax.rsqrt(jnp.mean(x * x, axis=-1, keepdims=True) + EPS)
    normed = (x * scale * gain_ref[...].astype(F32)).astype(BF16)
    for j in range(copies_ref.shape[0]):
        copies_ref[j] = normed
    f = f_ref[0]
    depth = k_ref.shape[0]
    half = depth // 2
    rows = pl.ds(pl.multiple_of((f % 2) * half, half), half)
    part_ref[0:half] = jnp.where(f < 2, k_ref[rows, :], v_ref[rows, :])
    part_ref[half:depth] = jnp.where(f < 2, q_ref[rows, :], g_ref[rows, :])
    stacked[0:depth] = p_ref[...]
    stacked[depth : 2 * depth] = op_ref[...]
    stacked[2 * depth :] = od_ref[...]
    third = 3 * depth // 4
    part_ref[depth:] = stacked[pl.ds(pl.multiple_of(f * third, 32), third), :]


def exchange(copies, axis, groups=None):
    return lax.all_to_all(
        copies, axis, split_axis=0, concat_axis=0, tiled=True, axis_index_groups=groups
    )


def turns(x, axis, size):
    n = lax.axis_size(axis)
    out = [x]
    for d in range(1, size):
        out.append(lax.ppermute(x, axis, [(i, i - i % size + (i + d) % size) for i in range(n)]))
    return out


def gate_kernel(
    ids_ref, a_log_ref, rows_ref, tail_ref, wbd_ref, extra_ref, xn_ref, beta_ref, gc_ref, decay_ref
):
    length = rows_ref.shape[0]
    tail = tail_ref[...]
    xn_ref[0:HALO] = jnp.where(ids_ref[0] > 0, tail, jnp.zeros_like(tail))
    xn_ref[HALO:] = rows_ref[...]
    pre = dot(rows_ref[...], wbd_ref[...], ((1,), (1,)))
    heads = pre.shape[1] // 2
    col = lax.broadcasted_iota(jnp.int32, pre.shape, 1)
    lane = ids_ref[1]
    beta_pre = jnp.sum(jnp.where(col == lane, pre, 0.0), axis=1, keepdims=True)
    decay_pre = jnp.sum(jnp.where(col == lane + heads, pre, 0.0), axis=1, keepdims=True)
    wide = (length, 128)
    beta_ref[...] = jax.nn.sigmoid(jnp.broadcast_to(beta_pre, wide))
    rate = jnp.exp(jnp.full(wide, a_log_ref[0], F32))
    soft = jax.nn.softplus(jnp.broadcast_to(decay_pre, wide))
    log_gate = -rate * soft + jnp.broadcast_to(extra_ref[...], wide)
    r = lax.broadcasted_iota(jnp.int32, (length, length), 0)
    c = lax.broadcasted_iota(jnp.int32, (length, length), 1)
    lower = jnp.where(r >= c, 1.0, 0.0).astype(BF16)
    g1 = log_gate.astype(BF16)
    rest = log_gate - g1.astype(F32)
    g2 = rest.astype(BF16)
    g3 = (rest - g2.astype(F32)).astype(BF16)
    gc = dot(lower, g1) + (dot(lower, g2) + dot(lower, g3))
    gc_ref[...] = gc
    across = jnp.transpose(gc)
    across = jnp.concatenate([across] * (length // 128), axis=0)
    along = jnp.concatenate([gc] * (length // 128), axis=1)
    gaps = along - across
    decay_ref[...] = jnp.where(r >= c, jnp.exp(jnp.where(r >= c, gaps, 0.0)), 0.0)


def gather_two(f, pieces, w_scr):
    count, _, width = pieces[0].shape
    half = width // 2
    for d, piece in enumerate(pieces):
        slot = (f + 4 - d) % 4
        cols = pl.ds(pl.multiple_of((slot // 2) * width, width), width)
        for s in range(count):
            at = pl.multiple_of((2 * s + slot % 2) * half, half)
            w_scr[pl.ds(at, half), cols] = piece[s, 0:half]


def short_conv(raw, taps, length, x_scr):
    x_scr[...] = raw.astype(BF16).astype(F32)
    conv = jnp.zeros((length, raw.shape[1]), F32)
    for j in range(4):
        conv = conv + x_scr[HALO - 3 + j : HALO - 3 + j + length, :] * taps[j : j + 1, :]
    return jax.nn.silu(conv)


def unit_rows(x):
    return x * lax.rsqrt(jnp.sum(x * x, axis=-1, keepdims=True) + EPS)


def inverse_unit_lower(low, size):
    r = lax.broadcasted_iota(jnp.int32, (size, size), 0)
    c = lax.broadcasted_iota(jnp.int32, (size, size), 1)
    inv = [jnp.where(r == c, 1.0, 0.0) - jnp.where((r // 2 == c // 2) & (r > c), x, 0.0) for x in low]
    b = 2
    while b < size:
        mask = (r // (2 * b) == c // (2 * b)) & (r % (2 * b) >= b) & (c % (2 * b) < b)
        mid = [dot3(x, jnp.where(mask, y, 0.0)) for x, y in zip(inv, low)]
        inv = [x - dot3(y, x) for x, y in zip(inv, mid)]
        b *= 2
    return inv


def local_kernel(
    xn_ref, w_ref, taps_ref, beta_ref, gc_ref, decay_ref,
    ab_ref, k_ref, uw_ref,
    w_scr, k_scr, v_scr,
):
    length, width = k_ref.shape
    count, half = w_ref.shape[1:3]
    for m in range(2):
        for h in range(2):
            for i in range(count):
                at = (2 * i + h) * half
                w_scr[at : at + half, m * width : (m + 1) * width] = w_ref[2 * m + h, i]
    raw = dot(xn_ref[...], w_scr[...])
    keys = unit_rows(short_conv(raw[:, :width], taps_ref[0], length, k_scr))
    values = short_conv(raw[:, width:], taps_ref[1], length, v_scr)
    k_ref[...] = keys
    beta = beta_ref[...]
    gc = gc_ref[...]
    kb = keys * beta
    r = lax.broadcasted_iota(jnp.int32, (length, length), 0)
    c = lax.broadcasted_iota(jnp.int32, (length, length), 1)
    corr = jnp.where(r > c, dot3(kb, keys, ((1,), (1,))) * decay_ref[...], 0.0)
    half = length // 2
    first, second = inverse_unit_lower(
        [corr[:half, :half], corr[half:, half:]], half
    )
    rhs = jnp.concatenate([values * beta, kb * jnp.exp(gc)], axis=1)
    top = dot3(first, rhs[:half])
    bottom = dot3(second, rhs[half:] - dot3(corr[half:, :half], top))
    uw_ref[0:half] = top
    uw_ref[half:] = bottom
    last = gc[length - 1 : length, :]
    kd = keys * jnp.exp(last - gc)
    made = dot3(kd, uw_ref[...], ((0,), (0,)))
    ri = lax.broadcasted_iota(jnp.int32, (width, width), 0)
    ci = lax.broadcasted_iota(jnp.int32, (width, width), 1)
    linear = jnp.where(ri == ci, jnp.exp(last), 0.0) - made[:, width:]
    ab_ref[:, :width] = linear.astype(BF16)
    ab_ref[:, width:] = made[:, :width].astype(BF16)


def query_kernel(
    ids_ref, xn_ref, w0_ref, w1_ref, w2_ref, w3_ref, taps_ref, gc_ref, decay_ref, k_ref, uw_ref,
    own_ref, eff_ref, silu_ref,
    w_scr, q_scr,
):
    length, width = k_ref.shape
    gather_two(ids_ref[2], (w0_ref, w1_ref, w2_ref, w3_ref), w_scr)
    raw = dot(xn_ref[...], w_scr[...])
    query = unit_rows(short_conv(raw[:, :width], taps_ref[0], length, q_scr)) * width ** (-0.5)
    silu_ref[...] = jax.nn.silu(raw[HALO:, width:].astype(BF16).astype(F32))
    scores = dot3(query, k_ref[...], ((1,), (1,))) * decay_ref[...]
    both = dot3(scores, uw_ref[...])
    own_ref[...] = both[:, :width]
    eff_ref[...] = query * jnp.exp(gc_ref[...]) - both[:, width:]


def pool_kernel(
    ids_ref, xn_ref, w0_ref, w1_ref, w2_ref, w3_ref, mix_ref, scale_ref,
    out_ref, wo_ref, w_all, w_scr, a_scr, b_scr,
):
    count, part, width = w0_ref.shape
    skip = width // 2
    part = part - skip
    length = xn_ref.shape[0] - HALO
    for d, piece in enumerate((w0_ref, w1_ref, w2_ref, w3_ref)):
        at = pl.multiple_of(((ids_ref[2] + 4 - d) % 4) * part, 32)
        for s in range(count):
            w_all[pl.ds(at, part), s * width : (s + 1) * width] = piece[s, skip:]
    for s in range(count):
        w_scr[s * width : (s + 1) * width, :] = w_all[0:width, s * width : (s + 1) * width]
    wo_ref[...] = w_all[width:, :]
    x = dot(xn_ref[...], w_scr[...]).astype(BF16).astype(F32)
    kind = ids_ref[1] % 4
    total = HALO + length
    a_scr[0:HALO] = jnp.zeros((HALO, width), F32)
    b_scr[0:HALO] = jnp.zeros((HALO, width), F32)
    a_scr[HALO:] = x
    two = x + a_scr[HALO - 1 : HALO - 1 + total]
    b_scr[HALO:] = two
    four = two + b_scr[HALO - 2 : HALO - 2 + total]
    a_scr[HALO:] = four
    eight = four + a_scr[HALO - 4 : HALO - 4 + total]
    b_scr[HALO:] = eight
    sixteen = eight + b_scr[HALO - 8 : HALO - 8 + total]
    window = jnp.where(kind == 0, two, jnp.where(kind == 1, four, jnp.where(kind == 2, eight, sixteen)))
    window = window[HALO:]
    place = ids_ref[0] * length + lax.broadcasted_iota(jnp.int32, (length, width), 0)
    span = jnp.where(kind == 0, 2, jnp.where(kind == 1, 4, jnp.where(kind == 2, 8, 16)))
    counts = jnp.minimum(place + 1, span).astype(F32)
    pooled = (window / counts - x[HALO:]).astype(BF16)
    out_ref[...] = (dot(pooled, mix_ref[...]) * scale_ref[...]).astype(BF16)


def step_map(later, carry, width):
    ch, cl = split(carry)
    linear = later[:, :width]
    moved = dot(linear, ch) + dot(linear, cl)
    offset = later[:, width:].astype(F32)
    return jnp.concatenate([moved[:, :width], moved[:, width:] + offset], axis=1)


def group_kernel(
    ids_ref, m0_ref, m1_ref, m2_ref, m3_ref, total_ref, linear_ref, offset_ref, before_ref, maps
):
    count, width, _ = maps.shape
    place = ids_ref[0] % count
    for d, piece in enumerate((m0_ref, m1_ref, m2_ref, m3_ref)):
        maps[(place + count - d) % count] = piece[...]
    r = lax.broadcasted_iota(jnp.int32, (width, width), 0)
    c = lax.broadcasted_iota(jnp.int32, (width, width), 1)
    eye = jnp.where(r == c, 1.0, 0.0)
    before = jnp.concatenate([eye, jnp.zeros((width, width), F32)], axis=1)
    carry = maps[0].astype(F32)
    for i in range(1, count):
        before = jnp.where(place == i, carry, before)
        carry = step_map(maps[i], carry, width)
    before_ref[...] = before
    total = carry.astype(BF16)
    total_ref[...] = total
    linear_ref[...] = total[:, :width]
    offset_ref[...] = total[:, width:]


def apply(linear, state):
    high, low = split(state)
    return dot(linear, high) + dot(linear, low)


def attend_kernel(
    ids_ref, t4_ref, a8_ref, b8_ref, b12_ref, before_ref, own_ref, eff_ref, silu_ref, gain_ref,
    pool_ref, mine_ref, other_ref,
):
    width = b8_ref.shape[0]
    state = apply(a8_ref[...], b12_ref[...].astype(F32)) + b8_ref[...].astype(F32)
    state = apply(t4_ref[:, :width], state) + t4_ref[:, width:].astype(F32)
    state = dot3(before_ref[:, :width], state) + before_ref[:, width:]
    attended = own_ref[...] + dot3(eff_ref[...], state)
    scale = lax.rsqrt(jnp.mean(attended * attended, axis=-1, keepdims=True) + EPS)
    delta = (attended * scale * gain_ref[...] * silu_ref[...]).astype(BF16)
    both = jnp.concatenate([pool_ref[...], delta], axis=1)
    core = ids_ref[1] % 2
    chips, rows = mine_ref.shape[:2]
    for j in range(chips):
        even = both[2 * j * rows : (2 * j + 1) * rows]
        odd = both[(2 * j + 1) * rows : (2 * j + 2) * rows]
        mine_ref[j] = jnp.where(core == 0, even, odd)
        other_ref[j] = jnp.where(core == 0, odd, even)


def out_kernel(mine_ref, theirs_ref, w_mine_ref, w_theirs_ref, out_ref):
    chips, rows, width = mine_ref.shape
    mine = mine_ref[...].reshape(chips * rows, width)
    theirs = theirs_ref[...].reshape(chips * rows, width)
    cols = out_ref.shape[2]
    step = 512
    for at in range(0, cols, step):
        part = dot(mine, w_mine_ref[:, at : at + step]) + dot(theirs, w_theirs_ref[:, at : at + step])
        out_ref[:, :, at : at + step] = part.astype(BF16).reshape(chips, rows, step)


def sum_kernel(in_ref, out_ref):
    total = in_ref[0].astype(F32)
    for j in range(1, in_ref.shape[0]):
        total = total + in_ref[j].astype(F32)
    out_ref[...] = total.astype(BF16)


def layer(
    tokens,
    norm_gain,
    w_pool_in,
    w_query,
    w_key,
    w_value,
    w_gate,
    w_beta,
    w_decay,
    conv_weight,
    a_log,
    decay_extra,
    w_mix,
    pool_scale,
    delta_gain,
    w_out_pool,
    w_out_delta,
):
    n_sp = lax.axis_size("sp")
    n_tp = lax.axis_size("tp")
    sp_id = lax.axis_index("sp").astype(jnp.int32)
    tp_id = lax.axis_index("tp").astype(jnp.int32)
    fs_id = lax.axis_index("fs").astype(jnp.int32)
    ids = jnp.stack([sp_id, tp_id, fs_id])
    depth, width = w_key.shape
    rows, model = tokens.shape
    length = rows * n_tp
    half = depth // 2

    copies, part = call(
        start_kernel,
        (shape(n_tp, rows, model, dtype=BF16), shape(7 * depth // 4, width, dtype=BF16)),
        fs_id[None], tokens, norm_gain.reshape(1, model),
        w_key, w_value, w_query, w_gate, w_pool_in, w_out_pool, w_out_delta,
        smem=1, scratch=[pltpu.VMEM((3 * depth, width), BF16)], vmem=None,
    )
    all_rows = exchange(copies, "tp").reshape(length, model)
    tail = lax.ppermute(
        all_rows[length - HALO :], "sp", [(i, i + 1) for i in range(n_sp - 1)]
    )
    quarters = lax.all_gather(part, "sp", axis=0)
    kv = exchange(
        jnp.broadcast_to(quarters[:, :half], (4, n_sp, half, width)), "fs"
    )
    kv = kv.reshape(4, n_sp, half, width)
    rest = turns(quarters[:, half:], "fs", 4)

    wbd = jnp.concatenate([w_beta.T, w_decay.T], axis=0)
    xn, beta, gc, decay = call(
        gate_kernel,
        (
            shape(HALO + length, model, dtype=BF16),
            shape(length, 128),
            shape(length, 128),
            shape(length, length),
        ),
        ids, a_log, all_rows, tail, wbd, decay_extra,
        smem=2, flops=2 * length * model * 128,
    )
    ab, keys, uw = call(
        local_kernel,
        (shape(width, 2 * width, dtype=BF16), shape(length, width), shape(length, 2 * width)),
        xn, kv, conv_weight[1:], beta, gc, decay,
        scratch=[
            pltpu.VMEM((model, 2 * width), BF16),
            pltpu.VMEM((HALO + length, width), F32),
            pltpu.VMEM((HALO + length, width), F32),
        ],
        flops=20 * length * model * width,
    )
    quad = 4
    near = turns(ab, "sp", quad)
    total, linear, offset, before = call(
        group_kernel,
        (
            shape(width, 2 * width, dtype=BF16),
            shape(width, width, dtype=BF16),
            shape(width, width, dtype=BF16),
            shape(width, 2 * width),
        ),
        ids, *near,
        smem=1, scratch=[pltpu.VMEM((quad, width, 2 * width), BF16)], flops=20 * width**3,
    )

    def from_behind(x, first, last, distance):
        return lax.ppermute(x, "sp", [(i, i + distance) for i in range(first, last)])

    t4 = from_behind(total, 0, n_sp - quad, quad)
    b8 = from_behind(offset, 0, n_sp - 2 * quad, 2 * quad)
    a8 = from_behind(linear, quad, n_sp - 2 * quad, 2 * quad)
    b12 = from_behind(offset, 0, n_sp - 3 * quad, 3 * quad)

    own, eff, silu_gate = call(
        query_kernel,
        (shape(length, width), shape(length, width), shape(length, width)),
        ids, xn, *rest, conv_weight[:1], gc, decay, keys, uw,
        smem=1,
        scratch=[
            pltpu.VMEM((model, 2 * width), BF16),
            pltpu.VMEM((HALO + length, width), F32),
        ],
        flops=8 * length * model * width,
    )
    pool_out, w_mine = call(
        pool_kernel,
        (shape(length, width, dtype=BF16), shape(2 * width, model, dtype=BF16)),
        ids, xn, *rest, w_mix[0], pool_scale.reshape(1, width),
        smem=1,
        scratch=[
            pltpu.VMEM((3 * width, model), BF16),
            pltpu.VMEM((model, width), BF16),
            pltpu.VMEM((2 * HALO + length, width), F32),
            pltpu.VMEM((2 * HALO + length, width), F32),
        ],
        flops=8 * length * model * width,
    )
    swap = [(i, i ^ 1) for i in range(n_tp)]
    w_theirs = lax.ppermute(w_mine, "tp", swap)
    chips = n_tp // 2
    mine, other = call(
        attend_kernel,
        (shape(chips, rows, 2 * width, dtype=BF16), shape(chips, rows, 2 * width, dtype=BF16)),
        ids, t4, a8, b8, b12, before, own, eff, silu_gate, delta_gain.reshape(1, width), pool_out,
        smem=1, flops=4 * length * model * width,
    )
    theirs = lax.ppermute(other, "tp", swap)
    partial = call(
        out_kernel,
        shape(chips, rows, model, dtype=BF16),
        mine, theirs, w_mine, w_theirs,
        flops=4 * length * model * width,
    )
    cores = [[2 * x + c for x in range(chips)] for c in range(2)]
    arrived = exchange(partial, "tp", cores)
    return call(sum_kernel, shape(rows, model, dtype=BF16), arrived, flops=1000000)


def solution(mesh):
    placed = (
        P(("fs", "sp", "tp"), None),
        P(),
        P("sp", "tp"),
        P("sp", "tp"),
        P("sp", "tp"),
        P("sp", "tp"),
        P("sp", "tp"),
        P(),
        P(),
        P(None, None, "tp"),
        P("tp"),
        P(("fs", "sp"), "tp"),
        P("tp", None, None),
        P("tp"),
        P(),
        P("tp", "sp"),
        P("tp", "sp"),
    )
    return jax.shard_map(
        layer,
        mesh=mesh,
        in_specs=placed,
        out_specs=P(("fs", "sp", "tp"), None),
        check_vma=False,
    )
```

time: 230 us -> 155 us (0.67)
  blocking collectives: 129 us -> 41.9 us
  starting transfers between devices: 31.5 us -> 71.6 us
  waiting for transfers between devices: 27.4 us -> 10.6 us
  Pallas kernels: 28.2 us -> 19.1 us
    all_to_all x5 -> x1, blocking collectives: 107 us -> 11.8 us  [exchange(): lax.all_to_all(copies, axis, split_axis=0, concat_axis=0, tiled=True, axi...]
    ppermute x1 -> x13, starting transfers between devices: 3.26 us -> 56.8 us  [the longest x6 19.2 us: turns(): lax.ppermute(x, axis, [(i, i - i % size + (i + d) % size) for i in range(...]
    all_to_all x4 -> x2, waiting for transfers between devices: 21.5 us -> 0.01 us  [exchange(): lax.all_to_all(copies, axis, split_axis=0, concat_axis=0, tiled=True, axi...]
    all_to_all x4 -> x2, starting transfers between devices: 28.2 us -> 14.8 us  [exchange(): lax.all_to_all(copies, axis, split_axis=0, concat_axis=0, tiled=True, axi...]
    pallas_call x9, Pallas kernels: 28.2 us -> 19.1 us  [call(): pl.pallas_call(kernel, out_shape=list(outs) if many else outs, in_specs=i...]
    all_gather x1, blocking collectives: 22.4 us -> 30.2 us  [layer(): quarters = lax.all_gather(part, 'sp', axis=0)]
    unnamed x19 -> x41, local copies, waits for them, and re-layouts: 2.6 us -> 7.34 us
    ppermute x1 -> x13, waiting for transfers between devices: 5.88 us -> 10.6 us  [the longest x6 9.68 us: turns(): lax.ppermute(x, axis, [(i, i - i % size + (i + d) % size) for i in range(...]
  transfers between devices with their start and end apart: 5 -> 15, of which waited for: 3 -> 4; matrix products, arithmetic and copies ran while one was open for 2% -> 1% of each run, Pallas kernels for 8% -> 9%
where the time goes in v2:
time: 155 us; the launch traced here: 154 us
  starting transfers between devices  71.6 us (46%)
  blocking collectives  41.9 us (27%)
  Pallas kernels  19.1 us (12%)
  waiting for transfers between devices  10.6 us (7%)
  local copies, waits for them, and re-layouts  9.93 us (6%)
    all_gather x1, blocking collectives, layer(): quarters = lax.all_gather(part, 'sp', axis=0)  30.2 us
    ppermute x6, starting transfers between devices, turns(): lax.ppermute(x, axis, [(i, i - i % size + (i + d) % size) for i in range(...  19.2 us
    pallas_call x9, Pallas kernels, call(): pl.pallas_call(kernel, out_shape=list(outs) if many else outs, in_specs=i...  19.1 us
    ppermute x1, starting transfers between devices, layer(): w_theirs = lax.ppermute(w_mine, 'tp', swap)  16 us
    all_to_all x2, starting transfers between devices, exchange(): lax.all_to_all(copies, axis, split_axis=0, concat_axis=0, tiled=True, axi...  14.8 us
    ppermute x4, starting transfers between devices, from_behind(): lax.ppermute(x, 'sp', [(i, i + distance) for i in range(first, last)])  14.3 us
    all_to_all x1, blocking collectives, exchange(): lax.all_to_all(copies, axis, split_axis=0, concat_axis=0, tiled=True, axi...  11.8 us
    ppermute x6, waiting for transfers between devices, turns(): lax.ppermute(x, axis, [(i, i - i % size + (i + d) % size) for i in range(...  9.68 us
  transfers between devices with their start and end apart: 15, of which 4 were waited for; matrix products, arithmetic and copies ran while one was open for 1% of the time, Pallas kernels for 9%

profile of v2, /device:TPU:1, one launch (start us, length us, event | category | flops | bytes accessed | tf_op | source)
XLA Modules:
  0.0 154.3 jit_solution(14789165647294854995)
XLA Ops:
  1.3 2.2 %shard_map.163 = (bf16[8,32,2048]{2,1,0:T(8,128)(2,1)}, bf16[224,128]{1,0:T(8,128)(2,1)}) custom-call(s32[1]{0:T(128)} %bitcast.2.f_ref, bf16[32,2048]{1,0:T(8,128)(2,1)} %tok_ref.1, bf16[1,2048]{1,0:T(2,128)(2,1)} %reshape.12.gain_ref, bf16[128,128]{1,0:T(8,128)(2,1)} %k_ref.1, bf16[128,128]{1,0:T(8,128)(2,1)} %v_ref.1, bf16[128,128]{1,0:T(8,128)(2,1)} %q_ref.1, ...), custom_call_target="tpu_custom_call" | custom-call | tf_op jit(solution)/shard_map/pallas_call | solution.py:21
  3.4 10.4 %all-to-all-start = ((bf16[8,32,2048]{2,1,0:T(8,128)(2,1)}), bf16[8,32,2048]{2,1,0:T(8,128)(2,1)S(1)}, u32[]{:S(2)}, u32[]{:S(2)}) async-start(bf16[8,32,2048]{2,1,0:T(8,128)(2,1)} %get-tuple-element.25), calls=%async_computation | async-start | bytes 2097152 | tf_op jit(solution)/shard_map/all_to_all | solution.py:74
  13.9 30.2 %all-gather = bf16[3584,128]{1,0:T(8,128)(2,1)S(1)} all-gather(bf16[224,128]{1,0:T(8,128)(2,1)S(1)} %copy-done.15), channel_id=2, replica_groups=mesh['sp'=16,'fs'=4,'tp'=8] {'sp'}, dimensions={0}, use_global_device_ids=true | all-gather | bytes 974848 | tf_op jit(solution)/shard_map/all_gather | solution.py:366
  44.1 4.7 %collective-permute-start.10 = (bf16[16,160,128]{2,1,0:T(8,128)(2,1)S(1)}, bf16[16,160,128]{2,1,0:T(8,128)(2,1)S(1)}, u32[]{:S(2)}, u32[]{:S(2)}) collective-permute-start(bf16[16,160,128]{2,1,0:T(8,128)(2,1)S(1)} %slice.22.w0_ref), channel_id=1, source_target_pairs={{0,24},{8,0},{16,8},{24,16},{1,25},{9,1},{17,9},{25,17},{2,26},{10... | collective-permute-start | bytes 1966088 | tf_op jit(solution)/shard_map/ppermute | solution.py:83
  48.8 1.9 %collective-permute-start.8 = (bf16[16,160,128]{2,1,0:T(8,128)(2,1)S(1)}, bf16[16,160,128]{2,1,0:T(8,128)(2,1)}, u32[]{:S(2)}, u32[]{:S(2)}) collective-permute-start(bf16[16,160,128]{2,1,0:T(8,128)(2,1)S(1)} %slice.22.w0_ref), channel_id=1, source_target_pairs={{0,8},{8,16},{16,24},{24,0},{1,9},{9,17},{17,25},{25,1},{2,10},{10... | collective-permute-start | bytes 1966088 | tf_op jit(solution)/shard_map/ppermute | solution.py:83
  50.7 3.5 %collective-permute-start.9 = (bf16[16,160,128]{2,1,0:T(8,128)(2,1)S(1)}, bf16[16,160,128]{2,1,0:T(8,128)(2,1)}, u32[]{:S(2)}, u32[]{:S(2)}) collective-permute-start(bf16[16,160,128]{2,1,0:T(8,128)(2,1)S(1)} %slice.22.w0_ref), channel_id=1, source_target_pairs={{0,16},{8,24},{16,0},{24,8},{1,17},{9,25},{17,1},{25,9},{2,18},{10... | collective-permute-start | bytes 1966088 | tf_op jit(solution)/shard_map/ppermute | solution.py:83
  55.6 4.4 %all-to-all-start.1 = ((bf16[4,16,64,128]{3,2,1,0:T(8,128)(2,1)}), bf16[4,16,64,128]{3,2,1,0:T(8,128)(2,1)}, u32[]{:S(2)}, u32[]{:S(2)}) async-start(bf16[4,16,64,128]{3,2,1,0:T(8,128)(2,1)} %broadcast_in_dim.4), calls=%async_computation.1 | async-start | bytes 2097152 | tf_op jit(solution)/shard_map/all_to_all | solution.py:74
  60.0 1.8 %collective-permute-start = (bf16[16,2048]{1,0:T(8,128)(2,1)S(1)}, bf16[16,2048]{1,0:T(8,128)(2,1)S(1)}, u32[]{:S(2)}, u32[]{:S(2)}) collective-permute-start(bf16[16,2048]{1,0:T(8,128)(2,1)S(1)} %slice.20), channel_id=1, source_target_pairs={{0,32},{32,64},{64,96},{96,128},{128,160},{160,192},{192,224},{224... | collective-permute-start | bytes 196616 | tf_op jit(solution)/shard_map/ppermute | solution.py:363
  65.8 1.6 %shard_map.164 = (bf16[272,2048]{1,0:T(8,128)(2,1)S(1)}, f32[256,128]{1,0:T(8,128)S(1)}, f32[256,128]{1,0:T(8,128)S(1)}, f32[256,256]{1,0:T(8,128)S(1)}) custom-call(s32[3]{0:T(128)S(1)} %pad_add_fusion.ids_ref, f32[1]{0:T(128)S(6)} %copy.19.a_log_ref, bf16[256,2048]{1,0:T(8,128)(2,1)S(1)} %bitcast.11, bf16[16,2048]{1,0:T(8,128)(2,1)S(1)} %copy-done.7, ...), custom_call_target="tpu_custom_call" | custom-call | flops 134217728 | tf_op jit(solution)/shard_map/pallas_call | solution.py:21
  67.4 7.4 %collective-permute-done.9.w2_ref = bf16[16,160,128]{2,1,0:T(8,128)(2,1)} collective-permute-done((bf16[16,160,128]{2,1,0:T(8,128)(2,1)S(1)}, bf16[16,160,128]{2,1,0:T(8,128)(2,1)}, u32[]{:S(2)}, u32[]{:S(2)}) %collective-permute-start.9) | collective-permute-done | bytes 655392 | tf_op jit(solution)/shard_map/ppermute | solution.py:83
  75.5 2.4 %shard_map.168 = (bf16[256,128]{1,0:T(8,128)(2,1)S(1)}, bf16[256,2048]{1,0:T(8,128)(2,1)S(1)}) custom-call(s32[3]{0:T(128)S(1)} %pad_add_fusion.ids_ref, bf16[272,2048]{1,0:T(8,128)(2,1)S(1)} %get-tuple-element.26.xn_ref, bf16[16,160,128]{2,1,0:T(8,128)(2,1)S(1)} %slice.22.w0_ref, bf16[16,160,128]{2,1,0:T(8,128)(2,1)} %collective-permute-done.8.w1_ref, ...), custom_call_target="tpu_custom_call" | custom-call | flops 536870912 | tf_op jit(solution)/shard_map/pallas_call | solution.py:21
  78.6 16.0 %collective-permute-start.12 = (bf16[256,2048]{1,0:T(8,128)(2,1)S(1)}, bf16[256,2048]{1,0:T(8,128)(2,1)}, u32[]{:S(2)}, u32[]{:S(2)}) collective-permute-start(bf16[256,2048]{1,0:T(8,128)(2,1)S(1)} %get-tuple-element.44.w_mine_ref), channel_id=1, source_target_pairs={{0,1},{1,0},{2,3},{3,2},{4,5},{5,4},{6,7},{7,6},{8,9},{9,8},{10,11... | collective-permute-start | bytes 3145736 | tf_op jit(solution)/shard_map/ppermute | solution.py:443
  97.4 5.2 %shard_map.165 = (bf16[128,256]{1,0:T(8,128)(2,1)S(1)}, f32[256,128]{1,0:T(8,128)S(1)}, f32[256,256]{1,0:T(8,128)S(1)}) custom-call(bf16[272,2048]{1,0:T(8,128)(2,1)S(1)} %get-tuple-element.26.xn_ref, bf16[4,16,64,128]{3,2,1,0:T(8,128)(2,1)} %all-to-all-done.1.w_ref, f32[2,4,128]{2,1,0:T(4,128)S(1)} %slice.17.taps_ref, f32[256,128]{1,0:T(8,128)S(1)} %copy-done.11, ...), custom_call_target="tpu_custom_call" | custom-call | flops 1342177280 | tf_op jit(solution)/shard_map/pallas_call | solution.py:21
  102.6 1.9 %collective-permute-start.1 = (bf16[128,256]{1,0:T(8,128)(2,1)S(1)}, bf16[128,256]{1,0:T(8,128)(2,1)S(1)}, u32[]{:S(2)}, u32[]{:S(2)}) collective-permute-start(bf16[128,256]{1,0:T(8,128)(2,1)S(1)} %get-tuple-element.31.m0_ref), channel_id=1, source_target_pairs={{0,32},{32,64},{64,96},{96,0},{128,160},{160,192},{192,224},{224,1... | collective-permute-start | bytes 196616 | tf_op jit(solution)/shard_map/ppermute | solution.py:83
  104.6 1.9 %collective-permute-start.2 = (bf16[128,256]{1,0:T(8,128)(2,1)S(1)}, bf16[128,256]{1,0:T(8,128)(2,1)S(1)}, u32[]{:S(2)}, u32[]{:S(2)}) collective-permute-start(bf16[128,256]{1,0:T(8,128)(2,1)S(1)} %get-tuple-element.31.m0_ref), channel_id=1, source_target_pairs={{0,64},{32,96},{64,0},{96,32},{128,192},{160,224},{192,128},{224,1... | collective-permute-start | bytes 196616 | tf_op jit(solution)/shard_map/ppermute | solution.py:83
  106.5 5.2 %collective-permute-start.3 = (bf16[128,256]{1,0:T(8,128)(2,1)S(1)}, bf16[128,256]{1,0:T(8,128)(2,1)S(1)}, u32[]{:S(2)}, u32[]{:S(2)}) collective-permute-start(bf16[128,256]{1,0:T(8,128)(2,1)S(1)} %get-tuple-element.31.m0_ref), channel_id=1, source_target_pairs={{0,96},{32,0},{64,32},{96,64},{128,224},{160,128},{192,160},{224,1... | collective-permute-start | bytes 196616 | tf_op jit(solution)/shard_map/ppermute | solution.py:83
  115.1 3.2 %collective-permute-start.4 = (bf16[128,256]{1,0:T(8,128)(2,1)S(1)}, bf16[128,256]{1,0:T(8,128)(2,1)S(1)}, u32[]{:S(2)}, u32[]{:S(2)}) collective-permute-start(bf16[128,256]{1,0:T(8,128)(2,1)S(1)} %get-tuple-element.32), channel_id=1, source_target_pairs={{0,128},{32,160},{64,192},{96,224},{128,256},{160,288},{192,320},{... | collective-permute-start | bytes 196616 | tf_op jit(solution)/shard_map/ppermute | solution.py:411
  118.4 9.1 %collective-permute-start.6 = (bf16[128,128]{1,0:T(8,128)(2,1)S(1)}, bf16[128,128]{1,0:T(8,128)(2,1)S(1)}, u32[]{:S(2)}, u32[]{:S(2)}) collective-permute-start(bf16[128,128]{1,0:T(8,128)(2,1)S(1)} %get-tuple-element.34), channel_id=1, source_target_pairs={{0,256},{32,288},{64,320},{96,352},{128,384},{160,416},{192,448},{... | collective-permute-start | bytes 98312 | tf_op jit(solution)/shard_map/ppermute | solution.py:411
  127.5 1.3 collective-permute-start.7
  129.5 2.8 %shard_map.167 = (f32[256,128]{1,0:T(8,128)S(1)}, f32[256,128]{1,0:T(8,128)S(1)}, f32[256,128]{1,0:T(8,128)S(1)}) custom-call(s32[3]{0:T(128)S(1)} %pad_add_fusion.ids_ref, bf16[272,2048]{1,0:T(8,128)(2,1)S(1)} %get-tuple-element.26.xn_ref, bf16[16,160,128]{2,1,0:T(8,128)(2,1)S(1)} %slice.22.w0_ref, bf16[16,160,128]{2,1,0:T(8,128)(2,1)} %collective-permute-done.8.w1_ref, ...), custom_call_target="tpu_custom_call" | custom-call | flops 536870912 | tf_op jit(solution)/shard_map/pallas_call | solution.py:21
  132.4 1.3 shard_map.169
  133.7 5.5 %collective-permute-start.11 = (bf16[4,32,256]{2,1,0:T(8,128)(2,1)S(1)}, bf16[4,32,256]{2,1,0:T(8,128)(2,1)S(1)}, u32[]{:S(2)}, u32[]{:S(2)}) collective-permute-start(bf16[4,32,256]{2,1,0:T(8,128)(2,1)S(1)} %get-tuple-element.43), channel_id=1, source_target_pairs={{0,1},{1,0},{2,3},{3,2},{4,5},{5,4},{6,7},{7,6},{8,9},{9,8},{10,11... | collective-permute-start | bytes 196616 | tf_op jit(solution)/shard_map/ppermute | solution.py:451
  140.2 1.7 %shard_map.170 = bf16[4,32,2048]{2,1,0:T(8,128)(2,1)S(1)} custom-call(bf16[4,32,256]{2,1,0:T(8,128)(2,1)S(1)} %get-tuple-element.42.mine_ref, bf16[4,32,256]{2,1,0:T(8,128)(2,1)S(1)} %collective-permute-done.11.theirs_ref, bf16[256,2048]{1,0:T(8,128)(2,1)S(1)} %get-tuple-element.44.w_mine_ref, bf16[256,2048]{1,0:T(8,128)(2,1)} %collective-permute-done.12.w_theirs_ref), custom_call_target="tpu_custom_call" | custom-call | flops 268435456 | tf_op jit(solution)/shard_map/pallas_call | solution.py:21
  141.9 11.8 %all_to_all.15.in_ref = bf16[4,32,2048]{2,1,0:T(8,128)(2,1)S(1)} all-to-all(bf16[4,32,2048]{2,1,0:T(8,128)(2,1)S(1)} %shard_map.170), channel_id=1, replica_groups={{0,2,4,6},{1,3,5,7},{8,10,12,14},{9,11,13,15},{16,18,20,22},{17,19,21,2..., dimensions={0} | all-to-all | bytes 1048576 | tf_op jit(solution)/shard_map/all_to_all | solution.py:74
  (67 shorter events, 15.7 us)
Async XLA Ops:
  3.4 10.4 %copy-start.15 = (bf16[224,128]{1,0:T(8,128)(2,1)S(1)}, bf16[224,128]{1,0:T(8,128)(2,1)}, u32[]{:S(2)}) copy-start(bf16[224,128]{1,0:T(8,128)(2,1)} %get-tuple-element.27) | copy-start | bytes 172036
  3.4 50.9 %all-to-all-start = ((bf16[8,32,2048]{2,1,0:T(8,128)(2,1)}), bf16[8,32,2048]{2,1,0:T(8,128)(2,1)S(1)}, u32[]{:S(2)}, u32[]{:S(2)}) async-start(bf16[8,32,2048]{2,1,0:T(8,128)(2,1)} %get-tuple-element.25), calls=%async_computation | async-start | bytes 2097152 | tf_op jit(solution)/shard_map/all_to_all | solution.py:74
  44.0 10.3 %copy-start.16 = (bf16[2048,8]{0,1:T(8,128)(2,1)S(1)}, bf16[2048,8]{0,1:T(8,128)(2,1)}, u32[]{:S(2)}) copy-start(bf16[2048,8]{0,1:T(8,128)(2,1)} %param.25) | copy-start | bytes 98308
  44.0 10.3 %copy-start.17 = (bf16[2048,8]{0,1:T(8,128)(2,1)S(1)}, bf16[2048,8]{0,1:T(8,128)(2,1)}, u32[]{:S(2)}) copy-start(bf16[2048,8]{0,1:T(8,128)(2,1)} %param.24) | copy-start | bytes 98308
  44.1 23.3 %collective-permute-start.10 = (bf16[16,160,128]{2,1,0:T(8,128)(2,1)S(1)}, bf16[16,160,128]{2,1,0:T(8,128)(2,1)S(1)}, u32[]{:S(2)}, u32[]{:S(2)}) collective-permute-start(bf16[16,160,128]{2,1,0:T(8,128)(2,1)S(1)} %slice.22.w0_ref), channel_id=1, source_target_pairs={{0,24},{8,0},{16,8},{24,16},{1,25},{9,1},{17,9},{25,17},{2,26},{10... | collective-permute-start | bytes 1966088 | tf_op jit(solution)/shard_map/ppermute | solution.py:83
  48.8 18.6 %collective-permute-start.8 = (bf16[16,160,128]{2,1,0:T(8,128)(2,1)S(1)}, bf16[16,160,128]{2,1,0:T(8,128)(2,1)}, u32[]{:S(2)}, u32[]{:S(2)}) collective-permute-start(bf16[16,160,128]{2,1,0:T(8,128)(2,1)S(1)} %slice.22.w0_ref), channel_id=1, source_target_pairs={{0,8},{8,16},{16,24},{24,0},{1,9},{9,17},{17,25},{25,1},{2,10},{10... | collective-permute-start | bytes 1966088 | tf_op jit(solution)/shard_map/ppermute | solution.py:83
  50.7 24.0 %collective-permute-start.9 = (bf16[16,160,128]{2,1,0:T(8,128)(2,1)S(1)}, bf16[16,160,128]{2,1,0:T(8,128)(2,1)}, u32[]{:S(2)}, u32[]{:S(2)}) collective-permute-start(bf16[16,160,128]{2,1,0:T(8,128)(2,1)S(1)} %slice.22.w0_ref), channel_id=1, source_target_pairs={{0,16},{8,24},{16,0},{24,8},{1,17},{9,25},{17,1},{25,9},{2,18},{10... | collective-permute-start | bytes 1966088 | tf_op jit(solution)/shard_map/ppermute | solution.py:83
  55.6 39.0 %all-to-all-start.1 = ((bf16[4,16,64,128]{3,2,1,0:T(8,128)(2,1)}), bf16[4,16,64,128]{3,2,1,0:T(8,128)(2,1)}, u32[]{:S(2)}, u32[]{:S(2)}) async-start(bf16[4,16,64,128]{3,2,1,0:T(8,128)(2,1)} %broadcast_in_dim.4), calls=%async_computation.1 | async-start | bytes 2097152 | tf_op jit(solution)/shard_map/all_to_all | solution.py:74
  60.0 14.8 %copy-start.9 = (f32[128]{0:T(128)S(1)}, f32[128]{0:T(128)}, u32[]{:S(2)}) copy-start(f32[128]{0:T(128)} %param.30) | copy-start | bytes 1540
  60.0 3.4 %collective-permute-start = (bf16[16,2048]{1,0:T(8,128)(2,1)S(1)}, bf16[16,2048]{1,0:T(8,128)(2,1)S(1)}, u32[]{:S(2)}, u32[]{:S(2)}) collective-permute-start(bf16[16,2048]{1,0:T(8,128)(2,1)S(1)} %slice.20), channel_id=1, source_target_pairs={{0,32},{32,64},{64,96},{96,128},{128,160},{160,192},{192,224},{224... | collective-permute-start | bytes 196616 | tf_op jit(solution)/shard_map/ppermute | solution.py:363
  67.4 10.6 %copy-start.1 = (f32[256,256]{1,0:T(8,128)}, f32[256,256]{1,0:T(8,128)S(1)}, u32[]{:S(2)}) copy-start(f32[256,256]{1,0:T(8,128)S(1)} %get-tuple-element.30.decay_ref) | copy-start | bytes 786436
  67.4 10.6 %copy-start.4 = (f32[256,128]{1,0:T(8,128)}, f32[256,128]{1,0:T(8,128)S(1)}, u32[]{:S(2)}) copy-start(f32[256,128]{1,0:T(8,128)S(1)} %get-tuple-element.29.gc_ref) | copy-start | bytes 393220
  67.4 10.6 %copy-start.10 = (f32[256,128]{1,0:T(8,128)}, f32[256,128]{1,0:T(8,128)S(1)}, u32[]{:S(2)}) copy-start(f32[256,128]{1,0:T(8,128)S(1)} %get-tuple-element.28.beta_ref) | copy-start | bytes 393220
  75.5 19.1 %copy-start.18 = (f32[3,4,128]{2,1,0:T(4,128)S(1)}, f32[3,4,128]{2,1,0:T(4,128)}, u32[]{:S(2)}) copy-start(f32[3,4,128]{2,1,0:T(4,128)} %param.26) | copy-start | bytes 18436
  78.6 61.5 %collective-permute-start.12 = (bf16[256,2048]{1,0:T(8,128)(2,1)S(1)}, bf16[256,2048]{1,0:T(8,128)(2,1)}, u32[]{:S(2)}, u32[]{:S(2)}) collective-permute-start(bf16[256,2048]{1,0:T(8,128)(2,1)S(1)} %get-tuple-element.44.w_mine_ref), channel_id=1, source_target_pairs={{0,1},{1,0},{2,3},{3,2},{4,5},{5,4},{6,7},{7,6},{8,9},{9,8},{10,11... | collective-permute-start | bytes 3145736 | tf_op jit(solution)/shard_map/ppermute | solution.py:443
  97.4 32.1 %copy-start.3 = (f32[256,256]{1,0:T(8,128)S(1)}, f32[256,256]{1,0:T(8,128)}, u32[]{:S(2)}) copy-start(f32[256,256]{1,0:T(8,128)} %copy-done.1) | copy-start | bytes 786436
  102.6 9.0 %collective-permute-start.1 = (bf16[128,256]{1,0:T(8,128)(2,1)S(1)}, bf16[128,256]{1,0:T(8,128)(2,1)S(1)}, u32[]{:S(2)}, u32[]{:S(2)}) collective-permute-start(bf16[128,256]{1,0:T(8,128)(2,1)S(1)} %get-tuple-element.31.m0_ref), channel_id=1, source_target_pairs={{0,32},{32,64},{64,96},{96,0},{128,160},{160,192},{192,224},{224,1... | collective-permute-start | bytes 196616 | tf_op jit(solution)/shard_map/ppermute | solution.py:83
  104.6 8.4 %collective-permute-start.2 = (bf16[128,256]{1,0:T(8,128)(2,1)S(1)}, bf16[128,256]{1,0:T(8,128)(2,1)S(1)}, u32[]{:S(2)}, u32[]{:S(2)}) collective-permute-start(bf16[128,256]{1,0:T(8,128)(2,1)S(1)} %get-tuple-element.31.m0_ref), channel_id=1, source_target_pairs={{0,64},{32,96},{64,0},{96,32},{128,192},{160,224},{192,128},{224,1... | collective-permute-start | bytes 196616 | tf_op jit(solution)/shard_map/ppermute | solution.py:83
  106.5 7.5 %collective-permute-start.3 = (bf16[128,256]{1,0:T(8,128)(2,1)S(1)}, bf16[128,256]{1,0:T(8,128)(2,1)S(1)}, u32[]{:S(2)}, u32[]{:S(2)}) collective-permute-start(bf16[128,256]{1,0:T(8,128)(2,1)S(1)} %get-tuple-element.31.m0_ref), channel_id=1, source_target_pairs={{0,96},{32,0},{64,32},{96,64},{128,224},{160,128},{192,160},{224,1... | collective-permute-start | bytes 196616 | tf_op jit(solution)/shard_map/ppermute | solution.py:83
  115.1 17.2 %collective-permute-start.4 = (bf16[128,256]{1,0:T(8,128)(2,1)S(1)}, bf16[128,256]{1,0:T(8,128)(2,1)S(1)}, u32[]{:S(2)}, u32[]{:S(2)}) collective-permute-start(bf16[128,256]{1,0:T(8,128)(2,1)S(1)} %get-tuple-element.32), channel_id=1, source_target_pairs={{0,128},{32,160},{64,192},{96,224},{128,256},{160,288},{192,320},{... | collective-permute-start | bytes 196616 | tf_op jit(solution)/shard_map/ppermute | solution.py:411
  118.4 14.0 %collective-permute-start.6 = (bf16[128,128]{1,0:T(8,128)(2,1)S(1)}, bf16[128,128]{1,0:T(8,128)(2,1)S(1)}, u32[]{:S(2)}, u32[]{:S(2)}) collective-permute-start(bf16[128,128]{1,0:T(8,128)(2,1)S(1)} %get-tuple-element.34), channel_id=1, source_target_pairs={{0,256},{32,288},{64,320},{96,352},{128,384},{160,416},{192,448},{... | collective-permute-start | bytes 98312 | tf_op jit(solution)/shard_map/ppermute | solution.py:411
  127.5 4.9 %collective-permute-start.7 = (bf16[128,128]{1,0:T(8,128)(2,1)S(1)}, bf16[128,128]{1,0:T(8,128)(2,1)S(1)}, u32[]{:S(2)}, u32[]{:S(2)}) collective-permute-start(bf16[128,128]{1,0:T(8,128)(2,1)S(1)} %get-tuple-element.34), channel_id=1, source_target_pairs={{0,384},{32,416},{64,448},{96,480},{1,385},{33,417},{65,449},{97,4... | collective-permute-start | bytes 98312 | tf_op jit(solution)/shard_map/ppermute | solution.py:411
  128.8 3.6 %collective-permute-start.5 = (bf16[128,128]{1,0:T(8,128)(2,1)S(1)}, bf16[128,128]{1,0:T(8,128)(2,1)S(1)}, u32[]{:S(2)}, u32[]{:S(2)}) collective-permute-start(bf16[128,128]{1,0:T(8,128)(2,1)S(1)} %get-tuple-element.33), channel_id=1, source_target_pairs={{128,384},{160,416},{192,448},{224,480},{129,385},{161,417},{193,4... | collective-permute-start | bytes 98312 | tf_op jit(solution)/shard_map/ppermute | solution.py:411
  133.7 6.4 %collective-permute-start.11 = (bf16[4,32,256]{2,1,0:T(8,128)(2,1)S(1)}, bf16[4,32,256]{2,1,0:T(8,128)(2,1)S(1)}, u32[]{:S(2)}, u32[]{:S(2)}) collective-permute-start(bf16[4,32,256]{2,1,0:T(8,128)(2,1)S(1)} %get-tuple-element.43), channel_id=1, source_target_pairs={{0,1},{1,0},{2,3},{3,2},{4,5},{5,4},{6,7},{7,6},{8,9},{9,8},{10,11... | collective-permute-start | bytes 196616 | tf_op jit(solution)/shard_map/ppermute | solution.py:451
  (11 other events, 18.7 us)

commit v3 on v2

--- a/solution.py
+++ b/solution.py
@@ -12,7 +12,7 @@
 BF16 = jnp.bfloat16
 
 
-def call(kernel, outs, *args, smem=0, scratch=(), flops=0, vmem=16):
+def call(kernel, outs, *args, smem=3, scratch=(), flops=0, vmem=16):
     in_specs = [pl.BlockSpec(memory_space=pltpu.SMEM)] * smem + [
         pl.BlockSpec(memory_space=pltpu.VMEM)
     ] * (len(args) - smem)
@@ -49,15 +49,16 @@
 
 
 def start_kernel(
-    f_ref, tok_ref, gain_ref, k_ref, v_ref, q_ref, g_ref, p_ref, op_ref, od_ref,
+    sp_ref, tp_ref, fs_ref, tok_ref, gain_ref, k_ref, v_ref, q_ref, g_ref, p_ref, op_ref, od_ref,
     copies_ref, part_ref, stacked,
 ):
     x = tok_ref[...].astype(F32)
     scale = lax.rsqrt(jnp.mean(x * x, axis=-1, keepdims=True) + EPS)
-    normed = (x * scale * gain_ref[...].astype(F32)).astype(BF16)
+    gain = gain_ref[...].astype(F32).reshape(1, x.shape[1])
+    normed = (x * scale * gain).astype(BF16)
     for j in range(copies_ref.shape[0]):
         copies_ref[j] = normed
-    f = f_ref[0]
+    f = fs_ref[0]
     depth = k_ref.shape[0]
     half = depth // 2
     rows = pl.ds(pl.multiple_of((f % 2) * half, half), half)
@@ -85,23 +86,27 @@
 
 
 def gate_kernel(
-    ids_ref, a_log_ref, rows_ref, tail_ref, wbd_ref, extra_ref, xn_ref, beta_ref, gc_ref, decay_ref
+    sp_ref, tp_ref, fs_ref, a_log_ref, rows_ref, tail_ref, wb_ref, wd_ref, extra_ref,
+    xn_ref, beta_ref, gc_ref, decay_ref,
 ):
     length = rows_ref.shape[0]
     tail = tail_ref[...]
-    xn_ref[0:HALO] = jnp.where(ids_ref[0] > 0, tail, jnp.zeros_like(tail))
+    xn_ref[0:HALO] = jnp.where(sp_ref[0] > 0, tail, jnp.zeros_like(tail))
     xn_ref[HALO:] = rows_ref[...]
-    pre = dot(rows_ref[...], wbd_ref[...], ((1,), (1,)))
-    heads = pre.shape[1] // 2
-    col = lax.broadcasted_iota(jnp.int32, pre.shape, 1)
-    lane = ids_ref[1]
-    beta_pre = jnp.sum(jnp.where(col == lane, pre, 0.0), axis=1, keepdims=True)
-    decay_pre = jnp.sum(jnp.where(col == lane + heads, pre, 0.0), axis=1, keepdims=True)
+    lane = tp_ref[0]
+
+    def own_column(w_ref):
+        pre = dot(rows_ref[...], w_ref[...], ((1,), (1,)))
+        col = lax.broadcasted_iota(jnp.int32, pre.shape, 1)
+        return jnp.sum(jnp.where(col == lane, pre, 0.0), axis=1, keepdims=True)
+
+    beta_pre, decay_pre = own_column(wb_ref), own_column(wd_ref)
     wide = (length, 128)
     beta_ref[...] = jax.nn.sigmoid(jnp.broadcast_to(beta_pre, wide))
     rate = jnp.exp(jnp.full(wide, a_log_ref[0], F32))
     soft = jax.nn.softplus(jnp.broadcast_to(decay_pre, wide))
-    log_gate = -rate * soft + jnp.broadcast_to(extra_ref[...], wide)
+    extra = jnp.transpose(jnp.broadcast_to(extra_ref[...], (128, length)))
+    log_gate = -rate * soft + extra
     r = lax.broadcasted_iota(jnp.int32, (length, length), 0)
     c = lax.broadcasted_iota(jnp.int32, (length, length), 1)
     lower = jnp.where(r >= c, 1.0, 0.0).astype(BF16)
@@ -155,20 +160,15 @@
 
 
 def local_kernel(
-    xn_ref, w_ref, taps_ref, beta_ref, gc_ref, decay_ref,
+    sp_ref, tp_ref, fs_ref, xn_ref, w0_ref, w1_ref, w2_ref, w3_ref, taps_ref, beta_ref, gc_ref, decay_ref,
     ab_ref, k_ref, uw_ref,
     w_scr, k_scr, v_scr,
 ):
     length, width = k_ref.shape
-    count, half = w_ref.shape[1:3]
-    for m in range(2):
-        for h in range(2):
-            for i in range(count):
-                at = (2 * i + h) * half
-                w_scr[at : at + half, m * width : (m + 1) * width] = w_ref[2 * m + h, i]
+    gather_two(fs_ref[0], (w0_ref, w1_ref, w2_ref, w3_ref), w_scr)
     raw = dot(xn_ref[...], w_scr[...])
-    keys = unit_rows(short_conv(raw[:, :width], taps_ref[0], length, k_scr))
-    values = short_conv(raw[:, width:], taps_ref[1], length, v_scr)
+    keys = unit_rows(short_conv(raw[:, :width], taps_ref[1], length, k_scr))
+    values = short_conv(raw[:, width:], taps_ref[2], length, v_scr)
     k_ref[...] = keys
     beta = beta_ref[...]
     gc = gc_ref[...]
@@ -196,12 +196,12 @@
 
 
 def query_kernel(
-    ids_ref, xn_ref, w0_ref, w1_ref, w2_ref, w3_ref, taps_ref, gc_ref, decay_ref, k_ref, uw_ref,
+    sp_ref, tp_ref, fs_ref, xn_ref, w0_ref, w1_ref, w2_ref, w3_ref, taps_ref, gc_ref, decay_ref, k_ref, uw_ref,
     own_ref, eff_ref, silu_ref,
     w_scr, q_scr,
 ):
     length, width = k_ref.shape
-    gather_two(ids_ref[2], (w0_ref, w1_ref, w2_ref, w3_ref), w_scr)
+    gather_two(fs_ref[0], (w0_ref, w1_ref, w2_ref, w3_ref), w_scr)
     raw = dot(xn_ref[...], w_scr[...])
     query = unit_rows(short_conv(raw[:, :width], taps_ref[0], length, q_scr)) * width ** (-0.5)
     silu_ref[...] = jax.nn.silu(raw[HALO:, width:].astype(BF16).astype(F32))
@@ -212,7 +212,7 @@
 
 
 def pool_kernel(
-    ids_ref, xn_ref, w0_ref, w1_ref, w2_ref, w3_ref, mix_ref, scale_ref,
+    sp_ref, tp_ref, fs_ref, xn_ref, w0_ref, w1_ref, w2_ref, w3_ref, mix_ref, scale_ref,
     out_ref, wo_ref, w_all, w_scr, a_scr, b_scr,
 ):
     count, part, width = w0_ref.shape
@@ -220,14 +220,14 @@
     part = part - skip
     length = xn_ref.shape[0] - HALO
     for d, piece in enumerate((w0_ref, w1_ref, w2_ref, w3_ref)):
-        at = pl.multiple_of(((ids_ref[2] + 4 - d) % 4) * part, 32)
+        at = pl.multiple_of(((fs_ref[0] + 4 - d) % 4) * part, 32)
         for s in range(count):
             w_all[pl.ds(at, part), s * width : (s + 1) * width] = piece[s, skip:]
     for s in range(count):
         w_scr[s * width : (s + 1) * width, :] = w_all[0:width, s * width : (s + 1) * width]
     wo_ref[...] = w_all[width:, :]
     x = dot(xn_ref[...], w_scr[...]).astype(BF16).astype(F32)
-    kind = ids_ref[1] % 4
+    kind = tp_ref[0] % 4
     total = HALO + length
     a_scr[0:HALO] = jnp.zeros((HALO, width), F32)
     b_scr[0:HALO] = jnp.zeros((HALO, width), F32)
@@ -241,7 +241,7 @@
     sixteen = eight + b_scr[HALO - 8 : HALO - 8 + total]
     window = jnp.where(kind == 0, two, jnp.where(kind == 1, four, jnp.where(kind == 2, eight, sixteen)))
     window = window[HALO:]
-    place = ids_ref[0] * length + lax.broadcasted_iota(jnp.int32, (length, width), 0)
+    place = sp_ref[0] * length + lax.broadcasted_iota(jnp.int32, (length, width), 0)
     span = jnp.where(kind == 0, 2, jnp.where(kind == 1, 4, jnp.where(kind == 2, 8, 16)))
     counts = jnp.minimum(place + 1, span).astype(F32)
     pooled = (window / counts - x[HALO:]).astype(BF16)
@@ -257,10 +257,10 @@
 
 
 def group_kernel(
-    ids_ref, m0_ref, m1_ref, m2_ref, m3_ref, total_ref, linear_ref, offset_ref, before_ref, maps
+    sp_ref, tp_ref, fs_ref, m0_ref, m1_ref, m2_ref, m3_ref, total_ref, linear_ref, offset_ref, before_ref, maps
 ):
     count, width, _ = maps.shape
-    place = ids_ref[0] % count
+    place = sp_ref[0] % count
     for d, piece in enumerate((m0_ref, m1_ref, m2_ref, m3_ref)):
         maps[(place + count - d) % count] = piece[...]
     r = lax.broadcasted_iota(jnp.int32, (width, width), 0)
@@ -284,8 +284,8 @@
 
 
 def attend_kernel(
-    ids_ref, t4_ref, a8_ref, b8_ref, b12_ref, before_ref, own_ref, eff_ref, silu_ref, gain_ref,
-    pool_ref, mine_ref, other_ref,
+    sp_ref, tp_ref, fs_ref, t4_ref, a8_ref, b8_ref, b12_ref, before_ref, own_ref, eff_ref, silu_ref, gain_ref,
+    pool_ref, wo_ref, mine_ref, other_ref,
 ):
     width = b8_ref.shape[0]
     state = apply(a8_ref[...], b12_ref[...].astype(F32)) + b8_ref[...].astype(F32)
@@ -295,24 +295,20 @@
     scale = lax.rsqrt(jnp.mean(attended * attended, axis=-1, keepdims=True) + EPS)
     delta = (attended * scale * gain_ref[...] * silu_ref[...]).astype(BF16)
     both = jnp.concatenate([pool_ref[...], delta], axis=1)
-    core = ids_ref[1] % 2
-    chips, rows = mine_ref.shape[:2]
-    for j in range(chips):
-        even = both[2 * j * rows : (2 * j + 1) * rows]
-        odd = both[(2 * j + 1) * rows : (2 * j + 2) * rows]
-        mine_ref[j] = jnp.where(core == 0, even, odd)
-        other_ref[j] = jnp.where(core == 0, odd, even)
-
-
-def out_kernel(mine_ref, theirs_ref, w_mine_ref, w_theirs_ref, out_ref):
-    chips, rows, width = mine_ref.shape
-    mine = mine_ref[...].reshape(chips * rows, width)
-    theirs = theirs_ref[...].reshape(chips * rows, width)
-    cols = out_ref.shape[2]
+    core = tp_ref[0] % 2
+    chips, rows, cols = mine_ref.shape
     step = 512
     for at in range(0, cols, step):
-        part = dot(mine, w_mine_ref[:, at : at + step]) + dot(theirs, w_theirs_ref[:, at : at + step])
-        out_ref[:, :, at : at + step] = part.astype(BF16).reshape(chips, rows, step)
+        part = dot(both, wo_ref[:, at : at + step]).astype(BF16)
+        for j in range(chips):
+            even = part[2 * j * rows : (2 * j + 1) * rows]
+            odd = part[(2 * j + 1) * rows : (2 * j + 2) * rows]
+            mine_ref[j, :, at : at + step] = jnp.where(core == 0, even, odd)
+            other_ref[j, :, at : at + step] = jnp.where(core == 0, odd, even)
+
+
+def pair_kernel(mine_ref, theirs_ref, out_ref):
+    out_ref[...] = (mine_ref[...].astype(F32) + theirs_ref[...].astype(F32)).astype(BF16)
 
 
 def sum_kernel(in_ref, out_ref):
@@ -346,7 +342,7 @@
     sp_id = lax.axis_index("sp").astype(jnp.int32)
     tp_id = lax.axis_index("tp").astype(jnp.int32)
     fs_id = lax.axis_index("fs").astype(jnp.int32)
-    ids = jnp.stack([sp_id, tp_id, fs_id])
+    ids = (sp_id[None], tp_id[None], fs_id[None])
     depth, width = w_key.shape
     rows, model = tokens.shape
     length = rows * n_tp
@@ -355,22 +351,18 @@
     copies, part = call(
         start_kernel,
         (shape(n_tp, rows, model, dtype=BF16), shape(7 * depth // 4, width, dtype=BF16)),
-        fs_id[None], tokens, norm_gain.reshape(1, model),
+        *ids, tokens, norm_gain,
         w_key, w_value, w_query, w_gate, w_pool_in, w_out_pool, w_out_delta,
-        smem=1, scratch=[pltpu.VMEM((3 * depth, width), BF16)], vmem=None,
+        scratch=[pltpu.VMEM((3 * depth, width), BF16)], vmem=None,
     )
     all_rows = exchange(copies, "tp").reshape(length, model)
     tail = lax.ppermute(
         all_rows[length - HALO :], "sp", [(i, i + 1) for i in range(n_sp - 1)]
     )
     quarters = lax.all_gather(part, "sp", axis=0)
-    kv = exchange(
-        jnp.broadcast_to(quarters[:, :half], (4, n_sp, half, width)), "fs"
-    )
-    kv = kv.reshape(4, n_sp, half, width)
+    kv = turns(quarters[:, :half], "fs", 4)
     rest = turns(quarters[:, half:], "fs", 4)
 
-    wbd = jnp.concatenate([w_beta.T, w_decay.T], axis=0)
     xn, beta, gc, decay = call(
         gate_kernel,
         (
@@ -379,13 +371,13 @@
             shape(length, 128),
             shape(length, length),
         ),
-        ids, a_log, all_rows, tail, wbd, decay_extra,
-        smem=2, flops=2 * length * model * 128,
+        *ids, a_log, all_rows, tail, w_beta.T, w_decay.T, decay_extra.T,
+        smem=4, flops=2 * length * model * 128,
     )
     ab, keys, uw = call(
         local_kernel,
         (shape(width, 2 * width, dtype=BF16), shape(length, width), shape(length, 2 * width)),
-        xn, kv, conv_weight[1:], beta, gc, decay,
+        *ids, xn, *kv, conv_weight, beta, gc, decay,
         scratch=[
             pltpu.VMEM((model, 2 * width), BF16),
             pltpu.VMEM((HALO + length, width), F32),
@@ -403,8 +395,8 @@
             shape(width, width, dtype=BF16),
             shape(width, 2 * width),
         ),
-        ids, *near,
-        smem=1, scratch=[pltpu.VMEM((quad, width, 2 * width), BF16)], flops=20 * width**3,
+        *ids, *near,
+        scratch=[pltpu.VMEM((quad, width, 2 * width), BF16)], flops=20 * width**3,
     )
 
     def from_behind(x, first, last, distance):
@@ -418,8 +410,7 @@
     own, eff, silu_gate = call(
         query_kernel,
         (shape(length, width), shape(length, width), shape(length, width)),
-        ids, xn, *rest, conv_weight[:1], gc, decay, keys, uw,
-        smem=1,
+        *ids, xn, *rest, conv_weight, gc, decay, keys, uw,
         scratch=[
             pltpu.VMEM((model, 2 * width), BF16),
             pltpu.VMEM((HALO + length, width), F32),
@@ -429,8 +420,7 @@
     pool_out, w_mine = call(
         pool_kernel,
         (shape(length, width, dtype=BF16), shape(2 * width, model, dtype=BF16)),
-        ids, xn, *rest, w_mix[0], pool_scale.reshape(1, width),
-        smem=1,
+        *ids, xn, *rest, w_mix[0], pool_scale.reshape(1, width),
         scratch=[
             pltpu.VMEM((3 * width, model), BF16),
             pltpu.VMEM((model, width), BF16),
@@ -439,25 +429,21 @@
         ],
         flops=8 * length * model * width,
     )
-    swap = [(i, i ^ 1) for i in range(n_tp)]
-    w_theirs = lax.ppermute(w_mine, "tp", swap)
     chips = n_tp // 2
     mine, other = call(
         attend_kernel,
-        (shape(chips, rows, 2 * width, dtype=BF16), shape(chips, rows, 2 * width, dtype=BF16)),
-        ids, t4, a8, b8, b12, before, own, eff, silu_gate, delta_gain.reshape(1, width), pool_out,
-        smem=1, flops=4 * length * model * width,
-    )
-    theirs = lax.ppermute(other, "tp", swap)
+        (shape(chips, rows, model, dtype=BF16), shape(chips, rows, model, dtype=BF16)),
+        *ids, t4, a8, b8, b12, before, own, eff, silu_gate, delta_gain.reshape(1, width), pool_out,
+        w_mine,
+        flops=4 * length * model * width,
+    )
+    theirs = lax.ppermute(other, "tp", [(i, i ^ 1) for i in range(n_tp)])
     partial = call(
-        out_kernel,
-        shape(chips, rows, model, dtype=BF16),
-        mine, theirs, w_mine, w_theirs,
-        flops=4 * length * model * width,
+        pair_kernel, shape(chips, rows, model, dtype=BF16), mine, theirs, smem=0, flops=1000000
     )
     cores = [[2 * x + c for x in range(chips)] for c in range(2)]
     arrived = exchange(partial, "tp", cores)
-    return call(sum_kernel, shape(rows, model, dtype=BF16), arrived, flops=1000000)
+    return call(sum_kernel, shape(rows, model, dtype=BF16), arrived, smem=0, flops=1000000)
 
 
 def solution(mesh):

time: 155 us -> 153 us (0.987)
  waiting for transfers between devices: 10.6 us -> 32.1 us
  starting transfers between devices: 71.6 us -> 60.8 us
  local copies, waits for them, and re-layouts: 9.93 us -> 0.11 us
  Pallas kernels: 19.1 us -> 15.9 us
    ppermute x6 -> x9, waiting for transfers between devices: 9.68 us -> 30.6 us  [turns(): lax.ppermute(x, axis, [(i, i - i % size + (i + d) % size) for i in range(...]
    ppermute x2 -> x1, starting transfers between devices: 21.5 us -> 7.99 us  [layer(): theirs = lax.ppermute(other, 'tp', [(i, i ^ 1) for i in range(n_tp)])]
    unnamed x41 -> x16, local copies, waits for them, and re-layouts: 7.34 us -> 0.04 us
    ppermute x6 -> x9, starting transfers between devices: 19.2 us -> 26 us  [turns(): lax.ppermute(x, axis, [(i, i - i % size + (i + d) % size) for i in range(...]
    all_to_all x2 -> x1, starting transfers between devices: 14.8 us -> 10.4 us  [exchange(): lax.all_to_all(copies, axis, split_axis=0, concat_axis=0, tiled=True, axi...]
    pallas_call x9, Pallas kernels: 19.1 us -> 15.9 us  [call(): pl.pallas_call(kernel, out_shape=list(outs) if many else outs, in_specs=i...]
  transfers between devices with their start and end apart: 15 -> 16, of which waited for: 4 -> 5; matrix products, arithmetic and copies ran while one was open for 1% -> 0% of each run, Pallas kernels for 9% -> 8%
where the time goes in v3:
time: 153 us; the launch traced here: 151 us
  starting transfers between devices  60.8 us (40%)
  blocking collectives  41.3 us (27%)
  waiting for transfers between devices  32.1 us (21%)
  Pallas kernels  15.9 us (10%)
    ppermute x9, waiting for transfers between devices, turns(): lax.ppermute(x, axis, [(i, i - i % size + (i + d) % size) for i in range(...  30.6 us
    all_gather x1, blocking collectives, layer(): quarters = lax.all_gather(part, 'sp', axis=0)  30.2 us
    ppermute x9, starting transfers between devices, turns(): lax.ppermute(x, axis, [(i, i - i % size + (i + d) % size) for i in range(...  26 us
    pallas_call x9, Pallas kernels, call(): pl.pallas_call(kernel, out_shape=list(outs) if many else outs, in_specs=i...  15.9 us
    ppermute x4, starting transfers between devices, from_behind(): lax.ppermute(x, 'sp', [(i, i + distance) for i in range(first, last)])  14.6 us
    all_to_all x1, blocking collectives, exchange(): lax.all_to_all(copies, axis, split_axis=0, concat_axis=0, tiled=True, axi...  11.1 us
    all_to_all x1, starting transfers between devices, exchange(): lax.all_to_all(copies, axis, split_axis=0, concat_axis=0, tiled=True, axi...  10.4 us
    ppermute x1, starting transfers between devices, layer(): theirs = lax.ppermute(other, 'tp', [(i, i ^ 1) for i in range(n_tp)])  7.99 us
  transfers between devices with their start and end apart: 16, of which 5 were waited for; matrix products, arithmetic and copies ran while one was open for 0% of the time, Pallas kernels for 8%

profile of v3, /device:TPU:1, one launch (start us, length us, event | category | flops | bytes accessed | tf_op | source)
XLA Modules:
  0.0 151.2 jit_solution(673604419712629163)
XLA Ops:
  0.0 2.2 %shard_map.163 = (bf16[8,32,2048]{2,1,0:T(8,128)(2,1)}, bf16[224,128]{1,0:T(8,128)(2,1)}) custom-call(s32[1]{0:T(128)} %bitcast.sp_ref, s32[1]{0:T(128)} %bitcast.1.tp_ref, s32[1]{0:T(128)} %bitcast.2.fs_ref, bf16[32,2048]{1,0:T(8,128)(2,1)} %tok_ref.1, bf16[2048]{0:T(1024)(128)(2,1)} %gain_ref.1, bf16[128,128]{1,0:T(8,128)(2,1)} %k_ref.1, ...), custom_call_target="tpu_custom_call" | custom-call | tf_op jit(solution)/shard_map/pallas_call | solution.py:21
  2.2 10.4 %all-to-all-start = ((bf16[8,32,2048]{2,1,0:T(8,128)(2,1)}), bf16[8,32,2048]{2,1,0:T(8,128)(2,1)S(1)}, u32[]{:S(2)}, u32[]{:S(2)}) async-start(bf16[8,32,2048]{2,1,0:T(8,128)(2,1)} %get-tuple-element.25), calls=%async_computation | async-start | bytes 2097152 | tf_op jit(solution)/shard_map/all_to_all | solution.py:75
  12.6 30.2 %all-gather = bf16[3584,128]{1,0:T(8,128)(2,1)S(1)} all-gather(bf16[224,128]{1,0:T(8,128)(2,1)S(1)} %copy-done.7), channel_id=2, replica_groups=mesh['sp'=16,'fs'=4,'tp'=8] {'sp'}, dimensions={0}, use_global_device_ids=true | all-gather | bytes 974848 | tf_op jit(solution)/shard_map/all_gather | solution.py:362
  42.8 3.4 %collective-permute-start.1 = (bf16[16,64,128]{2,1,0:T(8,128)(2,1)S(1)}, bf16[16,64,128]{2,1,0:T(8,128)(2,1)}, u32[]{:S(2)}, u32[]{:S(2)}) collective-permute-start(bf16[16,64,128]{2,1,0:T(8,128)(2,1)S(1)} %slice.13.w0_ref), channel_id=1, source_target_pairs={{0,8},{8,16},{16,24},{24,0},{1,9},{9,17},{17,25},{25,1},{2,10},{10... | collective-permute-start | bytes 786440 | tf_op jit(solution)/shard_map/ppermute | solution.py:84
  46.3 3.2 %collective-permute-start.11 = (bf16[16,160,128]{2,1,0:T(8,128)(2,1)S(1)}, bf16[16,160,128]{2,1,0:T(8,128)(2,1)S(1)}, u32[]{:S(2)}, u32[]{:S(2)}) collective-permute-start(bf16[16,160,128]{2,1,0:T(8,128)(2,1)S(1)} %slice.14.w0_ref), channel_id=1, source_target_pairs={{0,8},{8,16},{16,24},{24,0},{1,9},{9,17},{17,25},{25,1},{2,10},{10... | collective-permute-start | bytes 1966088 | tf_op jit(solution)/shard_map/ppermute | solution.py:84
  49.5 3.2 %collective-permute-start.12 = (bf16[16,160,128]{2,1,0:T(8,128)(2,1)S(1)}, bf16[16,160,128]{2,1,0:T(8,128)(2,1)S(1)}, u32[]{:S(2)}, u32[]{:S(2)}) collective-permute-start(bf16[16,160,128]{2,1,0:T(8,128)(2,1)S(1)} %slice.14.w0_ref), channel_id=1, source_target_pairs={{0,16},{8,24},{16,0},{24,8},{1,17},{9,25},{17,1},{25,9},{2,18},{10... | collective-permute-start | bytes 1966088 | tf_op jit(solution)/shard_map/ppermute | solution.py:84
  52.7 4.0 %collective-permute-start.13 = (bf16[16,160,128]{2,1,0:T(8,128)(2,1)S(1)}, bf16[16,160,128]{2,1,0:T(8,128)(2,1)}, u32[]{:S(2)}, u32[]{:S(2)}) collective-permute-start(bf16[16,160,128]{2,1,0:T(8,128)(2,1)S(1)} %slice.14.w0_ref), channel_id=1, source_target_pairs={{0,24},{8,0},{16,8},{24,16},{1,25},{9,1},{17,9},{25,17},{2,26},{10... | collective-permute-start | bytes 1966088 | tf_op jit(solution)/shard_map/ppermute | solution.py:84
  56.7 1.8 %collective-permute-start = (bf16[16,2048]{1,0:T(8,128)(2,1)S(1)}, bf16[16,2048]{1,0:T(8,128)(2,1)S(1)}, u32[]{:S(2)}, u32[]{:S(2)}) collective-permute-start(bf16[16,2048]{1,0:T(8,128)(2,1)S(1)} %slice.12), channel_id=1, source_target_pairs={{0,32},{32,64},{64,96},{96,128},{128,160},{160,192},{192,224},{224... | collective-permute-start | bytes 196616 | tf_op jit(solution)/shard_map/ppermute | solution.py:359
  58.6 2.3 %collective-permute-start.2 = (bf16[16,64,128]{2,1,0:T(8,128)(2,1)S(1)}, bf16[16,64,128]{2,1,0:T(8,128)(2,1)S(1)}, u32[]{:S(2)}, u32[]{:S(2)}) collective-permute-start(bf16[16,64,128]{2,1,0:T(8,128)(2,1)S(1)} %slice.13.w0_ref), channel_id=1, source_target_pairs={{0,16},{8,24},{16,0},{24,8},{1,17},{9,25},{17,1},{25,9},{2,18},{10... | collective-permute-start | bytes 786440 | tf_op jit(solution)/shard_map/ppermute | solution.py:84
  60.8 3.4 %collective-permute-start.3 = (bf16[16,64,128]{2,1,0:T(8,128)(2,1)S(1)}, bf16[16,64,128]{2,1,0:T(8,128)(2,1)S(1)}, u32[]{:S(2)}, u32[]{:S(2)}) collective-permute-start(bf16[16,64,128]{2,1,0:T(8,128)(2,1)S(1)} %slice.13.w0_ref), channel_id=1, source_target_pairs={{0,24},{8,0},{16,8},{24,16},{1,25},{9,1},{17,9},{25,17},{2,26},{10... | collective-permute-start | bytes 786440 | tf_op jit(solution)/shard_map/ppermute | solution.py:84
  66.1 16.5 %collective-permute-done.2.w2_ref = bf16[16,64,128]{2,1,0:T(8,128)(2,1)S(1)} collective-permute-done((bf16[16,64,128]{2,1,0:T(8,128)(2,1)S(1)}, bf16[16,64,128]{2,1,0:T(8,128)(2,1)S(1)}, u32[]{:S(2)}, u32[]{:S(2)}) %collective-permute-start.2) | collective-permute-done | bytes 262176 | tf_op jit(solution)/shard_map/ppermute | solution.py:84
  82.6 7.9 %collective-permute-done.3.w3_ref = bf16[16,64,128]{2,1,0:T(8,128)(2,1)S(1)} collective-permute-done((bf16[16,64,128]{2,1,0:T(8,128)(2,1)S(1)}, bf16[16,64,128]{2,1,0:T(8,128)(2,1)S(1)}, u32[]{:S(2)}, u32[]{:S(2)}) %collective-permute-start.3) | collective-permute-done | bytes 262176 | tf_op jit(solution)/shard_map/ppermute | solution.py:84
  90.5 5.1 %shard_map.165 = (bf16[128,256]{1,0:T(8,128)(2,1)S(1)}, f32[256,128]{1,0:T(8,128)S(1)}, f32[256,256]{1,0:T(8,128)S(1)}) custom-call(s32[1]{0:T(128)} %bitcast.sp_ref, s32[1]{0:T(128)} %bitcast.1.tp_ref, s32[1]{0:T(128)} %bitcast.2.fs_ref, bf16[272,2048]{1,0:T(8,128)(2,1)S(1)} %get-tuple-element.26.xn_ref, bf16[16,64,128]{2,1,0:T(8,128)(2,1)S(1)} %slice.13.w0_ref, ...), custom_call_target="tpu_custom_call" | custom-call | flops 1342177280 | tf_op jit(solution)/shard_map/pallas_call | solution.py:21
  95.6 2.3 %collective-permute-start.4 = (bf16[128,256]{1,0:T(8,128)(2,1)S(1)}, bf16[128,256]{1,0:T(8,128)(2,1)S(1)}, u32[]{:S(2)}, u32[]{:S(2)}) collective-permute-start(bf16[128,256]{1,0:T(8,128)(2,1)S(1)} %get-tuple-element.31.m0_ref), channel_id=1, source_target_pairs={{0,32},{32,64},{64,96},{96,0},{128,160},{160,192},{192,224},{224,1... | collective-permute-start | bytes 196616 | tf_op jit(solution)/shard_map/ppermute | solution.py:84
  97.9 2.0 %collective-permute-start.5 = (bf16[128,256]{1,0:T(8,128)(2,1)S(1)}, bf16[128,256]{1,0:T(8,128)(2,1)S(1)}, u32[]{:S(2)}, u32[]{:S(2)}) collective-permute-start(bf16[128,256]{1,0:T(8,128)(2,1)S(1)} %get-tuple-element.31.m0_ref), channel_id=1, source_target_pairs={{0,64},{32,96},{64,0},{96,32},{128,192},{160,224},{192,128},{224,1... | collective-permute-start | bytes 196616 | tf_op jit(solution)/shard_map/ppermute | solution.py:84
  99.9 2.5 %collective-permute-done.4.m1_ref = bf16[128,256]{1,0:T(8,128)(2,1)S(1)} collective-permute-done((bf16[128,256]{1,0:T(8,128)(2,1)S(1)}, bf16[128,256]{1,0:T(8,128)(2,1)S(1)}, u32[]{:S(2)}, u32[]{:S(2)}) %collective-permute-start.4) | collective-permute-done | bytes 65568 | tf_op jit(solution)/shard_map/ppermute | solution.py:84
  102.4 2.2 %collective-permute-start.6 = (bf16[128,256]{1,0:T(8,128)(2,1)S(1)}, bf16[128,256]{1,0:T(8,128)(2,1)S(1)}, u32[]{:S(2)}, u32[]{:S(2)}) collective-permute-start(bf16[128,256]{1,0:T(8,128)(2,1)S(1)} %get-tuple-element.31.m0_ref), channel_id=1, source_target_pairs={{0,96},{32,0},{64,32},{96,64},{128,224},{160,128},{192,160},{224,1... | collective-permute-start | bytes 196616 | tf_op jit(solution)/shard_map/ppermute | solution.py:84
  104.6 3.7 %collective-permute-done.6.m3_ref = bf16[128,256]{1,0:T(8,128)(2,1)S(1)} collective-permute-done((bf16[128,256]{1,0:T(8,128)(2,1)S(1)}, bf16[128,256]{1,0:T(8,128)(2,1)S(1)}, u32[]{:S(2)}, u32[]{:S(2)}) %collective-permute-start.6) | collective-permute-done | bytes 65568 | tf_op jit(solution)/shard_map/ppermute | solution.py:84
  109.0 2.9 %collective-permute-start.7 = (bf16[128,256]{1,0:T(8,128)(2,1)S(1)}, bf16[128,256]{1,0:T(8,128)(2,1)S(1)}, u32[]{:S(2)}, u32[]{:S(2)}) collective-permute-start(bf16[128,256]{1,0:T(8,128)(2,1)S(1)} %get-tuple-element.32), channel_id=1, source_target_pairs={{0,128},{32,160},{64,192},{96,224},{128,256},{160,288},{192,320},{... | collective-permute-start | bytes 196616 | tf_op jit(solution)/shard_map/ppermute | solution.py:403
  111.9 2.6 %shard_map.167 = (f32[256,128]{1,0:T(8,128)S(1)}, f32[256,128]{1,0:T(8,128)S(1)}, f32[256,128]{1,0:T(8,128)S(1)}) custom-call(s32[1]{0:T(128)} %bitcast.sp_ref, s32[1]{0:T(128)} %bitcast.1.tp_ref, s32[1]{0:T(128)} %bitcast.2.fs_ref, bf16[272,2048]{1,0:T(8,128)(2,1)S(1)} %get-tuple-element.26.xn_ref, bf16[16,160,128]{2,1,0:T(8,128)(2,1)S(1)} %slice.14.w0_ref, ...), custom_call_target="tpu_custom_call" | custom-call | flops 536870912 | tf_op jit(solution)/shard_map/pallas_call | solution.py:21
  114.5 9.8 %collective-permute-start.9 = (bf16[128,128]{1,0:T(8,128)(2,1)S(1)}, bf16[128,128]{1,0:T(8,128)(2,1)S(1)}, u32[]{:S(2)}, u32[]{:S(2)}) collective-permute-start(bf16[128,128]{1,0:T(8,128)(2,1)S(1)} %get-tuple-element.34), channel_id=1, source_target_pairs={{0,256},{32,288},{64,320},{96,352},{128,384},{160,416},{192,448},{... | collective-permute-start | bytes 98312 | tf_op jit(solution)/shard_map/ppermute | solution.py:403
  126.3 2.2 %shard_map.168 = (bf16[256,128]{1,0:T(8,128)(2,1)S(1)}, bf16[256,2048]{1,0:T(8,128)(2,1)S(1)}) custom-call(s32[1]{0:T(128)} %bitcast.sp_ref, s32[1]{0:T(128)} %bitcast.1.tp_ref, s32[1]{0:T(128)} %bitcast.2.fs_ref, bf16[272,2048]{1,0:T(8,128)(2,1)S(1)} %get-tuple-element.26.xn_ref, bf16[16,160,128]{2,1,0:T(8,128)(2,1)S(1)} %slice.14.w0_ref, ...), custom_call_target="tpu_custom_call" | custom-call | flops 536870912 | tf_op jit(solution)/shard_map/pallas_call | solution.py:21
  129.8 8.0 %collective-permute-start.14 = (bf16[4,32,2048]{2,1,0:T(8,128)(2,1)S(1)}, bf16[4,32,2048]{2,1,0:T(8,128)(2,1)S(1)}, u32[]{:S(2)}, u32[]{:S(2)}) collective-permute-start(bf16[4,32,2048]{2,1,0:T(8,128)(2,1)S(1)} %get-tuple-element.44), channel_id=1, source_target_pairs={{0,1},{1,0},{2,3},{3,2},{4,5},{5,4},{6,7},{7,6},{8,9},{9,8},{10,11... | collective-permute-start | bytes 1572872 | tf_op jit(solution)/shard_map/ppermute | solution.py:440
  139.4 11.1 %all_to_all.10.in_ref = bf16[4,32,2048]{2,1,0:T(8,128)(2,1)S(1)} all-to-all(bf16[4,32,2048]{2,1,0:T(8,128)(2,1)S(1)} %shard_map.170), channel_id=1, replica_groups={{0,2,4,6},{1,3,5,7},{8,10,12,14},{9,11,13,15},{16,18,20,22},{17,19,21,2..., dimensions={0} | all-to-all | bytes 1048576 | tf_op jit(solution)/shard_map/all_to_all | solution.py:75
  (38 shorter events, 7.4 us)
Async XLA Ops:
  2.2 10.4 %copy-start.7 = (bf16[224,128]{1,0:T(8,128)(2,1)S(1)}, bf16[224,128]{1,0:T(8,128)(2,1)}, u32[]{:S(2)}) copy-start(bf16[224,128]{1,0:T(8,128)(2,1)} %get-tuple-element.27) | copy-start | bytes 172036
  2.2 54.5 %all-to-all-start = ((bf16[8,32,2048]{2,1,0:T(8,128)(2,1)}), bf16[8,32,2048]{2,1,0:T(8,128)(2,1)S(1)}, u32[]{:S(2)}, u32[]{:S(2)}) async-start(bf16[8,32,2048]{2,1,0:T(8,128)(2,1)} %get-tuple-element.25), calls=%async_computation | async-start | bytes 2097152 | tf_op jit(solution)/shard_map/all_to_all | solution.py:75
  42.7 22.1 %copy-start.1 = (bf16[2048,8]{0,1:T(8,128)(2,1)S(1)}, bf16[2048,8]{0,1:T(8,128)(2,1)}, u32[]{:S(2)}) copy-start(bf16[2048,8]{0,1:T(8,128)(2,1)} %param.24) | copy-start | bytes 98308
  42.7 22.1 %copy-start.2 = (bf16[2048,8]{0,1:T(8,128)(2,1)S(1)}, bf16[2048,8]{0,1:T(8,128)(2,1)}, u32[]{:S(2)}) copy-start(bf16[2048,8]{0,1:T(8,128)(2,1)} %param.25) | copy-start | bytes 98308
  42.8 22.1 %copy-start.4 = (f32[256,1]{0,1:T(1,128)S(1)}, f32[256,1]{0,1:T(1,128)}, u32[]{:S(2)}) copy-start(f32[256,1]{0,1:T(1,128)} %param.28) | copy-start | bytes 3076
  42.8 47.7 %copy-start.3 = (f32[3,4,128]{2,1,0:T(4,128)S(1)}, f32[3,4,128]{2,1,0:T(4,128)}, u32[]{:S(2)}) copy-start(f32[3,4,128]{2,1,0:T(4,128)} %taps_ref.3) | copy-start | bytes 18436
  42.8 15.8 %collective-permute-start.1 = (bf16[16,64,128]{2,1,0:T(8,128)(2,1)S(1)}, bf16[16,64,128]{2,1,0:T(8,128)(2,1)}, u32[]{:S(2)}, u32[]{:S(2)}) collective-permute-start(bf16[16,64,128]{2,1,0:T(8,128)(2,1)S(1)} %slice.13.w0_ref), channel_id=1, source_target_pairs={{0,8},{8,16},{16,24},{24,0},{1,9},{9,17},{17,25},{25,1},{2,10},{10... | collective-permute-start | bytes 786440 | tf_op jit(solution)/shard_map/ppermute | solution.py:84
  46.3 65.6 %collective-permute-start.11 = (bf16[16,160,128]{2,1,0:T(8,128)(2,1)S(1)}, bf16[16,160,128]{2,1,0:T(8,128)(2,1)S(1)}, u32[]{:S(2)}, u32[]{:S(2)}) collective-permute-start(bf16[16,160,128]{2,1,0:T(8,128)(2,1)S(1)} %slice.14.w0_ref), channel_id=1, source_target_pairs={{0,8},{8,16},{16,24},{24,0},{1,9},{9,17},{17,25},{25,1},{2,10},{10... | collective-permute-start | bytes 1966088 | tf_op jit(solution)/shard_map/ppermute | solution.py:84
  49.5 62.4 %collective-permute-start.12 = (bf16[16,160,128]{2,1,0:T(8,128)(2,1)S(1)}, bf16[16,160,128]{2,1,0:T(8,128)(2,1)S(1)}, u32[]{:S(2)}, u32[]{:S(2)}) collective-permute-start(bf16[16,160,128]{2,1,0:T(8,128)(2,1)S(1)} %slice.14.w0_ref), channel_id=1, source_target_pairs={{0,16},{8,24},{16,0},{24,8},{1,17},{9,25},{17,1},{25,9},{2,18},{10... | collective-permute-start | bytes 1966088 | tf_op jit(solution)/shard_map/ppermute | solution.py:84
  52.7 59.2 %collective-permute-start.13 = (bf16[16,160,128]{2,1,0:T(8,128)(2,1)S(1)}, bf16[16,160,128]{2,1,0:T(8,128)(2,1)}, u32[]{:S(2)}, u32[]{:S(2)}) collective-permute-start(bf16[16,160,128]{2,1,0:T(8,128)(2,1)S(1)} %slice.14.w0_ref), channel_id=1, source_target_pairs={{0,24},{8,0},{16,8},{24,16},{1,25},{9,1},{17,9},{25,17},{2,26},{10... | collective-permute-start | bytes 1966088 | tf_op jit(solution)/shard_map/ppermute | solution.py:84
  56.7 4.1 %collective-permute-start = (bf16[16,2048]{1,0:T(8,128)(2,1)S(1)}, bf16[16,2048]{1,0:T(8,128)(2,1)S(1)}, u32[]{:S(2)}, u32[]{:S(2)}) collective-permute-start(bf16[16,2048]{1,0:T(8,128)(2,1)S(1)} %slice.12), channel_id=1, source_target_pairs={{0,32},{32,64},{64,96},{96,128},{128,160},{160,192},{192,224},{224... | collective-permute-start | bytes 196616 | tf_op jit(solution)/shard_map/ppermute | solution.py:359
  58.6 24.1 %collective-permute-start.2 = (bf16[16,64,128]{2,1,0:T(8,128)(2,1)S(1)}, bf16[16,64,128]{2,1,0:T(8,128)(2,1)S(1)}, u32[]{:S(2)}, u32[]{:S(2)}) collective-permute-start(bf16[16,64,128]{2,1,0:T(8,128)(2,1)S(1)} %slice.13.w0_ref), channel_id=1, source_target_pairs={{0,16},{8,24},{16,0},{24,8},{1,17},{9,25},{17,1},{25,9},{2,18},{10... | collective-permute-start | bytes 786440 | tf_op jit(solution)/shard_map/ppermute | solution.py:84
  60.8 29.6 %collective-permute-start.3 = (bf16[16,64,128]{2,1,0:T(8,128)(2,1)S(1)}, bf16[16,64,128]{2,1,0:T(8,128)(2,1)S(1)}, u32[]{:S(2)}, u32[]{:S(2)}) collective-permute-start(bf16[16,64,128]{2,1,0:T(8,128)(2,1)S(1)} %slice.13.w0_ref), channel_id=1, source_target_pairs={{0,24},{8,0},{16,8},{24,16},{1,25},{9,1},{17,9},{25,17},{2,26},{10... | collective-permute-start | bytes 786440 | tf_op jit(solution)/shard_map/ppermute | solution.py:84
  95.6 6.8 %collective-permute-start.4 = (bf16[128,256]{1,0:T(8,128)(2,1)S(1)}, bf16[128,256]{1,0:T(8,128)(2,1)S(1)}, u32[]{:S(2)}, u32[]{:S(2)}) collective-permute-start(bf16[128,256]{1,0:T(8,128)(2,1)S(1)} %get-tuple-element.31.m0_ref), channel_id=1, source_target_pairs={{0,32},{32,64},{64,96},{96,0},{128,160},{160,192},{192,224},{224,1... | collective-permute-start | bytes 196616 | tf_op jit(solution)/shard_map/ppermute | solution.py:84
  97.9 6.7 %collective-permute-start.5 = (bf16[128,256]{1,0:T(8,128)(2,1)S(1)}, bf16[128,256]{1,0:T(8,128)(2,1)S(1)}, u32[]{:S(2)}, u32[]{:S(2)}) collective-permute-start(bf16[128,256]{1,0:T(8,128)(2,1)S(1)} %get-tuple-element.31.m0_ref), channel_id=1, source_target_pairs={{0,64},{32,96},{64,0},{96,32},{128,192},{160,224},{192,128},{224,1... | collective-permute-start | bytes 196616 | tf_op jit(solution)/shard_map/ppermute | solution.py:84
  102.4 6.0 %collective-permute-start.6 = (bf16[128,256]{1,0:T(8,128)(2,1)S(1)}, bf16[128,256]{1,0:T(8,128)(2,1)S(1)}, u32[]{:S(2)}, u32[]{:S(2)}) collective-permute-start(bf16[128,256]{1,0:T(8,128)(2,1)S(1)} %get-tuple-element.31.m0_ref), channel_id=1, source_target_pairs={{0,96},{32,0},{64,32},{96,64},{128,224},{160,128},{192,160},{224,1... | collective-permute-start | bytes 196616 | tf_op jit(solution)/shard_map/ppermute | solution.py:84
  109.0 19.6 %collective-permute-start.7 = (bf16[128,256]{1,0:T(8,128)(2,1)S(1)}, bf16[128,256]{1,0:T(8,128)(2,1)S(1)}, u32[]{:S(2)}, u32[]{:S(2)}) collective-permute-start(bf16[128,256]{1,0:T(8,128)(2,1)S(1)} %get-tuple-element.32), channel_id=1, source_target_pairs={{0,128},{32,160},{64,192},{96,224},{128,256},{160,288},{192,320},{... | collective-permute-start | bytes 196616 | tf_op jit(solution)/shard_map/ppermute | solution.py:403
  111.9 14.4 %copy-start = (bf16[1,128,128]{2,1,0:T(8,128)(2,1)S(1)}, bf16[1,128,128]{2,1,0:T(8,128)(2,1)}, u32[]{:S(2)}) copy-start(bf16[1,128,128]{2,1,0:T(8,128)(2,1)} %param.29) | copy-start | bytes 98308
  111.9 14.4 %copy-start.5 = (f32[128]{0:T(128)S(1)}, f32[128]{0:T(128)}, u32[]{:S(2)}) copy-start(f32[128]{0:T(128)} %param.30) | copy-start | bytes 1540
  114.5 14.0 %collective-permute-start.9 = (bf16[128,128]{1,0:T(8,128)(2,1)S(1)}, bf16[128,128]{1,0:T(8,128)(2,1)S(1)}, u32[]{:S(2)}, u32[]{:S(2)}) collective-permute-start(bf16[128,128]{1,0:T(8,128)(2,1)S(1)} %get-tuple-element.34), channel_id=1, source_target_pairs={{0,256},{32,288},{64,320},{96,352},{128,384},{160,416},{192,448},{... | collective-permute-start | bytes 98312 | tf_op jit(solution)/shard_map/ppermute | solution.py:403
  124.3 4.3 %collective-permute-start.10 = (bf16[128,128]{1,0:T(8,128)(2,1)S(1)}, bf16[128,128]{1,0:T(8,128)(2,1)S(1)}, u32[]{:S(2)}, u32[]{:S(2)}) collective-permute-start(bf16[128,128]{1,0:T(8,128)(2,1)S(1)} %get-tuple-element.34), channel_id=1, source_target_pairs={{0,384},{32,416},{64,448},{96,480},{1,385},{33,417},{65,449},{97,4... | collective-permute-start | bytes 98312 | tf_op jit(solution)/shard_map/ppermute | solution.py:403
  125.6 2.9 %collective-permute-start.8 = (bf16[128,128]{1,0:T(8,128)(2,1)S(1)}, bf16[128,128]{1,0:T(8,128)(2,1)S(1)}, u32[]{:S(2)}, u32[]{:S(2)}) collective-permute-start(bf16[128,128]{1,0:T(8,128)(2,1)S(1)} %get-tuple-element.33), channel_id=1, source_target_pairs={{128,384},{160,416},{192,448},{224,480},{129,385},{161,417},{193,4... | collective-permute-start | bytes 98312 | tf_op jit(solution)/shard_map/ppermute | solution.py:403
  126.3 2.3 %copy-start.6 = (f32[128]{0:T(128)S(1)}, f32[128]{0:T(128)}, u32[]{:S(2)}) copy-start(f32[128]{0:T(128)} %param.31) | copy-start | bytes 1540
  129.8 9.5 %collective-permute-start.14 = (bf16[4,32,2048]{2,1,0:T(8,128)(2,1)S(1)}, bf16[4,32,2048]{2,1,0:T(8,128)(2,1)S(1)}, u32[]{:S(2)}, u32[]{:S(2)}) collective-permute-start(bf16[4,32,2048]{2,1,0:T(8,128)(2,1)S(1)} %get-tuple-element.44), channel_id=1, source_target_pairs={{0,1},{1,0},{2,3},{3,2},{4,5},{5,4},{6,7},{7,6},{8,9},{9,8},{10,11... | collective-permute-start | bytes 1572872 | tf_op jit(solution)/shard_map/ppermute | solution.py:440

commit v4 on v3

--- a/solution.py
+++ b/solution.py
@@ -256,26 +256,34 @@
     return jnp.concatenate([moved[:, :width], moved[:, width:] + offset], axis=1)
 
 
+def pair_map_kernel(sp_ref, tp_ref, fs_ref, own_ref, other_ref, pair_ref, before_ref):
+    width = own_ref.shape[0]
+    odd = sp_ref[0] % 2 == 1
+    own, other = own_ref[...], other_ref[...]
+    earlier = jnp.where(odd, other, own)
+    later = jnp.where(odd, own, other)
+    pair_ref[...] = step_map(later, earlier.astype(F32), width).astype(BF16)
+    r = lax.broadcasted_iota(jnp.int32, (width, 2 * width), 0)
+    c = lax.broadcasted_iota(jnp.int32, (width, 2 * width), 1)
+    before_ref[...] = jnp.where(odd, other, jnp.where(r == c, 1.0, 0.0).astype(BF16))
+
+
 def group_kernel(
-    sp_ref, tp_ref, fs_ref, m0_ref, m1_ref, m2_ref, m3_ref, total_ref, linear_ref, offset_ref, before_ref, maps
-):
-    count, width, _ = maps.shape
-    place = sp_ref[0] % count
-    for d, piece in enumerate((m0_ref, m1_ref, m2_ref, m3_ref)):
-        maps[(place + count - d) % count] = piece[...]
-    r = lax.broadcasted_iota(jnp.int32, (width, width), 0)
-    c = lax.broadcasted_iota(jnp.int32, (width, width), 1)
-    eye = jnp.where(r == c, 1.0, 0.0)
-    before = jnp.concatenate([eye, jnp.zeros((width, width), F32)], axis=1)
-    carry = maps[0].astype(F32)
-    for i in range(1, count):
-        before = jnp.where(place == i, carry, before)
-        carry = step_map(maps[i], carry, width)
-    before_ref[...] = before
-    total = carry.astype(BF16)
+    sp_ref, tp_ref, fs_ref, own_ref, other_ref, inner_ref,
+    total_ref, linear_ref, offset_ref, before_ref,
+):
+    width = own_ref.shape[0]
+    upper = (sp_ref[0] // 2) % 2 == 1
+    own, other = own_ref[...], other_ref[...]
+    earlier = jnp.where(upper, other, own)
+    later = jnp.where(upper, own, other)
+    total = step_map(later, earlier.astype(F32), width).astype(BF16)
     total_ref[...] = total
     linear_ref[...] = total[:, :width]
     offset_ref[...] = total[:, width:]
+    inner = inner_ref[...]
+    behind = step_map(inner, other.astype(F32), width)
+    before_ref[...] = jnp.where(upper, behind, inner.astype(F32))
 
 
 def apply(linear, state):
@@ -386,7 +394,16 @@
         flops=20 * length * model * width,
     )
     quad = 4
-    near = turns(ab, "sp", quad)
+
+    def meet(x, distance):
+        return lax.ppermute(x, "sp", [(i, i ^ distance) for i in range(n_sp)])
+
+    pair, inner = call(
+        pair_map_kernel,
+        (shape(width, 2 * width, dtype=BF16), shape(width, 2 * width, dtype=BF16)),
+        *ids, ab, meet(ab, 1),
+        flops=20 * width**3,
+    )
     total, linear, offset, before = call(
         group_kernel,
         (
@@ -395,8 +412,8 @@
             shape(width, width, dtype=BF16),
             shape(width, 2 * width),
         ),
-        *ids, *near,
-        scratch=[pltpu.VMEM((quad, width, 2 * width), BF16)], flops=20 * width**3,
+        *ids, pair, meet(pair, 2), inner,
+        flops=20 * width**3,
     )
 
     def from_behind(x, first, last, distance):

time: 153 us -> 152 us (level)
  starting transfers between devices: 60.8 us -> 58.3 us
    ppermute x0 -> x2, waiting for transfers between devices: none -> 7.39 us  [meet(): return lax.ppermute(x, 'sp', [(i, i ^ distance) for i in range(n_sp)])]
    ppermute x9 -> x6, starting transfers between devices: 26 us -> 19.4 us  [turns(): lax.ppermute(x, axis, [(i, i - i % size + (i + d) % size) for i in range(...]
    ppermute x9 -> x6, waiting for transfers between devices: 30.6 us -> 24.4 us  [turns(): lax.ppermute(x, axis, [(i, i - i % size + (i + d) % size) for i in range(...]
    ppermute x0 -> x2, starting transfers between devices: none -> 4.22 us  [meet(): return lax.ppermute(x, 'sp', [(i, i ^ distance) for i in range(n_sp)])]
    pallas_call x9 -> x10, Pallas kernels: 15.9 us -> 15.7 us  [call(): pl.pallas_call(kernel, out_shape=list(outs) if many else outs, in_specs=i...]
  transfers between devices with their start and end apart: 16 -> 15, of which waited for: 5 -> 5; matrix products, arithmetic and copies ran while one was open for 0% -> 0% of each run, Pallas kernels for 8% -> 8%
where the time goes in v4:
time: 152 us; the launch traced here: 150 us
  starting transfers between devices  58.3 us (38%)
  blocking collectives  41.9 us (28%)
  waiting for transfers between devices  33.3 us (22%)
  Pallas kernels  15.7 us (10%)
    all_gather x1, blocking collectives, layer(): quarters = lax.all_gather(part, 'sp', axis=0)  30.2 us
    ppermute x6, waiting for transfers between devices, turns(): lax.ppermute(x, axis, [(i, i - i % size + (i + d) % size) for i in range(...  24.4 us
    ppermute x6, starting transfers between devices, turns(): lax.ppermute(x, axis, [(i, i - i % size + (i + d) % size) for i in range(...  19.4 us
    pallas_call x10, Pallas kernels, call(): pl.pallas_call(kernel, out_shape=list(outs) if many else outs, in_specs=i...  15.7 us
    ppermute x4, starting transfers between devices, from_behind(): lax.ppermute(x, 'sp', [(i, i + distance) for i in range(first, last)])  14.4 us
    all_to_all x1, blocking collectives, exchange(): lax.all_to_all(copies, axis, split_axis=0, concat_axis=0, tiled=True, axi...  11.7 us
    all_to_all x1, starting transfers between devices, exchange(): lax.all_to_all(copies, axis, split_axis=0, concat_axis=0, tiled=True, axi...  10.4 us
    ppermute x1, starting transfers between devices, layer(): theirs = lax.ppermute(other, 'tp', [(i, i ^ 1) for i in range(n_tp)])  8.02 us
  transfers between devices with their start and end apart: 15, of which 5 were waited for; matrix products, arithmetic and copies ran while one was open for 0% of the time, Pallas kernels for 8%

profile of v4, /device:TPU:1, one launch (start us, length us, event | category | flops | bytes accessed | tf_op | source)
XLA Modules:
  0.0 150.3 jit_solution(2468159911817402079)
XLA Ops:
  0.0 2.2 %shard_map.163 = (bf16[8,32,2048]{2,1,0:T(8,128)(2,1)}, bf16[224,128]{1,0:T(8,128)(2,1)}) custom-call(s32[1]{0:T(128)} %bitcast.sp_ref, s32[1]{0:T(128)} %bitcast.1.tp_ref, s32[1]{0:T(128)} %bitcast.2.fs_ref, bf16[32,2048]{1,0:T(8,128)(2,1)} %tok_ref.1, bf16[2048]{0:T(1024)(128)(2,1)} %gain_ref.1, bf16[128,128]{1,0:T(8,128)(2,1)} %k_ref.1, ...), custom_call_target="tpu_custom_call" | custom-call | tf_op jit(solution)/shard_map/pallas_call | solution.py:21
  2.2 10.4 %all-to-all-start = ((bf16[8,32,2048]{2,1,0:T(8,128)(2,1)}), bf16[8,32,2048]{2,1,0:T(8,128)(2,1)S(1)}, u32[]{:S(2)}, u32[]{:S(2)}) async-start(bf16[8,32,2048]{2,1,0:T(8,128)(2,1)} %get-tuple-element.27), calls=%async_computation | async-start | bytes 2097152 | tf_op jit(solution)/shard_map/all_to_all | solution.py:75
  12.6 30.2 %all-gather = bf16[3584,128]{1,0:T(8,128)(2,1)S(1)} all-gather(bf16[224,128]{1,0:T(8,128)(2,1)S(1)} %copy-done.7), channel_id=2, replica_groups=mesh['sp'=16,'fs'=4,'tp'=8] {'sp'}, dimensions={0}, use_global_device_ids=true | all-gather | bytes 974848 | tf_op jit(solution)/shard_map/all_gather | solution.py:370
  42.8 3.4 %collective-permute-start.1 = (bf16[16,64,128]{2,1,0:T(8,128)(2,1)S(1)}, bf16[16,64,128]{2,1,0:T(8,128)(2,1)}, u32[]{:S(2)}, u32[]{:S(2)}) collective-permute-start(bf16[16,64,128]{2,1,0:T(8,128)(2,1)S(1)} %slice.13.w0_ref), channel_id=1, source_target_pairs={{0,8},{8,16},{16,24},{24,0},{1,9},{9,17},{17,25},{25,1},{2,10},{10... | collective-permute-start | bytes 786440 | tf_op jit(solution)/shard_map/ppermute | solution.py:84
  46.3 3.2 %collective-permute-start.10 = (bf16[16,160,128]{2,1,0:T(8,128)(2,1)S(1)}, bf16[16,160,128]{2,1,0:T(8,128)(2,1)S(1)}, u32[]{:S(2)}, u32[]{:S(2)}) collective-permute-start(bf16[16,160,128]{2,1,0:T(8,128)(2,1)S(1)} %slice.14.w0_ref), channel_id=1, source_target_pairs={{0,8},{8,16},{16,24},{24,0},{1,9},{9,17},{17,25},{25,1},{2,10},{10... | collective-permute-start | bytes 1966088 | tf_op jit(solution)/shard_map/ppermute | solution.py:84
  49.5 3.2 %collective-permute-start.11 = (bf16[16,160,128]{2,1,0:T(8,128)(2,1)S(1)}, bf16[16,160,128]{2,1,0:T(8,128)(2,1)S(1)}, u32[]{:S(2)}, u32[]{:S(2)}) collective-permute-start(bf16[16,160,128]{2,1,0:T(8,128)(2,1)S(1)} %slice.14.w0_ref), channel_id=1, source_target_pairs={{0,16},{8,24},{16,0},{24,8},{1,17},{9,25},{17,1},{25,9},{2,18},{10... | collective-permute-start | bytes 1966088 | tf_op jit(solution)/shard_map/ppermute | solution.py:84
  52.7 4.0 %collective-permute-start.12 = (bf16[16,160,128]{2,1,0:T(8,128)(2,1)S(1)}, bf16[16,160,128]{2,1,0:T(8,128)(2,1)}, u32[]{:S(2)}, u32[]{:S(2)}) collective-permute-start(bf16[16,160,128]{2,1,0:T(8,128)(2,1)S(1)} %slice.14.w0_ref), channel_id=1, source_target_pairs={{0,24},{8,0},{16,8},{24,16},{1,25},{9,1},{17,9},{25,17},{2,26},{10... | collective-permute-start | bytes 1966088 | tf_op jit(solution)/shard_map/ppermute | solution.py:84
  56.7 1.8 %collective-permute-start = (bf16[16,2048]{1,0:T(8,128)(2,1)S(1)}, bf16[16,2048]{1,0:T(8,128)(2,1)S(1)}, u32[]{:S(2)}, u32[]{:S(2)}) collective-permute-start(bf16[16,2048]{1,0:T(8,128)(2,1)S(1)} %slice.12), channel_id=1, source_target_pairs={{0,32},{32,64},{64,96},{96,128},{128,160},{160,192},{192,224},{224... | collective-permute-start | bytes 196616 | tf_op jit(solution)/shard_map/ppermute | solution.py:367
  58.6 2.3 %collective-permute-start.2 = (bf16[16,64,128]{2,1,0:T(8,128)(2,1)S(1)}, bf16[16,64,128]{2,1,0:T(8,128)(2,1)S(1)}, u32[]{:S(2)}, u32[]{:S(2)}) collective-permute-start(bf16[16,64,128]{2,1,0:T(8,128)(2,1)S(1)} %slice.13.w0_ref), channel_id=1, source_target_pairs={{0,16},{8,24},{16,0},{24,8},{1,17},{9,25},{17,1},{25,9},{2,18},{10... | collective-permute-start | bytes 786440 | tf_op jit(solution)/shard_map/ppermute | solution.py:84
  60.8 3.4 %collective-permute-start.3 = (bf16[16,64,128]{2,1,0:T(8,128)(2,1)S(1)}, bf16[16,64,128]{2,1,0:T(8,128)(2,1)S(1)}, u32[]{:S(2)}, u32[]{:S(2)}) collective-permute-start(bf16[16,64,128]{2,1,0:T(8,128)(2,1)S(1)} %slice.13.w0_ref), channel_id=1, source_target_pairs={{0,24},{8,0},{16,8},{24,16},{1,25},{9,1},{17,9},{25,17},{2,26},{10... | collective-permute-start | bytes 786440 | tf_op jit(solution)/shard_map/ppermute | solution.py:84
  66.1 16.5 %collective-permute-done.2.w2_ref = bf16[16,64,128]{2,1,0:T(8,128)(2,1)S(1)} collective-permute-done((bf16[16,64,128]{2,1,0:T(8,128)(2,1)S(1)}, bf16[16,64,128]{2,1,0:T(8,128)(2,1)S(1)}, u32[]{:S(2)}, u32[]{:S(2)}) %collective-permute-start.2) | collective-permute-done | bytes 262176 | tf_op jit(solution)/shard_map/ppermute | solution.py:84
  82.6 7.9 %collective-permute-done.3.w3_ref = bf16[16,64,128]{2,1,0:T(8,128)(2,1)S(1)} collective-permute-done((bf16[16,64,128]{2,1,0:T(8,128)(2,1)S(1)}, bf16[16,64,128]{2,1,0:T(8,128)(2,1)S(1)}, u32[]{:S(2)}, u32[]{:S(2)}) %collective-permute-start.3) | collective-permute-done | bytes 262176 | tf_op jit(solution)/shard_map/ppermute | solution.py:84
  90.5 5.1 %shard_map.165 = (bf16[128,256]{1,0:T(8,128)(2,1)S(1)}, f32[256,128]{1,0:T(8,128)S(1)}, f32[256,256]{1,0:T(8,128)S(1)}) custom-call(s32[1]{0:T(128)} %bitcast.sp_ref, s32[1]{0:T(128)} %bitcast.1.tp_ref, s32[1]{0:T(128)} %bitcast.2.fs_ref, bf16[272,2048]{1,0:T(8,128)(2,1)S(1)} %get-tuple-element.28.xn_ref, bf16[16,64,128]{2,1,0:T(8,128)(2,1)S(1)} %slice.13.w0_ref, ...), custom_call_target="tpu_custom_call" | custom-call | flops 1342177280 | tf_op jit(solution)/shard_map/pallas_call | solution.py:21
  95.6 2.3 %collective-permute-start.4 = (bf16[128,256]{1,0:T(8,128)(2,1)S(1)}, bf16[128,256]{1,0:T(8,128)(2,1)S(1)}, u32[]{:S(2)}, u32[]{:S(2)}) collective-permute-start(bf16[128,256]{1,0:T(8,128)(2,1)S(1)} %get-tuple-element.33.own_ref), channel_id=1, source_target_pairs={{0,32},{32,0},{64,96},{96,64},{128,160},{160,128},{192,224},{224,1... | collective-permute-start | bytes 196616 | tf_op jit(solution)/shard_map/ppermute | solution.py:399
  97.9 2.7 %collective-permute-done.4.other_ref = bf16[128,256]{1,0:T(8,128)(2,1)S(1)} collective-permute-done((bf16[128,256]{1,0:T(8,128)(2,1)S(1)}, bf16[128,256]{1,0:T(8,128)(2,1)S(1)}, u32[]{:S(2)}, u32[]{:S(2)}) %collective-permute-start.4) | collective-permute-done | bytes 65568 | tf_op jit(solution)/shard_map/ppermute | solution.py:399
  100.8 1.9 %collective-permute-start.5 = (bf16[128,256]{1,0:T(8,128)(2,1)S(1)}, bf16[128,256]{1,0:T(8,128)(2,1)S(1)}, u32[]{:S(2)}, u32[]{:S(2)}) collective-permute-start(bf16[128,256]{1,0:T(8,128)(2,1)S(1)} %get-tuple-element.34.own_ref), channel_id=1, source_target_pairs={{0,64},{32,96},{64,0},{96,32},{128,192},{160,224},{192,128},{224,1... | collective-permute-start | bytes 196616 | tf_op jit(solution)/shard_map/ppermute | solution.py:399
  102.7 4.7 %collective-permute-done.5.other_ref = bf16[128,256]{1,0:T(8,128)(2,1)S(1)} collective-permute-done((bf16[128,256]{1,0:T(8,128)(2,1)S(1)}, bf16[128,256]{1,0:T(8,128)(2,1)S(1)}, u32[]{:S(2)}, u32[]{:S(2)}) %collective-permute-start.5) | collective-permute-done | bytes 65568 | tf_op jit(solution)/shard_map/ppermute | solution.py:399
  107.6 3.2 %collective-permute-start.6 = (bf16[128,256]{1,0:T(8,128)(2,1)S(1)}, bf16[128,256]{1,0:T(8,128)(2,1)S(1)}, u32[]{:S(2)}, u32[]{:S(2)}) collective-permute-start(bf16[128,256]{1,0:T(8,128)(2,1)S(1)} %get-tuple-element.36), channel_id=1, source_target_pairs={{0,128},{32,160},{64,192},{96,224},{128,256},{160,288},{192,320},{... | collective-permute-start | bytes 196616 | tf_op jit(solution)/shard_map/ppermute | solution.py:420
  110.9 2.6 %shard_map.168 = (f32[256,128]{1,0:T(8,128)S(1)}, f32[256,128]{1,0:T(8,128)S(1)}, f32[256,128]{1,0:T(8,128)S(1)}) custom-call(s32[1]{0:T(128)} %bitcast.sp_ref, s32[1]{0:T(128)} %bitcast.1.tp_ref, s32[1]{0:T(128)} %bitcast.2.fs_ref, bf16[272,2048]{1,0:T(8,128)(2,1)S(1)} %get-tuple-element.28.xn_ref, bf16[16,160,128]{2,1,0:T(8,128)(2,1)S(1)} %slice.14.w0_ref, ...), custom_call_target="tpu_custom_call" | custom-call | flops 536870912 | tf_op jit(solution)/shard_map/pallas_call | solution.py:21
  113.5 9.2 %collective-permute-start.8 = (bf16[128,128]{1,0:T(8,128)(2,1)S(1)}, bf16[128,128]{1,0:T(8,128)(2,1)S(1)}, u32[]{:S(2)}, u32[]{:S(2)}) collective-permute-start(bf16[128,128]{1,0:T(8,128)(2,1)S(1)} %get-tuple-element.38), channel_id=1, source_target_pairs={{0,256},{32,288},{64,320},{96,352},{128,384},{160,416},{192,448},{... | collective-permute-start | bytes 98312 | tf_op jit(solution)/shard_map/ppermute | solution.py:420
  124.7 2.2 %shard_map.169 = (bf16[256,128]{1,0:T(8,128)(2,1)S(1)}, bf16[256,2048]{1,0:T(8,128)(2,1)S(1)}) custom-call(s32[1]{0:T(128)} %bitcast.sp_ref, s32[1]{0:T(128)} %bitcast.1.tp_ref, s32[1]{0:T(128)} %bitcast.2.fs_ref, bf16[272,2048]{1,0:T(8,128)(2,1)S(1)} %get-tuple-element.28.xn_ref, bf16[16,160,128]{2,1,0:T(8,128)(2,1)S(1)} %slice.14.w0_ref, ...), custom_call_target="tpu_custom_call" | custom-call | flops 536870912 | tf_op jit(solution)/shard_map/pallas_call | solution.py:21
  128.2 8.0 %collective-permute-start.13 = (bf16[4,32,2048]{2,1,0:T(8,128)(2,1)S(1)}, bf16[4,32,2048]{2,1,0:T(8,128)(2,1)S(1)}, u32[]{:S(2)}, u32[]{:S(2)}) collective-permute-start(bf16[4,32,2048]{2,1,0:T(8,128)(2,1)S(1)} %get-tuple-element.48), channel_id=1, source_target_pairs={{0,1},{1,0},{2,3},{3,2},{4,5},{5,4},{6,7},{7,6},{8,9},{9,8},{10,11... | collective-permute-start | bytes 1572872 | tf_op jit(solution)/shard_map/ppermute | solution.py:457
  136.2 1.5 %collective-permute-done.13.theirs_ref = bf16[4,32,2048]{2,1,0:T(8,128)(2,1)S(1)} collective-permute-done((bf16[4,32,2048]{2,1,0:T(8,128)(2,1)S(1)}, bf16[4,32,2048]{2,1,0:T(8,128)(2,1)S(1)}, u32[]{:S(2)}, u32[]{:S(2)}) %collective-permute-start.13) | collective-permute-done | bytes 524320 | tf_op jit(solution)/shard_map/ppermute | solution.py:457
  137.9 11.7 %all_to_all.10.in_ref = bf16[4,32,2048]{2,1,0:T(8,128)(2,1)S(1)} all-to-all(bf16[4,32,2048]{2,1,0:T(8,128)(2,1)S(1)} %shard_map.171), channel_id=1, replica_groups={{0,2,4,6},{1,3,5,7},{8,10,12,14},{9,11,13,15},{16,18,20,22},{17,19,21,2..., dimensions={0} | all-to-all | bytes 1048576 | tf_op jit(solution)/shard_map/all_to_all | solution.py:75
  (37 shorter events, 5.7 us)
Async XLA Ops:
  2.2 10.4 %copy-start.7 = (bf16[224,128]{1,0:T(8,128)(2,1)S(1)}, bf16[224,128]{1,0:T(8,128)(2,1)}, u32[]{:S(2)}) copy-start(bf16[224,128]{1,0:T(8,128)(2,1)} %get-tuple-element.29) | copy-start | bytes 172036
  2.2 54.5 %all-to-all-start = ((bf16[8,32,2048]{2,1,0:T(8,128)(2,1)}), bf16[8,32,2048]{2,1,0:T(8,128)(2,1)S(1)}, u32[]{:S(2)}, u32[]{:S(2)}) async-start(bf16[8,32,2048]{2,1,0:T(8,128)(2,1)} %get-tuple-element.27), calls=%async_computation | async-start | bytes 2097152 | tf_op jit(solution)/shard_map/all_to_all | solution.py:75
  42.7 22.1 %copy-start.1 = (bf16[2048,8]{0,1:T(8,128)(2,1)S(1)}, bf16[2048,8]{0,1:T(8,128)(2,1)}, u32[]{:S(2)}) copy-start(bf16[2048,8]{0,1:T(8,128)(2,1)} %param.24) | copy-start | bytes 98308
  42.7 22.1 %copy-start.2 = (bf16[2048,8]{0,1:T(8,128)(2,1)S(1)}, bf16[2048,8]{0,1:T(8,128)(2,1)}, u32[]{:S(2)}) copy-start(bf16[2048,8]{0,1:T(8,128)(2,1)} %param.25) | copy-start | bytes 98308
  42.8 22.1 %copy-start.4 = (f32[256,1]{0,1:T(1,128)S(1)}, f32[256,1]{0,1:T(1,128)}, u32[]{:S(2)}) copy-start(f32[256,1]{0,1:T(1,128)} %param.28) | copy-start | bytes 3076
  42.8 47.7 %copy-start.3 = (f32[3,4,128]{2,1,0:T(4,128)S(1)}, f32[3,4,128]{2,1,0:T(4,128)}, u32[]{:S(2)}) copy-start(f32[3,4,128]{2,1,0:T(4,128)} %taps_ref.3) | copy-start | bytes 18436
  42.8 15.8 %collective-permute-start.1 = (bf16[16,64,128]{2,1,0:T(8,128)(2,1)S(1)}, bf16[16,64,128]{2,1,0:T(8,128)(2,1)}, u32[]{:S(2)}, u32[]{:S(2)}) collective-permute-start(bf16[16,64,128]{2,1,0:T(8,128)(2,1)S(1)} %slice.13.w0_ref), channel_id=1, source_target_pairs={{0,8},{8,16},{16,24},{24,0},{1,9},{9,17},{17,25},{25,1},{2,10},{10... | collective-permute-start | bytes 786440 | tf_op jit(solution)/shard_map/ppermute | solution.py:84
  46.3 64.6 %collective-permute-start.10 = (bf16[16,160,128]{2,1,0:T(8,128)(2,1)S(1)}, bf16[16,160,128]{2,1,0:T(8,128)(2,1)S(1)}, u32[]{:S(2)}, u32[]{:S(2)}) collective-permute-start(bf16[16,160,128]{2,1,0:T(8,128)(2,1)S(1)} %slice.14.w0_ref), channel_id=1, source_target_pairs={{0,8},{8,16},{16,24},{24,0},{1,9},{9,17},{17,25},{25,1},{2,10},{10... | collective-permute-start | bytes 1966088 | tf_op jit(solution)/shard_map/ppermute | solution.py:84
  49.5 61.4 %collective-permute-start.11 = (bf16[16,160,128]{2,1,0:T(8,128)(2,1)S(1)}, bf16[16,160,128]{2,1,0:T(8,128)(2,1)S(1)}, u32[]{:S(2)}, u32[]{:S(2)}) collective-permute-start(bf16[16,160,128]{2,1,0:T(8,128)(2,1)S(1)} %slice.14.w0_ref), channel_id=1, source_target_pairs={{0,16},{8,24},{16,0},{24,8},{1,17},{9,25},{17,1},{25,9},{2,18},{10... | collective-permute-start | bytes 1966088 | tf_op jit(solution)/shard_map/ppermute | solution.py:84
  52.7 58.1 %collective-permute-start.12 = (bf16[16,160,128]{2,1,0:T(8,128)(2,1)S(1)}, bf16[16,160,128]{2,1,0:T(8,128)(2,1)}, u32[]{:S(2)}, u32[]{:S(2)}) collective-permute-start(bf16[16,160,128]{2,1,0:T(8,128)(2,1)S(1)} %slice.14.w0_ref), channel_id=1, source_target_pairs={{0,24},{8,0},{16,8},{24,16},{1,25},{9,1},{17,9},{25,17},{2,26},{10... | collective-permute-start | bytes 1966088 | tf_op jit(solution)/shard_map/ppermute | solution.py:84
  56.7 4.1 %collective-permute-start = (bf16[16,2048]{1,0:T(8,128)(2,1)S(1)}, bf16[16,2048]{1,0:T(8,128)(2,1)S(1)}, u32[]{:S(2)}, u32[]{:S(2)}) collective-permute-start(bf16[16,2048]{1,0:T(8,128)(2,1)S(1)} %slice.12), channel_id=1, source_target_pairs={{0,32},{32,64},{64,96},{96,128},{128,160},{160,192},{192,224},{224... | collective-permute-start | bytes 196616 | tf_op jit(solution)/shard_map/ppermute | solution.py:367
  58.6 24.1 %collective-permute-start.2 = (bf16[16,64,128]{2,1,0:T(8,128)(2,1)S(1)}, bf16[16,64,128]{2,1,0:T(8,128)(2,1)S(1)}, u32[]{:S(2)}, u32[]{:S(2)}) collective-permute-start(bf16[16,64,128]{2,1,0:T(8,128)(2,1)S(1)} %slice.13.w0_ref), channel_id=1, source_target_pairs={{0,16},{8,24},{16,0},{24,8},{1,17},{9,25},{17,1},{25,9},{2,18},{10... | collective-permute-start | bytes 786440 | tf_op jit(solution)/shard_map/ppermute | solution.py:84
  60.8 29.6 %collective-permute-start.3 = (bf16[16,64,128]{2,1,0:T(8,128)(2,1)S(1)}, bf16[16,64,128]{2,1,0:T(8,128)(2,1)S(1)}, u32[]{:S(2)}, u32[]{:S(2)}) collective-permute-start(bf16[16,64,128]{2,1,0:T(8,128)(2,1)S(1)} %slice.13.w0_ref), channel_id=1, source_target_pairs={{0,24},{8,0},{16,8},{24,16},{1,25},{9,1},{17,9},{25,17},{2,26},{10... | collective-permute-start | bytes 786440 | tf_op jit(solution)/shard_map/ppermute | solution.py:84
  95.6 5.0 %collective-permute-start.4 = (bf16[128,256]{1,0:T(8,128)(2,1)S(1)}, bf16[128,256]{1,0:T(8,128)(2,1)S(1)}, u32[]{:S(2)}, u32[]{:S(2)}) collective-permute-start(bf16[128,256]{1,0:T(8,128)(2,1)S(1)} %get-tuple-element.33.own_ref), channel_id=1, source_target_pairs={{0,32},{32,0},{64,96},{96,64},{128,160},{160,128},{192,224},{224,1... | collective-permute-start | bytes 196616 | tf_op jit(solution)/shard_map/ppermute | solution.py:399
  100.8 6.6 %collective-permute-start.5 = (bf16[128,256]{1,0:T(8,128)(2,1)S(1)}, bf16[128,256]{1,0:T(8,128)(2,1)S(1)}, u32[]{:S(2)}, u32[]{:S(2)}) collective-permute-start(bf16[128,256]{1,0:T(8,128)(2,1)S(1)} %get-tuple-element.34.own_ref), channel_id=1, source_target_pairs={{0,64},{32,96},{64,0},{96,32},{128,192},{160,224},{192,128},{224,1... | collective-permute-start | bytes 196616 | tf_op jit(solution)/shard_map/ppermute | solution.py:399
  107.6 19.4 %collective-permute-start.6 = (bf16[128,256]{1,0:T(8,128)(2,1)S(1)}, bf16[128,256]{1,0:T(8,128)(2,1)S(1)}, u32[]{:S(2)}, u32[]{:S(2)}) collective-permute-start(bf16[128,256]{1,0:T(8,128)(2,1)S(1)} %get-tuple-element.36), channel_id=1, source_target_pairs={{0,128},{32,160},{64,192},{96,224},{128,256},{160,288},{192,320},{... | collective-permute-start | bytes 196616 | tf_op jit(solution)/shard_map/ppermute | solution.py:420
  110.9 13.9 %copy-start = (bf16[1,128,128]{2,1,0:T(8,128)(2,1)S(1)}, bf16[1,128,128]{2,1,0:T(8,128)(2,1)}, u32[]{:S(2)}) copy-start(bf16[1,128,128]{2,1,0:T(8,128)(2,1)} %param.29) | copy-start | bytes 98308
  110.9 13.9 %copy-start.5 = (f32[128]{0:T(128)S(1)}, f32[128]{0:T(128)}, u32[]{:S(2)}) copy-start(f32[128]{0:T(128)} %param.30) | copy-start | bytes 1540
  113.5 13.5 %collective-permute-start.8 = (bf16[128,128]{1,0:T(8,128)(2,1)S(1)}, bf16[128,128]{1,0:T(8,128)(2,1)S(1)}, u32[]{:S(2)}, u32[]{:S(2)}) collective-permute-start(bf16[128,128]{1,0:T(8,128)(2,1)S(1)} %get-tuple-element.38), channel_id=1, source_target_pairs={{0,256},{32,288},{64,320},{96,352},{128,384},{160,416},{192,448},{... | collective-permute-start | bytes 98312 | tf_op jit(solution)/shard_map/ppermute | solution.py:420
  122.7 4.3 %collective-permute-start.9 = (bf16[128,128]{1,0:T(8,128)(2,1)S(1)}, bf16[128,128]{1,0:T(8,128)(2,1)S(1)}, u32[]{:S(2)}, u32[]{:S(2)}) collective-permute-start(bf16[128,128]{1,0:T(8,128)(2,1)S(1)} %get-tuple-element.38), channel_id=1, source_target_pairs={{0,384},{32,416},{64,448},{96,480},{1,385},{33,417},{65,449},{97,4... | collective-permute-start | bytes 98312 | tf_op jit(solution)/shard_map/ppermute | solution.py:420
  124.0 2.9 %collective-permute-start.7 = (bf16[128,128]{1,0:T(8,128)(2,1)S(1)}, bf16[128,128]{1,0:T(8,128)(2,1)S(1)}, u32[]{:S(2)}, u32[]{:S(2)}) collective-permute-start(bf16[128,128]{1,0:T(8,128)(2,1)S(1)} %get-tuple-element.37), channel_id=1, source_target_pairs={{128,384},{160,416},{192,448},{224,480},{129,385},{161,417},{193,4... | collective-permute-start | bytes 98312 | tf_op jit(solution)/shard_map/ppermute | solution.py:420
  124.7 2.3 %copy-start.6 = (f32[128]{0:T(128)S(1)}, f32[128]{0:T(128)}, u32[]{:S(2)}) copy-start(f32[128]{0:T(128)} %param.31) | copy-start | bytes 1540
  128.2 9.5 %collective-permute-start.13 = (bf16[4,32,2048]{2,1,0:T(8,128)(2,1)S(1)}, bf16[4,32,2048]{2,1,0:T(8,128)(2,1)S(1)}, u32[]{:S(2)}, u32[]{:S(2)}) collective-permute-start(bf16[4,32,2048]{2,1,0:T(8,128)(2,1)S(1)} %get-tuple-element.48), channel_id=1, source_target_pairs={{0,1},{1,0},{2,3},{3,2},{4,5},{5,4},{6,7},{7,6},{8,9},{9,8},{10,11... | collective-permute-start | bytes 1572872 | tf_op jit(solution)/shard_map/ppermute | solution.py:457

commit v5 on v4

--- a/solution.py
+++ b/solution.py
@@ -46,6 +46,11 @@
     ah, al = split(a)
     bh, bl = split(b)
     return dot(ah, bh, dims) + (dot(ah, bl, dims) + dot(al, bh, dims))
+
+
+def product(a, b):
+    (ah, al), (bh, bl) = a, b
+    return dot(jnp.concatenate([ah, al], axis=1), jnp.concatenate([bh, bh], axis=0)) + dot(ah, bl)
 
 
 def start_kernel(
@@ -149,12 +154,14 @@
 def inverse_unit_lower(low, size):
     r = lax.broadcasted_iota(jnp.int32, (size, size), 0)
     c = lax.broadcasted_iota(jnp.int32, (size, size), 1)
-    inv = [jnp.where(r == c, 1.0, 0.0) - jnp.where((r // 2 == c // 2) & (r > c), x, 0.0) for x in low]
+    apart = r ^ c
+    inv = [jnp.where(apart == 0, 1.0, jnp.where(apart == 1, -x, 0.0)) for x in low]
     b = 2
     while b < size:
-        mask = (r // (2 * b) == c // (2 * b)) & (r % (2 * b) >= b) & (c % (2 * b) < b)
-        mid = [dot3(x, jnp.where(mask, y, 0.0)) for x, y in zip(inv, low)]
-        inv = [x - dot3(y, x) for x, y in zip(inv, mid)]
+        here = (apart >= b) & (apart < 2 * b)
+        parts = [split(x) for x in inv]
+        mid = [product(x, split(jnp.where(here, y, 0.0))) for x, y in zip(parts, low)]
+        inv = [x - product(split(y), p) for x, y, p in zip(inv, mid, parts)]
         b *= 2
     return inv
 
@@ -195,38 +202,82 @@
     ab_ref[:, width:] = made[:, :width].astype(BF16)
 
 
-def query_kernel(
-    sp_ref, tp_ref, fs_ref, xn_ref, w0_ref, w1_ref, w2_ref, w3_ref, taps_ref, gc_ref, decay_ref, k_ref, uw_ref,
-    own_ref, eff_ref, silu_ref,
-    w_scr, q_scr,
+def step_map(later, carry, width):
+    ch, cl = split(carry)
+    linear = later[:, :width]
+    moved = dot(linear, ch) + dot(linear, cl)
+    offset = later[:, width:].astype(F32)
+    return jnp.concatenate([moved[:, :width], moved[:, width:] + offset], axis=1)
+
+
+def pair_map_kernel(sp_ref, tp_ref, fs_ref, own_ref, other_ref, pair_ref, before_ref):
+    width = own_ref.shape[0]
+    odd = sp_ref[0] % 2 == 1
+    own, other = own_ref[...], other_ref[...]
+    earlier = jnp.where(odd, other, own)
+    later = jnp.where(odd, own, other)
+    pair_ref[...] = step_map(later, earlier.astype(F32), width).astype(BF16)
+    r = lax.broadcasted_iota(jnp.int32, (width, 2 * width), 0)
+    c = lax.broadcasted_iota(jnp.int32, (width, 2 * width), 1)
+    before_ref[...] = jnp.where(odd, other, jnp.where(r == c, 1.0, 0.0).astype(BF16))
+
+
+def group_kernel(
+    sp_ref, tp_ref, fs_ref, own_ref, other_ref, inner_ref,
+    total_ref, linear_ref, offset_ref, before_ref,
+):
+    width = own_ref.shape[0]
+    upper = (sp_ref[0] // 2) % 2 == 1
+    own, other = own_ref[...], other_ref[...]
+    earlier = jnp.where(upper, other, own)
+    later = jnp.where(upper, own, other)
+    total = step_map(later, earlier.astype(F32), width).astype(BF16)
+    total_ref[...] = total
+    linear_ref[...] = total[:, :width]
+    offset_ref[...] = total[:, width:]
+    inner = inner_ref[...]
+    behind = step_map(inner, other.astype(F32), width)
+    before_ref[...] = jnp.where(upper, behind, inner.astype(F32))
+
+
+def apply(linear, state):
+    high, low = split(state)
+    return dot(linear, high) + dot(linear, low)
+
+
+def output_kernel(
+    sp_ref, tp_ref, fs_ref, xn_ref, w0_ref, w1_ref, w2_ref, w3_ref, taps_ref, gc_ref, decay_ref,
+    k_ref, uw_ref, mix_ref, scale_ref, t4_ref, a8_ref, b8_ref, b12_ref, before_ref, gain_ref,
+    mine_ref, other_ref,
+    w_scr, w_all, q_scr, a_scr, b_scr,
 ):
     length, width = k_ref.shape
-    gather_two(fs_ref[0], (w0_ref, w1_ref, w2_ref, w3_ref), w_scr)
-    raw = dot(xn_ref[...], w_scr[...])
-    query = unit_rows(short_conv(raw[:, :width], taps_ref[0], length, q_scr)) * width ** (-0.5)
-    silu_ref[...] = jax.nn.silu(raw[HALO:, width:].astype(BF16).astype(F32))
-    scores = dot3(query, k_ref[...], ((1,), (1,))) * decay_ref[...]
-    both = dot3(scores, uw_ref[...])
-    own_ref[...] = both[:, :width]
-    eff_ref[...] = query * jnp.exp(gc_ref[...]) - both[:, width:]
-
-
-def pool_kernel(
-    sp_ref, tp_ref, fs_ref, xn_ref, w0_ref, w1_ref, w2_ref, w3_ref, mix_ref, scale_ref,
-    out_ref, wo_ref, w_all, w_scr, a_scr, b_scr,
-):
-    count, part, width = w0_ref.shape
+    pieces = (w0_ref, w1_ref, w2_ref, w3_ref)
+    state = apply(a8_ref[...], b12_ref[...].astype(F32)) + b8_ref[...].astype(F32)
+    state = apply(t4_ref[:, :width], state) + t4_ref[:, width:].astype(F32)
+    state = dot3(before_ref[:, :width], state) + before_ref[:, width:]
+    gather_two(fs_ref[0], pieces, w_scr)
+    count, part, _ = w0_ref.shape
     skip = width // 2
     part = part - skip
-    length = xn_ref.shape[0] - HALO
-    for d, piece in enumerate((w0_ref, w1_ref, w2_ref, w3_ref)):
+    for d, piece in enumerate(pieces):
         at = pl.multiple_of(((fs_ref[0] + 4 - d) % 4) * part, 32)
         for s in range(count):
             w_all[pl.ds(at, part), s * width : (s + 1) * width] = piece[s, skip:]
     for s in range(count):
-        w_scr[s * width : (s + 1) * width, :] = w_all[0:width, s * width : (s + 1) * width]
-    wo_ref[...] = w_all[width:, :]
-    x = dot(xn_ref[...], w_scr[...]).astype(BF16).astype(F32)
+        w_scr[s * width : (s + 1) * width, 2 * width :] = w_all[
+            0:width, s * width : (s + 1) * width
+        ]
+    raw = dot(xn_ref[...], w_scr[...])
+    query = unit_rows(short_conv(raw[:, :width], taps_ref[0], length, q_scr)) * width ** (-0.5)
+    silu_gate = jax.nn.silu(raw[HALO:, width : 2 * width].astype(BF16).astype(F32))
+    scores = dot3(query, k_ref[...], ((1,), (1,))) * decay_ref[...]
+    both = dot3(scores, uw_ref[...])
+    effect = query * jnp.exp(gc_ref[...]) - both[:, width:]
+    attended = both[:, :width] + dot3(effect, state)
+    scale = lax.rsqrt(jnp.mean(attended * attended, axis=-1, keepdims=True) + EPS)
+    delta = (attended * scale * gain_ref[...] * silu_gate).astype(BF16)
+    x = raw[:, 2 * width :].astype(BF16).astype(F32)
     kind = tp_ref[0] % 4
     total = HALO + length
     a_scr[0:HALO] = jnp.zeros((HALO, width), F32)
@@ -239,78 +290,24 @@
     eight = four + a_scr[HALO - 4 : HALO - 4 + total]
     b_scr[HALO:] = eight
     sixteen = eight + b_scr[HALO - 8 : HALO - 8 + total]
-    window = jnp.where(kind == 0, two, jnp.where(kind == 1, four, jnp.where(kind == 2, eight, sixteen)))
+    window = jnp.where(
+        kind == 0, two, jnp.where(kind == 1, four, jnp.where(kind == 2, eight, sixteen))
+    )
     window = window[HALO:]
     place = sp_ref[0] * length + lax.broadcasted_iota(jnp.int32, (length, width), 0)
     span = jnp.where(kind == 0, 2, jnp.where(kind == 1, 4, jnp.where(kind == 2, 8, 16)))
     counts = jnp.minimum(place + 1, span).astype(F32)
     pooled = (window / counts - x[HALO:]).astype(BF16)
-    out_ref[...] = (dot(pooled, mix_ref[...]) * scale_ref[...]).astype(BF16)
-
-
-def step_map(later, carry, width):
-    ch, cl = split(carry)
-    linear = later[:, :width]
-    moved = dot(linear, ch) + dot(linear, cl)
-    offset = later[:, width:].astype(F32)
-    return jnp.concatenate([moved[:, :width], moved[:, width:] + offset], axis=1)
-
-
-def pair_map_kernel(sp_ref, tp_ref, fs_ref, own_ref, other_ref, pair_ref, before_ref):
-    width = own_ref.shape[0]
-    odd = sp_ref[0] % 2 == 1
-    own, other = own_ref[...], other_ref[...]
-    earlier = jnp.where(odd, other, own)
-    later = jnp.where(odd, own, other)
-    pair_ref[...] = step_map(later, earlier.astype(F32), width).astype(BF16)
-    r = lax.broadcasted_iota(jnp.int32, (width, 2 * width), 0)
-    c = lax.broadcasted_iota(jnp.int32, (width, 2 * width), 1)
-    before_ref[...] = jnp.where(odd, other, jnp.where(r == c, 1.0, 0.0).astype(BF16))
-
-
-def group_kernel(
-    sp_ref, tp_ref, fs_ref, own_ref, other_ref, inner_ref,
-    total_ref, linear_ref, offset_ref, before_ref,
-):
-    width = own_ref.shape[0]
-    upper = (sp_ref[0] // 2) % 2 == 1
-    own, other = own_ref[...], other_ref[...]
-    earlier = jnp.where(upper, other, own)
-    later = jnp.where(upper, own, other)
-    total = step_map(later, earlier.astype(F32), width).astype(BF16)
-    total_ref[...] = total
-    linear_ref[...] = total[:, :width]
-    offset_ref[...] = total[:, width:]
-    inner = inner_ref[...]
-    behind = step_map(inner, other.astype(F32), width)
-    before_ref[...] = jnp.where(upper, behind, inner.astype(F32))
-
-
-def apply(linear, state):
-    high, low = split(state)
-    return dot(linear, high) + dot(linear, low)
-
-
-def attend_kernel(
-    sp_ref, tp_ref, fs_ref, t4_ref, a8_ref, b8_ref, b12_ref, before_ref, own_ref, eff_ref, silu_ref, gain_ref,
-    pool_ref, wo_ref, mine_ref, other_ref,
-):
-    width = b8_ref.shape[0]
-    state = apply(a8_ref[...], b12_ref[...].astype(F32)) + b8_ref[...].astype(F32)
-    state = apply(t4_ref[:, :width], state) + t4_ref[:, width:].astype(F32)
-    state = dot3(before_ref[:, :width], state) + before_ref[:, width:]
-    attended = own_ref[...] + dot3(eff_ref[...], state)
-    scale = lax.rsqrt(jnp.mean(attended * attended, axis=-1, keepdims=True) + EPS)
-    delta = (attended * scale * gain_ref[...] * silu_ref[...]).astype(BF16)
-    both = jnp.concatenate([pool_ref[...], delta], axis=1)
+    pool_out = (dot(pooled, mix_ref[...]) * scale_ref[...]).astype(BF16)
+    channels = jnp.concatenate([pool_out, delta], axis=1)
     core = tp_ref[0] % 2
     chips, rows, cols = mine_ref.shape
     step = 512
     for at in range(0, cols, step):
-        part = dot(both, wo_ref[:, at : at + step]).astype(BF16)
+        made = dot(channels, w_all[width:, at : at + step]).astype(BF16)
         for j in range(chips):
-            even = part[2 * j * rows : (2 * j + 1) * rows]
-            odd = part[(2 * j + 1) * rows : (2 * j + 2) * rows]
+            even = made[2 * j * rows : (2 * j + 1) * rows]
+            odd = made[(2 * j + 1) * rows : (2 * j + 2) * rows]
             mine_ref[j, :, at : at + step] = jnp.where(core == 0, even, odd)
             other_ref[j, :, at : at + step] = jnp.where(core == 0, odd, even)
 
@@ -424,35 +421,20 @@
     a8 = from_behind(linear, quad, n_sp - 2 * quad, 2 * quad)
     b12 = from_behind(offset, 0, n_sp - 3 * quad, 3 * quad)
 
-    own, eff, silu_gate = call(
-        query_kernel,
-        (shape(length, width), shape(length, width), shape(length, width)),
-        *ids, xn, *rest, conv_weight, gc, decay, keys, uw,
+    chips = n_tp // 2
+    mine, other = call(
+        output_kernel,
+        (shape(chips, rows, model, dtype=BF16), shape(chips, rows, model, dtype=BF16)),
+        *ids, xn, *rest, conv_weight, gc, decay, keys, uw, w_mix[0], pool_scale.reshape(1, width),
+        t4, a8, b8, b12, before, delta_gain.reshape(1, width),
         scratch=[
-            pltpu.VMEM((model, 2 * width), BF16),
+            pltpu.VMEM((model, 3 * width), BF16),
+            pltpu.VMEM((3 * width, model), BF16),
             pltpu.VMEM((HALO + length, width), F32),
-        ],
-        flops=8 * length * model * width,
-    )
-    pool_out, w_mine = call(
-        pool_kernel,
-        (shape(length, width, dtype=BF16), shape(2 * width, model, dtype=BF16)),
-        *ids, xn, *rest, w_mix[0], pool_scale.reshape(1, width),
-        scratch=[
-            pltpu.VMEM((3 * width, model), BF16),
-            pltpu.VMEM((model, width), BF16),
             pltpu.VMEM((2 * HALO + length, width), F32),
             pltpu.VMEM((2 * HALO + length, width), F32),
         ],
-        flops=8 * length * model * width,
-    )
-    chips = n_tp // 2
-    mine, other = call(
-        attend_kernel,
-        (shape(chips, rows, model, dtype=BF16), shape(chips, rows, model, dtype=BF16)),
-        *ids, t4, a8, b8, b12, before, own, eff, silu_gate, delta_gain.reshape(1, width), pool_out,
-        w_mine,
-        flops=4 * length * model * width,
+        flops=20 * length * model * width,
     )
     theirs = lax.ppermute(other, "tp", [(i, i ^ 1) for i in range(n_tp)])
     partial = call(

time: 152 us -> 150 us (0.987)
  waiting for transfers between devices: 33.3 us -> 37.1 us
  Pallas kernels: 15.7 us -> 12.4 us
    pallas_call x10 -> x8, Pallas kernels: 15.7 us -> 12.4 us  [call(): pl.pallas_call(kernel, out_shape=list(outs) if many else outs, in_specs=i...]
    ppermute x6, waiting for transfers between devices: 24.4 us -> 27.1 us  [turns(): lax.ppermute(x, axis, [(i, i - i % size + (i + d) % size) for i in range(...]
  transfers between devices with their start and end apart: 15 -> 15, of which waited for: 5 -> 6; matrix products, arithmetic and copies ran while one was open for 0% -> 0% of each run, Pallas kernels for 8% -> 4%
where the time goes in v5:
time: 150 us
  starting transfers between devices  56.9 us (38%)
  blocking collectives  42.2 us (28%)
  waiting for transfers between devices  37.1 us (25%)
  Pallas kernels  12.4 us (8%)
    all_gather x1, blocking collectives, layer(): quarters = lax.all_gather(part, 'sp', axis=0)  30.2 us
    ppermute x6, waiting for transfers between devices, turns(): lax.ppermute(x, axis, [(i, i - i % size + (i + d) % size) for i in range(...  27.1 us
    ppermute x6, starting transfers between devices, turns(): lax.ppermute(x, axis, [(i, i - i % size + (i + d) % size) for i in range(...  19.4 us
    ppermute x4, starting transfers between devices, from_behind(): lax.ppermute(x, 'sp', [(i, i + distance) for i in range(first, last)])  13.9 us
    pallas_call x8, Pallas kernels, call(): pl.pallas_call(kernel, out_shape=list(outs) if many else outs, in_specs=i...  12.4 us
    all_to_all x1, blocking collectives, exchange(): lax.all_to_all(copies, axis, split_axis=0, concat_axis=0, tiled=True, axi...  12 us
    all_to_all x1, starting transfers between devices, exchange(): lax.all_to_all(copies, axis, split_axis=0, concat_axis=0, tiled=True, axi...  10.4 us
    ppermute x1, starting transfers between devices, layer(): theirs = lax.ppermute(other, 'tp', [(i, i ^ 1) for i in range(n_tp)])  7.53 us
  transfers between devices with their start and end apart: 15, of which 6 were waited for; matrix products, arithmetic and copies ran while one was open for 0% of the time, Pallas kernels for 4%

profile of v5, /device:TPU:1, one launch (start us, length us, event | category | flops | bytes accessed | tf_op | source)
XLA Modules:
  0.0 149.6 jit_solution(8186382957268107186)
XLA Ops:
  0.0 2.2 %shard_map.163 = (bf16[8,32,2048]{2,1,0:T(8,128)(2,1)}, bf16[224,128]{1,0:T(8,128)(2,1)}) custom-call(s32[1]{0:T(128)} %bitcast.sp_ref, s32[1]{0:T(128)} %bitcast.1.tp_ref, s32[1]{0:T(128)} %bitcast.2.fs_ref, bf16[32,2048]{1,0:T(8,128)(2,1)} %tok_ref.1, bf16[2048]{0:T(1024)(128)(2,1)} %gain_ref.1, bf16[128,128]{1,0:T(8,128)(2,1)} %k_ref.1, ...), custom_call_target="tpu_custom_call" | custom-call | tf_op jit(solution)/shard_map/pallas_call | solution.py:21
  2.2 10.4 %all-to-all-start = ((bf16[8,32,2048]{2,1,0:T(8,128)(2,1)}), bf16[8,32,2048]{2,1,0:T(8,128)(2,1)S(1)}, u32[]{:S(2)}, u32[]{:S(2)}) async-start(bf16[8,32,2048]{2,1,0:T(8,128)(2,1)} %get-tuple-element.22), calls=%async_computation | async-start | bytes 2097152 | tf_op jit(solution)/shard_map/all_to_all | solution.py:80
  12.6 30.2 %all-gather = bf16[3584,128]{1,0:T(8,128)(2,1)S(1)} all-gather(bf16[224,128]{1,0:T(8,128)(2,1)S(1)} %copy-done.7), channel_id=2, replica_groups=mesh['sp'=16,'fs'=4,'tp'=8] {'sp'}, dimensions={0}, use_global_device_ids=true | all-gather | bytes 974848 | tf_op jit(solution)/shard_map/all_gather | solution.py:367
  42.8 4.8 %collective-permute-start.6 = (bf16[16,64,128]{2,1,0:T(8,128)(2,1)S(1)}, bf16[16,64,128]{2,1,0:T(8,128)(2,1)}, u32[]{:S(2)}, u32[]{:S(2)}) collective-permute-start(bf16[16,64,128]{2,1,0:T(8,128)(2,1)S(1)} %slice.14.w0_ref), channel_id=1, source_target_pairs={{0,24},{8,0},{16,8},{24,16},{1,25},{9,1},{17,9},{25,17},{2,26},{10... | collective-permute-start | bytes 786440 | tf_op jit(solution)/shard_map/ppermute | solution.py:89
  47.7 2.4 %collective-permute-start.3 = (bf16[16,160,128]{2,1,0:T(8,128)(2,1)S(1)}, bf16[16,160,128]{2,1,0:T(8,128)(2,1)S(1)}, u32[]{:S(2)}, u32[]{:S(2)}) collective-permute-start(bf16[16,160,128]{2,1,0:T(8,128)(2,1)S(1)} %slice.13.w0_ref), channel_id=1, source_target_pairs={{0,24},{8,0},{16,8},{24,16},{1,25},{9,1},{17,9},{25,17},{2,26},{10... | collective-permute-start | bytes 1966088 | tf_op jit(solution)/shard_map/ppermute | solution.py:89
  50.1 1.9 %collective-permute-start.2 = (bf16[16,160,128]{2,1,0:T(8,128)(2,1)S(1)}, bf16[16,160,128]{2,1,0:T(8,128)(2,1)S(1)}, u32[]{:S(2)}, u32[]{:S(2)}) collective-permute-start(bf16[16,160,128]{2,1,0:T(8,128)(2,1)S(1)} %slice.13.w0_ref), channel_id=1, source_target_pairs={{0,16},{8,24},{16,0},{24,8},{1,17},{9,25},{17,1},{25,9},{2,18},{10... | collective-permute-start | bytes 1966088 | tf_op jit(solution)/shard_map/ppermute | solution.py:89
  52.0 1.8 %collective-permute-start = (bf16[16,2048]{1,0:T(8,128)(2,1)S(1)}, bf16[16,2048]{1,0:T(8,128)(2,1)S(1)}, u32[]{:S(2)}, u32[]{:S(2)}) collective-permute-start(bf16[16,2048]{1,0:T(8,128)(2,1)S(1)} %slice.12), channel_id=1, source_target_pairs={{0,32},{32,64},{64,96},{96,128},{128,160},{160,192},{192,224},{224... | collective-permute-start | bytes 196616 | tf_op jit(solution)/shard_map/ppermute | solution.py:364
  53.9 2.9 %collective-permute-start.1 = (bf16[16,160,128]{2,1,0:T(8,128)(2,1)S(1)}, bf16[16,160,128]{2,1,0:T(8,128)(2,1)S(1)}, u32[]{:S(2)}, u32[]{:S(2)}) collective-permute-start(bf16[16,160,128]{2,1,0:T(8,128)(2,1)S(1)} %slice.13.w0_ref), channel_id=1, source_target_pairs={{0,8},{8,16},{16,24},{24,0},{1,9},{9,17},{17,25},{25,1},{2,10},{10... | collective-permute-start | bytes 1966088 | tf_op jit(solution)/shard_map/ppermute | solution.py:89
  56.8 5.5 %collective-permute-start.5 = (bf16[16,64,128]{2,1,0:T(8,128)(2,1)S(1)}, bf16[16,64,128]{2,1,0:T(8,128)(2,1)S(1)}, u32[]{:S(2)}, u32[]{:S(2)}) collective-permute-start(bf16[16,64,128]{2,1,0:T(8,128)(2,1)S(1)} %slice.14.w0_ref), channel_id=1, source_target_pairs={{0,16},{8,24},{16,0},{24,8},{1,17},{9,25},{17,1},{25,9},{2,18},{10... | collective-permute-start | bytes 786440 | tf_op jit(solution)/shard_map/ppermute | solution.py:89
  62.3 1.9 %collective-permute-start.4 = (bf16[16,64,128]{2,1,0:T(8,128)(2,1)S(1)}, bf16[16,64,128]{2,1,0:T(8,128)(2,1)S(1)}, u32[]{:S(2)}, u32[]{:S(2)}) collective-permute-start(bf16[16,64,128]{2,1,0:T(8,128)(2,1)S(1)} %slice.14.w0_ref), channel_id=1, source_target_pairs={{0,8},{8,16},{16,24},{24,0},{1,9},{9,17},{17,25},{25,1},{2,10},{10... | collective-permute-start | bytes 786440 | tf_op jit(solution)/shard_map/ppermute | solution.py:89
  66.1 16.2 %collective-permute-done.5.w2_ref = bf16[16,64,128]{2,1,0:T(8,128)(2,1)S(1)} collective-permute-done((bf16[16,64,128]{2,1,0:T(8,128)(2,1)S(1)}, bf16[16,64,128]{2,1,0:T(8,128)(2,1)S(1)}, u32[]{:S(2)}, u32[]{:S(2)}) %collective-permute-start.5) | collective-permute-done | bytes 262176 | tf_op jit(solution)/shard_map/ppermute | solution.py:89
  82.4 10.8 %collective-permute-done.4.w1_ref = bf16[16,64,128]{2,1,0:T(8,128)(2,1)S(1)} collective-permute-done((bf16[16,64,128]{2,1,0:T(8,128)(2,1)S(1)}, bf16[16,64,128]{2,1,0:T(8,128)(2,1)S(1)}, u32[]{:S(2)}, u32[]{:S(2)}) %collective-permute-start.4) | collective-permute-done | bytes 262176 | tf_op jit(solution)/shard_map/ppermute | solution.py:89
  93.2 5.1 %shard_map.165 = (bf16[128,256]{1,0:T(8,128)(2,1)S(1)}, f32[256,128]{1,0:T(8,128)S(1)}, f32[256,256]{1,0:T(8,128)S(1)}) custom-call(s32[1]{0:T(128)} %bitcast.sp_ref, s32[1]{0:T(128)} %bitcast.1.tp_ref, s32[1]{0:T(128)} %bitcast.2.fs_ref, bf16[272,2048]{1,0:T(8,128)(2,1)S(1)} %get-tuple-element.23.xn_ref, bf16[16,64,128]{2,1,0:T(8,128)(2,1)S(1)} %slice.14.w0_ref, ...), custom_call_target="tpu_custom_call" | custom-call | flops 1342177280 | tf_op jit(solution)/shard_map/pallas_call | solution.py:21
  98.3 1.9 %collective-permute-start.7 = (bf16[128,256]{1,0:T(8,128)(2,1)S(1)}, bf16[128,256]{1,0:T(8,128)(2,1)S(1)}, u32[]{:S(2)}, u32[]{:S(2)}) collective-permute-start(bf16[128,256]{1,0:T(8,128)(2,1)S(1)} %get-tuple-element.30.own_ref), channel_id=1, source_target_pairs={{0,32},{32,0},{64,96},{96,64},{128,160},{160,128},{192,224},{224,1... | collective-permute-start | bytes 196616 | tf_op jit(solution)/shard_map/ppermute | solution.py:396
  100.2 3.1 %collective-permute-done.7.other_ref = bf16[128,256]{1,0:T(8,128)(2,1)S(1)} collective-permute-done((bf16[128,256]{1,0:T(8,128)(2,1)S(1)}, bf16[128,256]{1,0:T(8,128)(2,1)S(1)}, u32[]{:S(2)}, u32[]{:S(2)}) %collective-permute-start.7) | collective-permute-done | bytes 65568 | tf_op jit(solution)/shard_map/ppermute | solution.py:396
  103.5 1.9 %collective-permute-start.8 = (bf16[128,256]{1,0:T(8,128)(2,1)S(1)}, bf16[128,256]{1,0:T(8,128)(2,1)S(1)}, u32[]{:S(2)}, u32[]{:S(2)}) collective-permute-start(bf16[128,256]{1,0:T(8,128)(2,1)S(1)} %get-tuple-element.31.own_ref), channel_id=1, source_target_pairs={{0,64},{32,96},{64,0},{96,32},{128,192},{160,224},{192,128},{224,1... | collective-permute-start | bytes 196616 | tf_op jit(solution)/shard_map/ppermute | solution.py:396
  105.5 4.4 %collective-permute-done.8.other_ref = bf16[128,256]{1,0:T(8,128)(2,1)S(1)} collective-permute-done((bf16[128,256]{1,0:T(8,128)(2,1)S(1)}, bf16[128,256]{1,0:T(8,128)(2,1)S(1)}, u32[]{:S(2)}, u32[]{:S(2)}) %collective-permute-start.8) | collective-permute-done | bytes 65568 | tf_op jit(solution)/shard_map/ppermute | solution.py:396
  110.1 2.8 %collective-permute-start.9 = (bf16[128,256]{1,0:T(8,128)(2,1)S(1)}, bf16[128,256]{1,0:T(8,128)(2,1)S(1)}, u32[]{:S(2)}, u32[]{:S(2)}) collective-permute-start(bf16[128,256]{1,0:T(8,128)(2,1)S(1)} %get-tuple-element.33), channel_id=1, source_target_pairs={{0,128},{32,160},{64,192},{96,224},{128,256},{160,288},{192,320},{... | collective-permute-start | bytes 196616 | tf_op jit(solution)/shard_map/ppermute | solution.py:417
  113.6 4.7 %collective-permute-start.12 = (bf16[128,128]{1,0:T(8,128)(2,1)S(1)}, bf16[128,128]{1,0:T(8,128)(2,1)S(1)}, u32[]{:S(2)}, u32[]{:S(2)}) collective-permute-start(bf16[128,128]{1,0:T(8,128)(2,1)S(1)} %get-tuple-element.35), channel_id=1, source_target_pairs={{0,384},{32,416},{64,448},{96,480},{1,385},{33,417},{65,449},{97,4... | collective-permute-start | bytes 98312 | tf_op jit(solution)/shard_map/ppermute | solution.py:417
  118.3 5.7 %collective-permute-start.11 = (bf16[128,128]{1,0:T(8,128)(2,1)S(1)}, bf16[128,128]{1,0:T(8,128)(2,1)S(1)}, u32[]{:S(2)}, u32[]{:S(2)}) collective-permute-start(bf16[128,128]{1,0:T(8,128)(2,1)S(1)} %get-tuple-element.35), channel_id=1, source_target_pairs={{0,256},{32,288},{64,320},{96,352},{128,384},{160,416},{192,448},{... | collective-permute-start | bytes 98312 | tf_op jit(solution)/shard_map/ppermute | solution.py:417
  125.1 2.7 %shard_map.168 = (bf16[4,32,2048]{2,1,0:T(8,128)(2,1)S(1)}, bf16[4,32,2048]{2,1,0:T(8,128)(2,1)S(1)}) custom-call(s32[1]{0:T(128)} %bitcast.sp_ref, s32[1]{0:T(128)} %bitcast.1.tp_ref, s32[1]{0:T(128)} %bitcast.2.fs_ref, bf16[272,2048]{1,0:T(8,128)(2,1)S(1)} %get-tuple-element.23.xn_ref, bf16[16,160,128]{2,1,0:T(8,128)(2,1)S(1)} %slice.13.w0_ref, ...), custom_call_target="tpu_custom_call" | custom-call | flops 1342177280 | tf_op jit(solution)/shard_map/pallas_call | solution.py:21
  127.7 7.5 %collective-permute-start.13 = (bf16[4,32,2048]{2,1,0:T(8,128)(2,1)S(1)}, bf16[4,32,2048]{2,1,0:T(8,128)(2,1)S(1)}, u32[]{:S(2)}, u32[]{:S(2)}) collective-permute-start(bf16[4,32,2048]{2,1,0:T(8,128)(2,1)S(1)} %get-tuple-element.38), channel_id=1, source_target_pairs={{0,1},{1,0},{2,3},{3,2},{4,5},{5,4},{6,7},{7,6},{8,9},{9,8},{10,11... | collective-permute-start | bytes 1572872 | tf_op jit(solution)/shard_map/ppermute | solution.py:439
  135.3 1.5 %collective-permute-done.13.theirs_ref = bf16[4,32,2048]{2,1,0:T(8,128)(2,1)S(1)} collective-permute-done((bf16[4,32,2048]{2,1,0:T(8,128)(2,1)S(1)}, bf16[4,32,2048]{2,1,0:T(8,128)(2,1)S(1)}, u32[]{:S(2)}, u32[]{:S(2)}) %collective-permute-start.13) | collective-permute-done | bytes 524320 | tf_op jit(solution)/shard_map/ppermute | solution.py:439
  136.9 12.0 %all_to_all.10.in_ref = bf16[4,32,2048]{2,1,0:T(8,128)(2,1)S(1)} all-to-all(bf16[4,32,2048]{2,1,0:T(8,128)(2,1)S(1)} %shard_map.169), channel_id=1, replica_groups={{0,2,4,6},{1,3,5,7},{8,10,12,14},{9,11,13,15},{16,18,20,22},{17,19,21,2..., dimensions={0} | all-to-all | bytes 1048576 | tf_op jit(solution)/shard_map/all_to_all | solution.py:80
  (35 shorter events, 4.3 us)
Async XLA Ops:
  2.2 10.4 %copy-start.7 = (bf16[224,128]{1,0:T(8,128)(2,1)S(1)}, bf16[224,128]{1,0:T(8,128)(2,1)}, u32[]{:S(2)}) copy-start(bf16[224,128]{1,0:T(8,128)(2,1)} %get-tuple-element.24) | copy-start | bytes 172036
  2.2 49.8 %all-to-all-start = ((bf16[8,32,2048]{2,1,0:T(8,128)(2,1)}), bf16[8,32,2048]{2,1,0:T(8,128)(2,1)S(1)}, u32[]{:S(2)}, u32[]{:S(2)}) async-start(bf16[8,32,2048]{2,1,0:T(8,128)(2,1)} %get-tuple-element.22), calls=%async_computation | async-start | bytes 2097152 | tf_op jit(solution)/shard_map/all_to_all | solution.py:80
  42.8 22.1 %copy-start = (bf16[2048,8]{0,1:T(8,128)(2,1)S(1)}, bf16[2048,8]{0,1:T(8,128)(2,1)}, u32[]{:S(2)}) copy-start(bf16[2048,8]{0,1:T(8,128)(2,1)} %param.24) | copy-start | bytes 98308
  42.8 22.1 %copy-start.1 = (bf16[2048,8]{0,1:T(8,128)(2,1)S(1)}, bf16[2048,8]{0,1:T(8,128)(2,1)}, u32[]{:S(2)}) copy-start(bf16[2048,8]{0,1:T(8,128)(2,1)} %param.25) | copy-start | bytes 98308
  42.8 22.1 %copy-start.2 = (f32[256,1]{0,1:T(1,128)S(1)}, f32[256,1]{0,1:T(1,128)}, u32[]{:S(2)}) copy-start(f32[256,1]{0,1:T(1,128)} %param.28) | copy-start | bytes 3076
  42.8 50.4 %copy-start.4 = (f32[3,4,128]{2,1,0:T(4,128)S(1)}, f32[3,4,128]{2,1,0:T(4,128)}, u32[]{:S(2)}) copy-start(f32[3,4,128]{2,1,0:T(4,128)} %taps_ref.3) | copy-start | bytes 18436
  42.8 14.0 %collective-permute-start.6 = (bf16[16,64,128]{2,1,0:T(8,128)(2,1)S(1)}, bf16[16,64,128]{2,1,0:T(8,128)(2,1)}, u32[]{:S(2)}, u32[]{:S(2)}) collective-permute-start(bf16[16,64,128]{2,1,0:T(8,128)(2,1)S(1)} %slice.14.w0_ref), channel_id=1, source_target_pairs={{0,24},{8,0},{16,8},{24,16},{1,25},{9,1},{17,9},{25,17},{2,26},{10... | collective-permute-start | bytes 786440 | tf_op jit(solution)/shard_map/ppermute | solution.py:89
  47.7 65.9 %collective-permute-start.3 = (bf16[16,160,128]{2,1,0:T(8,128)(2,1)S(1)}, bf16[16,160,128]{2,1,0:T(8,128)(2,1)S(1)}, u32[]{:S(2)}, u32[]{:S(2)}) collective-permute-start(bf16[16,160,128]{2,1,0:T(8,128)(2,1)S(1)} %slice.13.w0_ref), channel_id=1, source_target_pairs={{0,24},{8,0},{16,8},{24,16},{1,25},{9,1},{17,9},{25,17},{2,26},{10... | collective-permute-start | bytes 1966088 | tf_op jit(solution)/shard_map/ppermute | solution.py:89
  50.1 68.2 %collective-permute-start.2 = (bf16[16,160,128]{2,1,0:T(8,128)(2,1)S(1)}, bf16[16,160,128]{2,1,0:T(8,128)(2,1)S(1)}, u32[]{:S(2)}, u32[]{:S(2)}) collective-permute-start(bf16[16,160,128]{2,1,0:T(8,128)(2,1)S(1)} %slice.13.w0_ref), channel_id=1, source_target_pairs={{0,16},{8,24},{16,0},{24,8},{1,17},{9,25},{17,1},{25,9},{2,18},{10... | collective-permute-start | bytes 1966088 | tf_op jit(solution)/shard_map/ppermute | solution.py:89
  52.0 10.3 %collective-permute-start = (bf16[16,2048]{1,0:T(8,128)(2,1)S(1)}, bf16[16,2048]{1,0:T(8,128)(2,1)S(1)}, u32[]{:S(2)}, u32[]{:S(2)}) collective-permute-start(bf16[16,2048]{1,0:T(8,128)(2,1)S(1)} %slice.12), channel_id=1, source_target_pairs={{0,32},{32,64},{64,96},{96,128},{128,160},{160,192},{192,224},{224... | collective-permute-start | bytes 196616 | tf_op jit(solution)/shard_map/ppermute | solution.py:364
  53.9 70.2 %collective-permute-start.1 = (bf16[16,160,128]{2,1,0:T(8,128)(2,1)S(1)}, bf16[16,160,128]{2,1,0:T(8,128)(2,1)S(1)}, u32[]{:S(2)}, u32[]{:S(2)}) collective-permute-start(bf16[16,160,128]{2,1,0:T(8,128)(2,1)S(1)} %slice.13.w0_ref), channel_id=1, source_target_pairs={{0,8},{8,16},{16,24},{24,0},{1,9},{9,17},{17,25},{25,1},{2,10},{10... | collective-permute-start | bytes 1966088 | tf_op jit(solution)/shard_map/ppermute | solution.py:89
  56.8 25.6 %collective-permute-start.5 = (bf16[16,64,128]{2,1,0:T(8,128)(2,1)S(1)}, bf16[16,64,128]{2,1,0:T(8,128)(2,1)S(1)}, u32[]{:S(2)}, u32[]{:S(2)}) collective-permute-start(bf16[16,64,128]{2,1,0:T(8,128)(2,1)S(1)} %slice.14.w0_ref), channel_id=1, source_target_pairs={{0,16},{8,24},{16,0},{24,8},{1,17},{9,25},{17,1},{25,9},{2,18},{10... | collective-permute-start | bytes 786440 | tf_op jit(solution)/shard_map/ppermute | solution.py:89
  62.3 30.9 %collective-permute-start.4 = (bf16[16,64,128]{2,1,0:T(8,128)(2,1)S(1)}, bf16[16,64,128]{2,1,0:T(8,128)(2,1)S(1)}, u32[]{:S(2)}, u32[]{:S(2)}) collective-permute-start(bf16[16,64,128]{2,1,0:T(8,128)(2,1)S(1)} %slice.14.w0_ref), channel_id=1, source_target_pairs={{0,8},{8,16},{16,24},{24,0},{1,9},{9,17},{17,25},{25,1},{2,10},{10... | collective-permute-start | bytes 786440 | tf_op jit(solution)/shard_map/ppermute | solution.py:89
  93.2 31.8 %copy-start.3 = (bf16[1,128,128]{2,1,0:T(8,128)(2,1)S(1)}, bf16[1,128,128]{2,1,0:T(8,128)(2,1)}, u32[]{:S(2)}) copy-start(bf16[1,128,128]{2,1,0:T(8,128)(2,1)} %param.29) | copy-start | bytes 98308
  93.2 31.8 %copy-start.5 = (f32[128]{0:T(128)S(1)}, f32[128]{0:T(128)}, u32[]{:S(2)}) copy-start(f32[128]{0:T(128)} %param.30) | copy-start | bytes 1540
  93.2 31.8 %copy-start.6 = (f32[128]{0:T(128)S(1)}, f32[128]{0:T(128)}, u32[]{:S(2)}) copy-start(f32[128]{0:T(128)} %param.31) | copy-start | bytes 1540
  98.3 5.0 %collective-permute-start.7 = (bf16[128,256]{1,0:T(8,128)(2,1)S(1)}, bf16[128,256]{1,0:T(8,128)(2,1)S(1)}, u32[]{:S(2)}, u32[]{:S(2)}) collective-permute-start(bf16[128,256]{1,0:T(8,128)(2,1)S(1)} %get-tuple-element.30.own_ref), channel_id=1, source_target_pairs={{0,32},{32,0},{64,96},{96,64},{128,160},{160,128},{192,224},{224,1... | collective-permute-start | bytes 196616 | tf_op jit(solution)/shard_map/ppermute | solution.py:396
  103.5 6.3 %collective-permute-start.8 = (bf16[128,256]{1,0:T(8,128)(2,1)S(1)}, bf16[128,256]{1,0:T(8,128)(2,1)S(1)}, u32[]{:S(2)}, u32[]{:S(2)}) collective-permute-start(bf16[128,256]{1,0:T(8,128)(2,1)S(1)} %get-tuple-element.31.own_ref), channel_id=1, source_target_pairs={{0,64},{32,96},{64,0},{96,32},{128,192},{160,224},{192,128},{224,1... | collective-permute-start | bytes 196616 | tf_op jit(solution)/shard_map/ppermute | solution.py:396
  110.1 14.9 %collective-permute-start.9 = (bf16[128,256]{1,0:T(8,128)(2,1)S(1)}, bf16[128,256]{1,0:T(8,128)(2,1)S(1)}, u32[]{:S(2)}, u32[]{:S(2)}) collective-permute-start(bf16[128,256]{1,0:T(8,128)(2,1)S(1)} %get-tuple-element.33), channel_id=1, source_target_pairs={{0,128},{32,160},{64,192},{96,224},{128,256},{160,288},{192,320},{... | collective-permute-start | bytes 196616 | tf_op jit(solution)/shard_map/ppermute | solution.py:417
  112.9 11.1 %collective-permute-start.10 = (bf16[128,128]{1,0:T(8,128)(2,1)S(1)}, bf16[128,128]{1,0:T(8,128)(2,1)S(1)}, u32[]{:S(2)}, u32[]{:S(2)}) collective-permute-start(bf16[128,128]{1,0:T(8,128)(2,1)S(1)} %get-tuple-element.34), channel_id=1, source_target_pairs={{128,384},{160,416},{192,448},{224,480},{129,385},{161,417},{193,4... | collective-permute-start | bytes 98312 | tf_op jit(solution)/shard_map/ppermute | solution.py:417
  113.6 10.4 %collective-permute-start.12 = (bf16[128,128]{1,0:T(8,128)(2,1)S(1)}, bf16[128,128]{1,0:T(8,128)(2,1)S(1)}, u32[]{:S(2)}, u32[]{:S(2)}) collective-permute-start(bf16[128,128]{1,0:T(8,128)(2,1)S(1)} %get-tuple-element.35), channel_id=1, source_target_pairs={{0,384},{32,416},{64,448},{96,480},{1,385},{33,417},{65,449},{97,4... | collective-permute-start | bytes 98312 | tf_op jit(solution)/shard_map/ppermute | solution.py:417
  118.3 6.8 %collective-permute-start.11 = (bf16[128,128]{1,0:T(8,128)(2,1)S(1)}, bf16[128,128]{1,0:T(8,128)(2,1)S(1)}, u32[]{:S(2)}, u32[]{:S(2)}) collective-permute-start(bf16[128,128]{1,0:T(8,128)(2,1)S(1)} %get-tuple-element.35), channel_id=1, source_target_pairs={{0,256},{32,288},{64,320},{96,352},{128,384},{160,416},{192,448},{... | collective-permute-start | bytes 98312 | tf_op jit(solution)/shard_map/ppermute | solution.py:417
  127.7 9.1 %collective-permute-start.13 = (bf16[4,32,2048]{2,1,0:T(8,128)(2,1)S(1)}, bf16[4,32,2048]{2,1,0:T(8,128)(2,1)S(1)}, u32[]{:S(2)}, u32[]{:S(2)}) collective-permute-start(bf16[4,32,2048]{2,1,0:T(8,128)(2,1)S(1)} %get-tuple-element.38), channel_id=1, source_target_pairs={{0,1},{1,0},{2,3},{3,2},{4,5},{5,4},{6,7},{7,6},{8,9},{9,8},{10,11... | collective-permute-start | bytes 1572872 | tf_op jit(solution)/shard_map/ppermute | solution.py:439

commit v6 on v5

--- a/solution.py
+++ b/solution.py
@@ -40,6 +40,10 @@
 def split(a):
     high = a.astype(BF16)
     return high, (a - high.astype(F32)).astype(BF16)
+
+
+def dot1(a, b, dims=((1,), (0,))):
+    return dot(a.astype(BF16), b.astype(BF16), dims)
 
 
 def dot3(a, b, dims=((1,), (0,))):
@@ -158,11 +162,15 @@
     inv = [jnp.where(apart == 0, 1.0, jnp.where(apart == 1, -x, 0.0)) for x in low]
     b = 2
     while b < size:
-        here = (apart >= b) & (apart < 2 * b)
+        here = (apart >= b) & (apart < 4 * b)
         parts = [split(x) for x in inv]
-        mid = [product(x, split(jnp.where(here, y, 0.0))) for x, y in zip(parts, low)]
-        inv = [x - product(split(y), p) for x, y, p in zip(inv, mid, parts)]
-        b *= 2
+        powers = [
+            split(product(x, split(jnp.where(here, y, 0.0)))) for x, y in zip(parts, low)
+        ]
+        squares = [split(product(n, n)) for n in powers]
+        inv = [x - product(n, p) for x, n, p in zip(inv, powers, parts)]
+        inv = [x + product(q, split(x)) for x, q in zip(inv, squares)]
+        b *= 4
     return inv
 
 
@@ -188,13 +196,13 @@
         [corr[:half, :half], corr[half:, half:]], half
     )
     rhs = jnp.concatenate([values * beta, kb * jnp.exp(gc)], axis=1)
-    top = dot3(first, rhs[:half])
-    bottom = dot3(second, rhs[half:] - dot3(corr[half:, :half], top))
+    top = dot1(first, rhs[:half])
+    bottom = dot1(second, rhs[half:] - dot1(corr[half:, :half], top))
     uw_ref[0:half] = top
     uw_ref[half:] = bottom
     last = gc[length - 1 : length, :]
     kd = keys * jnp.exp(last - gc)
-    made = dot3(kd, uw_ref[...], ((0,), (0,)))
+    made = dot1(kd, uw_ref[...], ((0,), (0,)))
     ri = lax.broadcasted_iota(jnp.int32, (width, width), 0)
     ci = lax.broadcasted_iota(jnp.int32, (width, width), 1)
     linear = jnp.where(ri == ci, jnp.exp(last), 0.0) - made[:, width:]
@@ -271,10 +279,10 @@
     raw = dot(xn_ref[...], w_scr[...])
     query = unit_rows(short_conv(raw[:, :width], taps_ref[0], length, q_scr)) * width ** (-0.5)
     silu_gate = jax.nn.silu(raw[HALO:, width : 2 * width].astype(BF16).astype(F32))
-    scores = dot3(query, k_ref[...], ((1,), (1,))) * decay_ref[...]
-    both = dot3(scores, uw_ref[...])
+    scores = dot1(query, k_ref[...], ((1,), (1,))) * decay_ref[...]
+    both = dot1(scores, uw_ref[...])
     effect = query * jnp.exp(gc_ref[...]) - both[:, width:]
-    attended = both[:, :width] + dot3(effect, state)
+    attended = both[:, :width] + dot1(effect, state)
     scale = lax.rsqrt(jnp.mean(attended * attended, axis=-1, keepdims=True) + EPS)
     delta = (attended * scale * gain_ref[...] * silu_gate).astype(BF16)
     x = raw[:, 2 * width :].astype(BF16).astype(F32)

time: 150 us -> 149 us (level)
  no operation moved by 1% of the time
where the time goes in v6:
time: 149 us
  starting transfers between devices  57 us (38%)
  blocking collectives  42.2 us (28%)
  waiting for transfers between devices  37.1 us (25%)
  Pallas kernels  11.6 us (8%)
    all_gather x1, blocking collectives, layer(): quarters = lax.all_gather(part, 'sp', axis=0)  30.2 us
    ppermute x6, waiting for transfers between devices, turns(): lax.ppermute(x, axis, [(i, i - i % size + (i + d) % size) for i in range(...  27.1 us
    ppermute x6, starting transfers between devices, turns(): lax.ppermute(x, axis, [(i, i - i % size + (i + d) % size) for i in range(...  19.4 us
    ppermute x4, starting transfers between devices, from_behind(): lax.ppermute(x, 'sp', [(i, i + distance) for i in range(first, last)])  13.9 us
    all_to_all x1, blocking collectives, exchange(): lax.all_to_all(copies, axis, split_axis=0, concat_axis=0, tiled=True, axi...  12 us
    pallas_call x8, Pallas kernels, call(): pl.pallas_call(kernel, out_shape=list(outs) if many else outs, in_specs=i...  11.6 us
    all_to_all x1, starting transfers between devices, exchange(): lax.all_to_all(copies, axis, split_axis=0, concat_axis=0, tiled=True, axi...  10.4 us
    ppermute x1, starting transfers between devices, layer(): theirs = lax.ppermute(other, 'tp', [(i, i ^ 1) for i in range(n_tp)])  7.54 us
  transfers between devices with their start and end apart: 15, of which 6 were waited for; matrix products, arithmetic and copies ran while one was open for 0% of the time, Pallas kernels for 4%

profile of v6, /device:TPU:1, one launch (start us, length us, event | category | flops | bytes accessed | tf_op | source)
XLA Modules:
  0.0 148.8 jit_solution(3362510093367060940)
XLA Ops:
  0.0 2.2 %shard_map.163 = (bf16[8,32,2048]{2,1,0:T(8,128)(2,1)}, bf16[224,128]{1,0:T(8,128)(2,1)}) custom-call(s32[1]{0:T(128)} %bitcast.sp_ref, s32[1]{0:T(128)} %bitcast.1.tp_ref, s32[1]{0:T(128)} %bitcast.2.fs_ref, bf16[32,2048]{1,0:T(8,128)(2,1)} %tok_ref.1, bf16[2048]{0:T(1024)(128)(2,1)} %gain_ref.1, bf16[128,128]{1,0:T(8,128)(2,1)} %k_ref.1, ...), custom_call_target="tpu_custom_call" | custom-call | tf_op jit(solution)/shard_map/pallas_call | solution.py:21
  2.2 10.4 %all-to-all-start = ((bf16[8,32,2048]{2,1,0:T(8,128)(2,1)}), bf16[8,32,2048]{2,1,0:T(8,128)(2,1)S(1)}, u32[]{:S(2)}, u32[]{:S(2)}) async-start(bf16[8,32,2048]{2,1,0:T(8,128)(2,1)} %get-tuple-element.22), calls=%async_computation | async-start | bytes 2097152 | tf_op jit(solution)/shard_map/all_to_all | solution.py:84
  12.6 30.2 %all-gather = bf16[3584,128]{1,0:T(8,128)(2,1)S(1)} all-gather(bf16[224,128]{1,0:T(8,128)(2,1)S(1)} %copy-done.7), channel_id=2, replica_groups=mesh['sp'=16,'fs'=4,'tp'=8] {'sp'}, dimensions={0}, use_global_device_ids=true | all-gather | bytes 974848 | tf_op jit(solution)/shard_map/all_gather | solution.py:375
  42.8 4.8 %collective-permute-start.6 = (bf16[16,64,128]{2,1,0:T(8,128)(2,1)S(1)}, bf16[16,64,128]{2,1,0:T(8,128)(2,1)}, u32[]{:S(2)}, u32[]{:S(2)}) collective-permute-start(bf16[16,64,128]{2,1,0:T(8,128)(2,1)S(1)} %slice.14.w0_ref), channel_id=1, source_target_pairs={{0,24},{8,0},{16,8},{24,16},{1,25},{9,1},{17,9},{25,17},{2,26},{10... | collective-permute-start | bytes 786440 | tf_op jit(solution)/shard_map/ppermute | solution.py:93
  47.7 2.4 %collective-permute-start.3 = (bf16[16,160,128]{2,1,0:T(8,128)(2,1)S(1)}, bf16[16,160,128]{2,1,0:T(8,128)(2,1)S(1)}, u32[]{:S(2)}, u32[]{:S(2)}) collective-permute-start(bf16[16,160,128]{2,1,0:T(8,128)(2,1)S(1)} %slice.13.w0_ref), channel_id=1, source_target_pairs={{0,24},{8,0},{16,8},{24,16},{1,25},{9,1},{17,9},{25,17},{2,26},{10... | collective-permute-start | bytes 1966088 | tf_op jit(solution)/shard_map/ppermute | solution.py:93
  50.1 1.9 %collective-permute-start.2 = (bf16[16,160,128]{2,1,0:T(8,128)(2,1)S(1)}, bf16[16,160,128]{2,1,0:T(8,128)(2,1)S(1)}, u32[]{:S(2)}, u32[]{:S(2)}) collective-permute-start(bf16[16,160,128]{2,1,0:T(8,128)(2,1)S(1)} %slice.13.w0_ref), channel_id=1, source_target_pairs={{0,16},{8,24},{16,0},{24,8},{1,17},{9,25},{17,1},{25,9},{2,18},{10... | collective-permute-start | bytes 1966088 | tf_op jit(solution)/shard_map/ppermute | solution.py:93
  52.0 1.8 %collective-permute-start = (bf16[16,2048]{1,0:T(8,128)(2,1)S(1)}, bf16[16,2048]{1,0:T(8,128)(2,1)S(1)}, u32[]{:S(2)}, u32[]{:S(2)}) collective-permute-start(bf16[16,2048]{1,0:T(8,128)(2,1)S(1)} %slice.12), channel_id=1, source_target_pairs={{0,32},{32,64},{64,96},{96,128},{128,160},{160,192},{192,224},{224... | collective-permute-start | bytes 196616 | tf_op jit(solution)/shard_map/ppermute | solution.py:372
  53.9 2.9 %collective-permute-start.1 = (bf16[16,160,128]{2,1,0:T(8,128)(2,1)S(1)}, bf16[16,160,128]{2,1,0:T(8,128)(2,1)S(1)}, u32[]{:S(2)}, u32[]{:S(2)}) collective-permute-start(bf16[16,160,128]{2,1,0:T(8,128)(2,1)S(1)} %slice.13.w0_ref), channel_id=1, source_target_pairs={{0,8},{8,16},{16,24},{24,0},{1,9},{9,17},{17,25},{25,1},{2,10},{10... | collective-permute-start | bytes 1966088 | tf_op jit(solution)/shard_map/ppermute | solution.py:93
  56.8 5.5 %collective-permute-start.5 = (bf16[16,64,128]{2,1,0:T(8,128)(2,1)S(1)}, bf16[16,64,128]{2,1,0:T(8,128)(2,1)S(1)}, u32[]{:S(2)}, u32[]{:S(2)}) collective-permute-start(bf16[16,64,128]{2,1,0:T(8,128)(2,1)S(1)} %slice.14.w0_ref), channel_id=1, source_target_pairs={{0,16},{8,24},{16,0},{24,8},{1,17},{9,25},{17,1},{25,9},{2,18},{10... | collective-permute-start | bytes 786440 | tf_op jit(solution)/shard_map/ppermute | solution.py:93
  62.3 1.9 %collective-permute-start.4 = (bf16[16,64,128]{2,1,0:T(8,128)(2,1)S(1)}, bf16[16,64,128]{2,1,0:T(8,128)(2,1)S(1)}, u32[]{:S(2)}, u32[]{:S(2)}) collective-permute-start(bf16[16,64,128]{2,1,0:T(8,128)(2,1)S(1)} %slice.14.w0_ref), channel_id=1, source_target_pairs={{0,8},{8,16},{16,24},{24,0},{1,9},{9,17},{17,25},{25,1},{2,10},{10... | collective-permute-start | bytes 786440 | tf_op jit(solution)/shard_map/ppermute | solution.py:93
  66.1 16.2 %collective-permute-done.5.w2_ref = bf16[16,64,128]{2,1,0:T(8,128)(2,1)S(1)} collective-permute-done((bf16[16,64,128]{2,1,0:T(8,128)(2,1)S(1)}, bf16[16,64,128]{2,1,0:T(8,128)(2,1)S(1)}, u32[]{:S(2)}, u32[]{:S(2)}) %collective-permute-start.5) | collective-permute-done | bytes 262176 | tf_op jit(solution)/shard_map/ppermute | solution.py:93
  82.4 10.8 %collective-permute-done.4.w1_ref = bf16[16,64,128]{2,1,0:T(8,128)(2,1)S(1)} collective-permute-done((bf16[16,64,128]{2,1,0:T(8,128)(2,1)S(1)}, bf16[16,64,128]{2,1,0:T(8,128)(2,1)S(1)}, u32[]{:S(2)}, u32[]{:S(2)}) %collective-permute-start.4) | collective-permute-done | bytes 262176 | tf_op jit(solution)/shard_map/ppermute | solution.py:93
  93.2 4.7 %shard_map.165 = (bf16[128,256]{1,0:T(8,128)(2,1)S(1)}, f32[256,128]{1,0:T(8,128)S(1)}, f32[256,256]{1,0:T(8,128)S(1)}) custom-call(s32[1]{0:T(128)} %bitcast.sp_ref, s32[1]{0:T(128)} %bitcast.1.tp_ref, s32[1]{0:T(128)} %bitcast.2.fs_ref, bf16[272,2048]{1,0:T(8,128)(2,1)S(1)} %get-tuple-element.23.xn_ref, bf16[16,64,128]{2,1,0:T(8,128)(2,1)S(1)} %slice.14.w0_ref, ...), custom_call_target="tpu_custom_call" | custom-call | flops 1342177280 | tf_op jit(solution)/shard_map/pallas_call | solution.py:21
  97.9 1.9 %collective-permute-start.7 = (bf16[128,256]{1,0:T(8,128)(2,1)S(1)}, bf16[128,256]{1,0:T(8,128)(2,1)S(1)}, u32[]{:S(2)}, u32[]{:S(2)}) collective-permute-start(bf16[128,256]{1,0:T(8,128)(2,1)S(1)} %get-tuple-element.30.own_ref), channel_id=1, source_target_pairs={{0,32},{32,0},{64,96},{96,64},{128,160},{160,128},{192,224},{224,1... | collective-permute-start | bytes 196616 | tf_op jit(solution)/shard_map/ppermute | solution.py:404
  99.8 3.1 %collective-permute-done.7.other_ref = bf16[128,256]{1,0:T(8,128)(2,1)S(1)} collective-permute-done((bf16[128,256]{1,0:T(8,128)(2,1)S(1)}, bf16[128,256]{1,0:T(8,128)(2,1)S(1)}, u32[]{:S(2)}, u32[]{:S(2)}) %collective-permute-start.7) | collective-permute-done | bytes 65568 | tf_op jit(solution)/shard_map/ppermute | solution.py:404
  103.1 1.9 %collective-permute-start.8 = (bf16[128,256]{1,0:T(8,128)(2,1)S(1)}, bf16[128,256]{1,0:T(8,128)(2,1)S(1)}, u32[]{:S(2)}, u32[]{:S(2)}) collective-permute-start(bf16[128,256]{1,0:T(8,128)(2,1)S(1)} %get-tuple-element.31.own_ref), channel_id=1, source_target_pairs={{0,64},{32,96},{64,0},{96,32},{128,192},{160,224},{192,128},{224,1... | collective-permute-start | bytes 196616 | tf_op jit(solution)/shard_map/ppermute | solution.py:404
  105.1 4.4 %collective-permute-done.8.other_ref = bf16[128,256]{1,0:T(8,128)(2,1)S(1)} collective-permute-done((bf16[128,256]{1,0:T(8,128)(2,1)S(1)}, bf16[128,256]{1,0:T(8,128)(2,1)S(1)}, u32[]{:S(2)}, u32[]{:S(2)}) %collective-permute-start.8) | collective-permute-done | bytes 65568 | tf_op jit(solution)/shard_map/ppermute | solution.py:404
  109.7 2.8 %collective-permute-start.9 = (bf16[128,256]{1,0:T(8,128)(2,1)S(1)}, bf16[128,256]{1,0:T(8,128)(2,1)S(1)}, u32[]{:S(2)}, u32[]{:S(2)}) collective-permute-start(bf16[128,256]{1,0:T(8,128)(2,1)S(1)} %get-tuple-element.33), channel_id=1, source_target_pairs={{0,128},{32,160},{64,192},{96,224},{128,256},{160,288},{192,320},{... | collective-permute-start | bytes 196616 | tf_op jit(solution)/shard_map/ppermute | solution.py:425
  113.2 4.7 %collective-permute-start.12 = (bf16[128,128]{1,0:T(8,128)(2,1)S(1)}, bf16[128,128]{1,0:T(8,128)(2,1)S(1)}, u32[]{:S(2)}, u32[]{:S(2)}) collective-permute-start(bf16[128,128]{1,0:T(8,128)(2,1)S(1)} %get-tuple-element.35), channel_id=1, source_target_pairs={{0,384},{32,416},{64,448},{96,480},{1,385},{33,417},{65,449},{97,4... | collective-permute-start | bytes 98312 | tf_op jit(solution)/shard_map/ppermute | solution.py:425
  117.9 5.7 %collective-permute-start.11 = (bf16[128,128]{1,0:T(8,128)(2,1)S(1)}, bf16[128,128]{1,0:T(8,128)(2,1)S(1)}, u32[]{:S(2)}, u32[]{:S(2)}) collective-permute-start(bf16[128,128]{1,0:T(8,128)(2,1)S(1)} %get-tuple-element.35), channel_id=1, source_target_pairs={{0,256},{32,288},{64,320},{96,352},{128,384},{160,416},{192,448},{... | collective-permute-start | bytes 98312 | tf_op jit(solution)/shard_map/ppermute | solution.py:425
  124.6 2.3 %shard_map.168 = (bf16[4,32,2048]{2,1,0:T(8,128)(2,1)S(1)}, bf16[4,32,2048]{2,1,0:T(8,128)(2,1)S(1)}) custom-call(s32[1]{0:T(128)} %bitcast.sp_ref, s32[1]{0:T(128)} %bitcast.1.tp_ref, s32[1]{0:T(128)} %bitcast.2.fs_ref, bf16[272,2048]{1,0:T(8,128)(2,1)S(1)} %get-tuple-element.23.xn_ref, bf16[16,160,128]{2,1,0:T(8,128)(2,1)S(1)} %slice.13.w0_ref, ...), custom_call_target="tpu_custom_call" | custom-call | flops 1342177280 | tf_op jit(solution)/shard_map/pallas_call | solution.py:21
  126.9 7.5 %collective-permute-start.13 = (bf16[4,32,2048]{2,1,0:T(8,128)(2,1)S(1)}, bf16[4,32,2048]{2,1,0:T(8,128)(2,1)S(1)}, u32[]{:S(2)}, u32[]{:S(2)}) collective-permute-start(bf16[4,32,2048]{2,1,0:T(8,128)(2,1)S(1)} %get-tuple-element.38), channel_id=1, source_target_pairs={{0,1},{1,0},{2,3},{3,2},{4,5},{5,4},{6,7},{7,6},{8,9},{9,8},{10,11... | collective-permute-start | bytes 1572872 | tf_op jit(solution)/shard_map/ppermute | solution.py:447
  134.5 1.5 %collective-permute-done.13.theirs_ref = bf16[4,32,2048]{2,1,0:T(8,128)(2,1)S(1)} collective-permute-done((bf16[4,32,2048]{2,1,0:T(8,128)(2,1)S(1)}, bf16[4,32,2048]{2,1,0:T(8,128)(2,1)S(1)}, u32[]{:S(2)}, u32[]{:S(2)}) %collective-permute-start.13) | collective-permute-done | bytes 524320 | tf_op jit(solution)/shard_map/ppermute | solution.py:447
  136.1 12.0 %all_to_all.10.in_ref = bf16[4,32,2048]{2,1,0:T(8,128)(2,1)S(1)} all-to-all(bf16[4,32,2048]{2,1,0:T(8,128)(2,1)S(1)} %shard_map.169), channel_id=1, replica_groups={{0,2,4,6},{1,3,5,7},{8,10,12,14},{9,11,13,15},{16,18,20,22},{17,19,21,2..., dimensions={0} | all-to-all | bytes 1048576 | tf_op jit(solution)/shard_map/all_to_all | solution.py:84
  (35 shorter events, 4.3 us)
Async XLA Ops:
  2.2 10.4 %copy-start.7 = (bf16[224,128]{1,0:T(8,128)(2,1)S(1)}, bf16[224,128]{1,0:T(8,128)(2,1)}, u32[]{:S(2)}) copy-start(bf16[224,128]{1,0:T(8,128)(2,1)} %get-tuple-element.24) | copy-start | bytes 172036
  2.2 49.8 %all-to-all-start = ((bf16[8,32,2048]{2,1,0:T(8,128)(2,1)}), bf16[8,32,2048]{2,1,0:T(8,128)(2,1)S(1)}, u32[]{:S(2)}, u32[]{:S(2)}) async-start(bf16[8,32,2048]{2,1,0:T(8,128)(2,1)} %get-tuple-element.22), calls=%async_computation | async-start | bytes 2097152 | tf_op jit(solution)/shard_map/all_to_all | solution.py:84
  42.8 22.1 %copy-start = (bf16[2048,8]{0,1:T(8,128)(2,1)S(1)}, bf16[2048,8]{0,1:T(8,128)(2,1)}, u32[]{:S(2)}) copy-start(bf16[2048,8]{0,1:T(8,128)(2,1)} %param.24) | copy-start | bytes 98308
  42.8 22.1 %copy-start.1 = (bf16[2048,8]{0,1:T(8,128)(2,1)S(1)}, bf16[2048,8]{0,1:T(8,128)(2,1)}, u32[]{:S(2)}) copy-start(bf16[2048,8]{0,1:T(8,128)(2,1)} %param.25) | copy-start | bytes 98308
  42.8 22.1 %copy-start.2 = (f32[256,1]{0,1:T(1,128)S(1)}, f32[256,1]{0,1:T(1,128)}, u32[]{:S(2)}) copy-start(f32[256,1]{0,1:T(1,128)} %param.28) | copy-start | bytes 3076
  42.8 50.4 %copy-start.4 = (f32[3,4,128]{2,1,0:T(4,128)S(1)}, f32[3,4,128]{2,1,0:T(4,128)}, u32[]{:S(2)}) copy-start(f32[3,4,128]{2,1,0:T(4,128)} %taps_ref.3) | copy-start | bytes 18436
  42.8 14.0 %collective-permute-start.6 = (bf16[16,64,128]{2,1,0:T(8,128)(2,1)S(1)}, bf16[16,64,128]{2,1,0:T(8,128)(2,1)}, u32[]{:S(2)}, u32[]{:S(2)}) collective-permute-start(bf16[16,64,128]{2,1,0:T(8,128)(2,1)S(1)} %slice.14.w0_ref), channel_id=1, source_target_pairs={{0,24},{8,0},{16,8},{24,16},{1,25},{9,1},{17,9},{25,17},{2,26},{10... | collective-permute-start | bytes 786440 | tf_op jit(solution)/shard_map/ppermute | solution.py:93
  47.7 65.5 %collective-permute-start.3 = (bf16[16,160,128]{2,1,0:T(8,128)(2,1)S(1)}, bf16[16,160,128]{2,1,0:T(8,128)(2,1)S(1)}, u32[]{:S(2)}, u32[]{:S(2)}) collective-permute-start(bf16[16,160,128]{2,1,0:T(8,128)(2,1)S(1)} %slice.13.w0_ref), channel_id=1, source_target_pairs={{0,24},{8,0},{16,8},{24,16},{1,25},{9,1},{17,9},{25,17},{2,26},{10... | collective-permute-start | bytes 1966088 | tf_op jit(solution)/shard_map/ppermute | solution.py:93
  50.1 67.8 %collective-permute-start.2 = (bf16[16,160,128]{2,1,0:T(8,128)(2,1)S(1)}, bf16[16,160,128]{2,1,0:T(8,128)(2,1)S(1)}, u32[]{:S(2)}, u32[]{:S(2)}) collective-permute-start(bf16[16,160,128]{2,1,0:T(8,128)(2,1)S(1)} %slice.13.w0_ref), channel_id=1, source_target_pairs={{0,16},{8,24},{16,0},{24,8},{1,17},{9,25},{17,1},{25,9},{2,18},{10... | collective-permute-start | bytes 1966088 | tf_op jit(solution)/shard_map/ppermute | solution.py:93
  52.0 10.3 %collective-permute-start = (bf16[16,2048]{1,0:T(8,128)(2,1)S(1)}, bf16[16,2048]{1,0:T(8,128)(2,1)S(1)}, u32[]{:S(2)}, u32[]{:S(2)}) collective-permute-start(bf16[16,2048]{1,0:T(8,128)(2,1)S(1)} %slice.12), channel_id=1, source_target_pairs={{0,32},{32,64},{64,96},{96,128},{128,160},{160,192},{192,224},{224... | collective-permute-start | bytes 196616 | tf_op jit(solution)/shard_map/ppermute | solution.py:372
  53.9 69.8 %collective-permute-start.1 = (bf16[16,160,128]{2,1,0:T(8,128)(2,1)S(1)}, bf16[16,160,128]{2,1,0:T(8,128)(2,1)S(1)}, u32[]{:S(2)}, u32[]{:S(2)}) collective-permute-start(bf16[16,160,128]{2,1,0:T(8,128)(2,1)S(1)} %slice.13.w0_ref), channel_id=1, source_target_pairs={{0,8},{8,16},{16,24},{24,0},{1,9},{9,17},{17,25},{25,1},{2,10},{10... | collective-permute-start | bytes 1966088 | tf_op jit(solution)/shard_map/ppermute | solution.py:93
  56.8 25.6 %collective-permute-start.5 = (bf16[16,64,128]{2,1,0:T(8,128)(2,1)S(1)}, bf16[16,64,128]{2,1,0:T(8,128)(2,1)S(1)}, u32[]{:S(2)}, u32[]{:S(2)}) collective-permute-start(bf16[16,64,128]{2,1,0:T(8,128)(2,1)S(1)} %slice.14.w0_ref), channel_id=1, source_target_pairs={{0,16},{8,24},{16,0},{24,8},{1,17},{9,25},{17,1},{25,9},{2,18},{10... | collective-permute-start | bytes 786440 | tf_op jit(solution)/shard_map/ppermute | solution.py:93
  62.3 30.9 %collective-permute-start.4 = (bf16[16,64,128]{2,1,0:T(8,128)(2,1)S(1)}, bf16[16,64,128]{2,1,0:T(8,128)(2,1)S(1)}, u32[]{:S(2)}, u32[]{:S(2)}) collective-permute-start(bf16[16,64,128]{2,1,0:T(8,128)(2,1)S(1)} %slice.14.w0_ref), channel_id=1, source_target_pairs={{0,8},{8,16},{16,24},{24,0},{1,9},{9,17},{17,25},{25,1},{2,10},{10... | collective-permute-start | bytes 786440 | tf_op jit(solution)/shard_map/ppermute | solution.py:93
  93.2 31.4 %copy-start.3 = (bf16[1,128,128]{2,1,0:T(8,128)(2,1)S(1)}, bf16[1,128,128]{2,1,0:T(8,128)(2,1)}, u32[]{:S(2)}) copy-start(bf16[1,128,128]{2,1,0:T(8,128)(2,1)} %param.29) | copy-start | bytes 98308
  93.2 31.4 %copy-start.5 = (f32[128]{0:T(128)S(1)}, f32[128]{0:T(128)}, u32[]{:S(2)}) copy-start(f32[128]{0:T(128)} %param.30) | copy-start | bytes 1540
  93.2 31.4 %copy-start.6 = (f32[128]{0:T(128)S(1)}, f32[128]{0:T(128)}, u32[]{:S(2)}) copy-start(f32[128]{0:T(128)} %param.31) | copy-start | bytes 1540
  97.9 5.0 %collective-permute-start.7 = (bf16[128,256]{1,0:T(8,128)(2,1)S(1)}, bf16[128,256]{1,0:T(8,128)(2,1)S(1)}, u32[]{:S(2)}, u32[]{:S(2)}) collective-permute-start(bf16[128,256]{1,0:T(8,128)(2,1)S(1)} %get-tuple-element.30.own_ref), channel_id=1, source_target_pairs={{0,32},{32,0},{64,96},{96,64},{128,160},{160,128},{192,224},{224,1... | collective-permute-start | bytes 196616 | tf_op jit(solution)/shard_map/ppermute | solution.py:404
  103.1 6.3 %collective-permute-start.8 = (bf16[128,256]{1,0:T(8,128)(2,1)S(1)}, bf16[128,256]{1,0:T(8,128)(2,1)S(1)}, u32[]{:S(2)}, u32[]{:S(2)}) collective-permute-start(bf16[128,256]{1,0:T(8,128)(2,1)S(1)} %get-tuple-element.31.own_ref), channel_id=1, source_target_pairs={{0,64},{32,96},{64,0},{96,32},{128,192},{160,224},{192,128},{224,1... | collective-permute-start | bytes 196616 | tf_op jit(solution)/shard_map/ppermute | solution.py:404
  109.7 14.9 %collective-permute-start.9 = (bf16[128,256]{1,0:T(8,128)(2,1)S(1)}, bf16[128,256]{1,0:T(8,128)(2,1)S(1)}, u32[]{:S(2)}, u32[]{:S(2)}) collective-permute-start(bf16[128,256]{1,0:T(8,128)(2,1)S(1)} %get-tuple-element.33), channel_id=1, source_target_pairs={{0,128},{32,160},{64,192},{96,224},{128,256},{160,288},{192,320},{... | collective-permute-start | bytes 196616 | tf_op jit(solution)/shard_map/ppermute | solution.py:425
  112.5 11.1 %collective-permute-start.10 = (bf16[128,128]{1,0:T(8,128)(2,1)S(1)}, bf16[128,128]{1,0:T(8,128)(2,1)S(1)}, u32[]{:S(2)}, u32[]{:S(2)}) collective-permute-start(bf16[128,128]{1,0:T(8,128)(2,1)S(1)} %get-tuple-element.34), channel_id=1, source_target_pairs={{128,384},{160,416},{192,448},{224,480},{129,385},{161,417},{193,4... | collective-permute-start | bytes 98312 | tf_op jit(solution)/shard_map/ppermute | solution.py:425
  113.2 10.4 %collective-permute-start.12 = (bf16[128,128]{1,0:T(8,128)(2,1)S(1)}, bf16[128,128]{1,0:T(8,128)(2,1)S(1)}, u32[]{:S(2)}, u32[]{:S(2)}) collective-permute-start(bf16[128,128]{1,0:T(8,128)(2,1)S(1)} %get-tuple-element.35), channel_id=1, source_target_pairs={{0,384},{32,416},{64,448},{96,480},{1,385},{33,417},{65,449},{97,4... | collective-permute-start | bytes 98312 | tf_op jit(solution)/shard_map/ppermute | solution.py:425
  117.9 6.8 %collective-permute-start.11 = (bf16[128,128]{1,0:T(8,128)(2,1)S(1)}, bf16[128,128]{1,0:T(8,128)(2,1)S(1)}, u32[]{:S(2)}, u32[]{:S(2)}) collective-permute-start(bf16[128,128]{1,0:T(8,128)(2,1)S(1)} %get-tuple-element.35), channel_id=1, source_target_pairs={{0,256},{32,288},{64,320},{96,352},{128,384},{160,416},{192,448},{... | collective-permute-start | bytes 98312 | tf_op jit(solution)/shard_map/ppermute | solution.py:425
  126.9 9.1 %collective-permute-start.13 = (bf16[4,32,2048]{2,1,0:T(8,128)(2,1)S(1)}, bf16[4,32,2048]{2,1,0:T(8,128)(2,1)S(1)}, u32[]{:S(2)}, u32[]{:S(2)}) collective-permute-start(bf16[4,32,2048]{2,1,0:T(8,128)(2,1)S(1)} %get-tuple-element.38), channel_id=1, source_target_pairs={{0,1},{1,0},{2,3},{3,2},{4,5},{5,4},{6,7},{7,6},{8,9},{9,8},{10,11... | collective-permute-start | bytes 1572872 | tf_op jit(solution)/shard_map/ppermute | solution.py:447

commit v7 on v6

--- a/solution.py
+++ b/solution.py
@@ -95,13 +95,10 @@
 
 
 def gate_kernel(
-    sp_ref, tp_ref, fs_ref, a_log_ref, rows_ref, tail_ref, wb_ref, wd_ref, extra_ref,
-    xn_ref, beta_ref, gc_ref, decay_ref,
+    sp_ref, tp_ref, fs_ref, a_log_ref, rows_ref, wb_ref, wd_ref, extra_ref,
+    beta_ref, gc_ref, decay_ref,
 ):
     length = rows_ref.shape[0]
-    tail = tail_ref[...]
-    xn_ref[0:HALO] = jnp.where(sp_ref[0] > 0, tail, jnp.zeros_like(tail))
-    xn_ref[HALO:] = rows_ref[...]
     lane = tp_ref[0]
 
     def own_column(w_ref):
@@ -175,11 +172,15 @@
 
 
 def local_kernel(
-    sp_ref, tp_ref, fs_ref, xn_ref, w0_ref, w1_ref, w2_ref, w3_ref, taps_ref, beta_ref, gc_ref, decay_ref,
-    ab_ref, k_ref, uw_ref,
+    sp_ref, tp_ref, fs_ref, rows_ref, tail_ref, w0_ref, w1_ref, w2_ref, w3_ref, taps_ref,
+    beta_ref, gc_ref, decay_ref,
+    ab_ref, k_ref, uw_ref, xn_ref,
     w_scr, k_scr, v_scr,
 ):
     length, width = k_ref.shape
+    tail = tail_ref[...]
+    xn_ref[0:HALO] = jnp.where(sp_ref[0] > 0, tail, jnp.zeros_like(tail))
+    xn_ref[HALO:] = rows_ref[...]
     gather_two(fs_ref[0], (w0_ref, w1_ref, w2_ref, w3_ref), w_scr)
     raw = dot(xn_ref[...], w_scr[...])
     keys = unit_rows(short_conv(raw[:, :width], taps_ref[1], length, k_scr))
@@ -376,21 +377,25 @@
     kv = turns(quarters[:, :half], "fs", 4)
     rest = turns(quarters[:, half:], "fs", 4)
 
-    xn, beta, gc, decay = call(
+    beta, gc, decay = call(
         gate_kernel,
         (
-            shape(HALO + length, model, dtype=BF16),
             shape(length, 128),
             shape(length, 128),
             shape(length, length),
         ),
-        *ids, a_log, all_rows, tail, w_beta.T, w_decay.T, decay_extra.T,
+        *ids, a_log, all_rows, w_beta.T, w_decay.T, decay_extra.T,
         smem=4, flops=2 * length * model * 128,
     )
-    ab, keys, uw = call(
+    ab, keys, uw, xn = call(
         local_kernel,
-        (shape(width, 2 * width, dtype=BF16), shape(length, width), shape(length, 2 * width)),
-        *ids, xn, *kv, conv_weight, beta, gc, decay,
+        (
+            shape(width, 2 * width, dtype=BF16),
+            shape(length, width),
+            shape(length, 2 * width),
+            shape(HALO + length, model, dtype=BF16),
+        ),
+        *ids, all_rows, tail, *kv, conv_weight, beta, gc, decay,
         scratch=[
             pltpu.VMEM((model, 2 * width), BF16),
             pltpu.VMEM((HALO + length, width), F32),

time: 149 us -> 152 us (1.020); the launches traced: 149 us -> 150 us
  no operation moved by 1% of the time
where the time goes in v7:
time: 152 us; the launch traced here: 150 us
  starting transfers between devices  55.6 us (37%)
  blocking collectives  41.9 us (28%)
  waiting for transfers between devices  37.9 us (25%)
  Pallas kernels  12.7 us (8%)
    all_gather x1, blocking collectives, layer(): quarters = lax.all_gather(part, 'sp', axis=0)  30.2 us
    ppermute x6, waiting for transfers between devices, turns(): lax.ppermute(x, axis, [(i, i - i % size + (i + d) % size) for i in range(...  28 us
    ppermute x6, starting transfers between devices, turns(): lax.ppermute(x, axis, [(i, i - i % size + (i + d) % size) for i in range(...  18.8 us
    ppermute x4, starting transfers between devices, from_behind(): lax.ppermute(x, 'sp', [(i, i + distance) for i in range(first, last)])  13.7 us
    pallas_call x8, Pallas kernels, call(): pl.pallas_call(kernel, out_shape=list(outs) if many else outs, in_specs=i...  12.7 us
    all_to_all x1, blocking collectives, exchange(): lax.all_to_all(copies, axis, split_axis=0, concat_axis=0, tiled=True, axi...  11.7 us
    all_to_all x1, starting transfers between devices, exchange(): lax.all_to_all(copies, axis, split_axis=0, concat_axis=0, tiled=True, axi...  10.4 us
    ppermute x2, waiting for transfers between devices, meet(): return lax.ppermute(x, 'sp', [(i, i ^ distance) for i in range(n_sp)])  7.39 us
  transfers between devices with their start and end apart: 15, of which 6 were waited for; matrix products, arithmetic and copies ran while one was open for 0% of the time, Pallas kernels for 4%

profile of v7, /device:TPU:1, one launch (start us, length us, event | category | flops | bytes accessed | tf_op | source)
XLA Modules:
  0.0 149.9 jit_solution(15345751619964602714)
XLA Ops:
  0.0 2.2 %shard_map.163 = (bf16[8,32,2048]{2,1,0:T(8,128)(2,1)}, bf16[224,128]{1,0:T(8,128)(2,1)}) custom-call(s32[1]{0:T(128)} %bitcast.sp_ref, s32[1]{0:T(128)} %bitcast.1.tp_ref, s32[1]{0:T(128)} %bitcast.2.fs_ref, bf16[32,2048]{1,0:T(8,128)(2,1)} %tok_ref.1, bf16[2048]{0:T(1024)(128)(2,1)} %gain_ref.1, bf16[128,128]{1,0:T(8,128)(2,1)} %k_ref.1, ...), custom_call_target="tpu_custom_call" | custom-call | tf_op jit(solution)/shard_map/pallas_call | solution.py:21
  2.2 10.4 %all-to-all-start = ((bf16[8,32,2048]{2,1,0:T(8,128)(2,1)}), bf16[8,32,2048]{2,1,0:T(8,128)(2,1)S(1)}, u32[]{:S(2)}, u32[]{:S(2)}) async-start(bf16[8,32,2048]{2,1,0:T(8,128)(2,1)} %get-tuple-element.22), calls=%async_computation | async-start | bytes 2097152 | tf_op jit(solution)/shard_map/all_to_all | solution.py:84
  12.6 30.2 %all-gather = bf16[3584,128]{1,0:T(8,128)(2,1)S(1)} all-gather(bf16[224,128]{1,0:T(8,128)(2,1)S(1)} %copy-done.9), channel_id=2, replica_groups=mesh['sp'=16,'fs'=4,'tp'=8] {'sp'}, dimensions={0}, use_global_device_ids=true | all-gather | bytes 974848 | tf_op jit(solution)/shard_map/all_gather | solution.py:376
  42.8 4.8 %collective-permute-start.3 = (bf16[16,64,128]{2,1,0:T(8,128)(2,1)S(1)}, bf16[16,64,128]{2,1,0:T(8,128)(2,1)S(1)}, u32[]{:S(2)}, u32[]{:S(2)}) collective-permute-start(bf16[16,64,128]{2,1,0:T(8,128)(2,1)S(1)} %slice.13.w0_ref), channel_id=1, source_target_pairs={{0,24},{8,0},{16,8},{24,16},{1,25},{9,1},{17,9},{25,17},{2,26},{10... | collective-permute-start | bytes 786440 | tf_op jit(solution)/shard_map/ppermute | solution.py:93
  47.7 2.4 %collective-permute-start.6 = (bf16[16,160,128]{2,1,0:T(8,128)(2,1)S(1)}, bf16[16,160,128]{2,1,0:T(8,128)(2,1)S(1)}, u32[]{:S(2)}, u32[]{:S(2)}) collective-permute-start(bf16[16,160,128]{2,1,0:T(8,128)(2,1)S(1)} %slice.14.w0_ref), channel_id=1, source_target_pairs={{0,24},{8,0},{16,8},{24,16},{1,25},{9,1},{17,9},{25,17},{2,26},{10... | collective-permute-start | bytes 1966088 | tf_op jit(solution)/shard_map/ppermute | solution.py:93
  50.1 1.9 %collective-permute-start.5 = (bf16[16,160,128]{2,1,0:T(8,128)(2,1)S(1)}, bf16[16,160,128]{2,1,0:T(8,128)(2,1)S(1)}, u32[]{:S(2)}, u32[]{:S(2)}) collective-permute-start(bf16[16,160,128]{2,1,0:T(8,128)(2,1)S(1)} %slice.14.w0_ref), channel_id=1, source_target_pairs={{0,16},{8,24},{16,0},{24,8},{1,17},{9,25},{17,1},{25,9},{2,18},{10... | collective-permute-start | bytes 1966088 | tf_op jit(solution)/shard_map/ppermute | solution.py:93
  52.0 4.9 %collective-permute-start.2 = (bf16[16,64,128]{2,1,0:T(8,128)(2,1)S(1)}, bf16[16,64,128]{2,1,0:T(8,128)(2,1)}, u32[]{:S(2)}, u32[]{:S(2)}) collective-permute-start(bf16[16,64,128]{2,1,0:T(8,128)(2,1)S(1)} %slice.13.w0_ref), channel_id=1, source_target_pairs={{0,16},{8,24},{16,0},{24,8},{1,17},{9,25},{17,1},{25,9},{2,18},{10... | collective-permute-start | bytes 786440 | tf_op jit(solution)/shard_map/ppermute | solution.py:93
  56.9 2.9 %collective-permute-start.4 = (bf16[16,160,128]{2,1,0:T(8,128)(2,1)S(1)}, bf16[16,160,128]{2,1,0:T(8,128)(2,1)}, u32[]{:S(2)}, u32[]{:S(2)}) collective-permute-start(bf16[16,160,128]{2,1,0:T(8,128)(2,1)S(1)} %slice.14.w0_ref), channel_id=1, source_target_pairs={{0,8},{8,16},{16,24},{24,0},{1,9},{9,17},{17,25},{25,1},{2,10},{10... | collective-permute-start | bytes 1966088 | tf_op jit(solution)/shard_map/ppermute | solution.py:93
  60.5 1.9 %collective-permute-start.1 = (bf16[16,64,128]{2,1,0:T(8,128)(2,1)S(1)}, bf16[16,64,128]{2,1,0:T(8,128)(2,1)}, u32[]{:S(2)}, u32[]{:S(2)}) collective-permute-start(bf16[16,64,128]{2,1,0:T(8,128)(2,1)S(1)} %slice.13.w0_ref), channel_id=1, source_target_pairs={{0,8},{8,16},{16,24},{24,0},{1,9},{9,17},{17,25},{25,1},{2,10},{10... | collective-permute-start | bytes 786440 | tf_op jit(solution)/shard_map/ppermute | solution.py:93
  62.5 6.1 %collective-permute-done.2.w2_ref = bf16[16,64,128]{2,1,0:T(8,128)(2,1)} collective-permute-done((bf16[16,64,128]{2,1,0:T(8,128)(2,1)S(1)}, bf16[16,64,128]{2,1,0:T(8,128)(2,1)}, u32[]{:S(2)}, u32[]{:S(2)}) %collective-permute-start.2) | collective-permute-done | bytes 262176 | tf_op jit(solution)/shard_map/ppermute | solution.py:93
  68.6 2.3 %collective-permute-start = (bf16[16,2048]{1,0:T(8,128)(2,1)S(1)}, bf16[16,2048]{1,0:T(8,128)(2,1)S(1)}, u32[]{:S(2)}, u32[]{:S(2)}) collective-permute-start(bf16[16,2048]{1,0:T(8,128)(2,1)S(1)} %slice.12), channel_id=1, source_target_pairs={{0,32},{32,64},{64,96},{96,128},{128,160},{160,192},{192,224},{224... | collective-permute-start | bytes 196616 | tf_op jit(solution)/shard_map/ppermute | solution.py:373
  72.8 21.8 %collective-permute-done.1.w1_ref = bf16[16,64,128]{2,1,0:T(8,128)(2,1)} collective-permute-done((bf16[16,64,128]{2,1,0:T(8,128)(2,1)S(1)}, bf16[16,64,128]{2,1,0:T(8,128)(2,1)}, u32[]{:S(2)}, u32[]{:S(2)}) %collective-permute-start.1) | collective-permute-done | bytes 262176 | tf_op jit(solution)/shard_map/ppermute | solution.py:93
  94.6 4.7 %shard_map.165 = (bf16[128,256]{1,0:T(8,128)(2,1)S(1)}, f32[256,128]{1,0:T(8,128)S(1)}, f32[256,256]{1,0:T(8,128)S(1)}, bf16[272,2048]{1,0:T(8,128)(2,1)S(1)}) custom-call(s32[1]{0:T(128)} %bitcast.sp_ref, s32[1]{0:T(128)} %bitcast.1.tp_ref, s32[1]{0:T(128)} %bitcast.2.fs_ref, bf16[256,2048]{1,0:T(8,128)(2,1)S(1)} %bitcast.13, ...), custom_call_target="tpu_custom_call" | custom-call | flops 1342177280 | tf_op jit(solution)/shard_map/pallas_call | solution.py:21
  99.4 2.3 %collective-permute-start.7 = (bf16[128,256]{1,0:T(8,128)(2,1)S(1)}, bf16[128,256]{1,0:T(8,128)(2,1)S(1)}, u32[]{:S(2)}, u32[]{:S(2)}) collective-permute-start(bf16[128,256]{1,0:T(8,128)(2,1)S(1)} %get-tuple-element.30.own_ref), channel_id=1, source_target_pairs={{0,32},{32,0},{64,96},{96,64},{128,160},{160,128},{192,224},{224,1... | collective-permute-start | bytes 196616 | tf_op jit(solution)/shard_map/ppermute | solution.py:409
  101.7 2.7 %collective-permute-done.7.other_ref = bf16[128,256]{1,0:T(8,128)(2,1)S(1)} collective-permute-done((bf16[128,256]{1,0:T(8,128)(2,1)S(1)}, bf16[128,256]{1,0:T(8,128)(2,1)S(1)}, u32[]{:S(2)}, u32[]{:S(2)}) %collective-permute-start.7) | collective-permute-done | bytes 65568 | tf_op jit(solution)/shard_map/ppermute | solution.py:409
  104.6 1.9 %collective-permute-start.8 = (bf16[128,256]{1,0:T(8,128)(2,1)S(1)}, bf16[128,256]{1,0:T(8,128)(2,1)S(1)}, u32[]{:S(2)}, u32[]{:S(2)}) collective-permute-start(bf16[128,256]{1,0:T(8,128)(2,1)S(1)} %get-tuple-element.31.own_ref), channel_id=1, source_target_pairs={{0,64},{32,96},{64,0},{96,32},{128,192},{160,224},{192,128},{224,1... | collective-permute-start | bytes 196616 | tf_op jit(solution)/shard_map/ppermute | solution.py:409
  106.5 4.7 %collective-permute-done.8.other_ref = bf16[128,256]{1,0:T(8,128)(2,1)S(1)} collective-permute-done((bf16[128,256]{1,0:T(8,128)(2,1)S(1)}, bf16[128,256]{1,0:T(8,128)(2,1)S(1)}, u32[]{:S(2)}, u32[]{:S(2)}) %collective-permute-start.8) | collective-permute-done | bytes 65568 | tf_op jit(solution)/shard_map/ppermute | solution.py:409
  111.4 3.2 %collective-permute-start.9 = (bf16[128,256]{1,0:T(8,128)(2,1)S(1)}, bf16[128,256]{1,0:T(8,128)(2,1)S(1)}, u32[]{:S(2)}, u32[]{:S(2)}) collective-permute-start(bf16[128,256]{1,0:T(8,128)(2,1)S(1)} %get-tuple-element.33), channel_id=1, source_target_pairs={{0,128},{32,160},{64,192},{96,224},{128,256},{160,288},{192,320},{... | collective-permute-start | bytes 196616 | tf_op jit(solution)/shard_map/ppermute | solution.py:430
  115.3 4.2 %collective-permute-start.12 = (bf16[128,128]{1,0:T(8,128)(2,1)S(1)}, bf16[128,128]{1,0:T(8,128)(2,1)S(1)}, u32[]{:S(2)}, u32[]{:S(2)}) collective-permute-start(bf16[128,128]{1,0:T(8,128)(2,1)S(1)} %get-tuple-element.35), channel_id=1, source_target_pairs={{0,384},{32,416},{64,448},{96,480},{1,385},{33,417},{65,449},{97,4... | collective-permute-start | bytes 98312 | tf_op jit(solution)/shard_map/ppermute | solution.py:430
  119.5 5.7 %collective-permute-start.11 = (bf16[128,128]{1,0:T(8,128)(2,1)S(1)}, bf16[128,128]{1,0:T(8,128)(2,1)S(1)}, u32[]{:S(2)}, u32[]{:S(2)}) collective-permute-start(bf16[128,128]{1,0:T(8,128)(2,1)S(1)} %get-tuple-element.35), channel_id=1, source_target_pairs={{0,256},{32,288},{64,320},{96,352},{128,384},{160,416},{192,448},{... | collective-permute-start | bytes 98312 | tf_op jit(solution)/shard_map/ppermute | solution.py:430
  126.2 3.4 %shard_map.168 = (bf16[4,32,2048]{2,1,0:T(8,128)(2,1)S(1)}, bf16[4,32,2048]{2,1,0:T(8,128)(2,1)S(1)}) custom-call(s32[1]{0:T(128)} %bitcast.sp_ref, s32[1]{0:T(128)} %bitcast.1.tp_ref, s32[1]{0:T(128)} %bitcast.2.fs_ref, bf16[272,2048]{1,0:T(8,128)(2,1)S(1)} %get-tuple-element.27.xn_ref, bf16[16,160,128]{2,1,0:T(8,128)(2,1)S(1)} %slice.14.w0_ref, ...), custom_call_target="tpu_custom_call" | custom-call | flops 1342177280 | tf_op jit(solution)/shard_map/pallas_call | solution.py:21
  129.6 6.1 %collective-permute-start.13 = (bf16[4,32,2048]{2,1,0:T(8,128)(2,1)S(1)}, bf16[4,32,2048]{2,1,0:T(8,128)(2,1)S(1)}, u32[]{:S(2)}, u32[]{:S(2)}) collective-permute-start(bf16[4,32,2048]{2,1,0:T(8,128)(2,1)S(1)} %get-tuple-element.38), channel_id=1, source_target_pairs={{0,1},{1,0},{2,3},{3,2},{4,5},{5,4},{6,7},{7,6},{8,9},{9,8},{10,11... | collective-permute-start | bytes 1572872 | tf_op jit(solution)/shard_map/ppermute | solution.py:452
  135.8 1.5 %collective-permute-done.13.theirs_ref = bf16[4,32,2048]{2,1,0:T(8,128)(2,1)S(1)} collective-permute-done((bf16[4,32,2048]{2,1,0:T(8,128)(2,1)S(1)}, bf16[4,32,2048]{2,1,0:T(8,128)(2,1)S(1)}, u32[]{:S(2)}, u32[]{:S(2)}) %collective-permute-start.13) | collective-permute-done | bytes 524320 | tf_op jit(solution)/shard_map/ppermute | solution.py:452
  137.4 11.7 %all_to_all.10.in_ref = bf16[4,32,2048]{2,1,0:T(8,128)(2,1)S(1)} all-to-all(bf16[4,32,2048]{2,1,0:T(8,128)(2,1)S(1)} %shard_map.169), channel_id=1, replica_groups={{0,2,4,6},{1,3,5,7},{8,10,12,14},{9,11,13,15},{16,18,20,22},{17,19,21,2..., dimensions={0} | all-to-all | bytes 1048576 | tf_op jit(solution)/shard_map/all_to_all | solution.py:84
  (39 shorter events, 4.9 us)
Async XLA Ops:
  2.2 10.4 %copy-start.9 = (bf16[224,128]{1,0:T(8,128)(2,1)S(1)}, bf16[224,128]{1,0:T(8,128)(2,1)}, u32[]{:S(2)}) copy-start(bf16[224,128]{1,0:T(8,128)(2,1)} %get-tuple-element.23) | copy-start | bytes 172036
  2.2 60.3 %all-to-all-start = ((bf16[8,32,2048]{2,1,0:T(8,128)(2,1)}), bf16[8,32,2048]{2,1,0:T(8,128)(2,1)S(1)}, u32[]{:S(2)}, u32[]{:S(2)}) async-start(bf16[8,32,2048]{2,1,0:T(8,128)(2,1)} %get-tuple-element.22), calls=%async_computation | async-start | bytes 2097152 | tf_op jit(solution)/shard_map/all_to_all | solution.py:84
  42.7 28.8 %copy-start = (bf16[2048,8]{0,1:T(8,128)(2,1)S(1)}, bf16[2048,8]{0,1:T(8,128)(2,1)}, u32[]{:S(2)}) copy-start(bf16[2048,8]{0,1:T(8,128)(2,1)} %param.24) | copy-start | bytes 98308
  42.7 28.8 %copy-start.1 = (bf16[2048,8]{0,1:T(8,128)(2,1)S(1)}, bf16[2048,8]{0,1:T(8,128)(2,1)}, u32[]{:S(2)}) copy-start(bf16[2048,8]{0,1:T(8,128)(2,1)} %param.25) | copy-start | bytes 98308
  42.8 28.8 %copy-start.2 = (f32[256,1]{0,1:T(1,128)S(1)}, f32[256,1]{0,1:T(1,128)}, u32[]{:S(2)}) copy-start(f32[256,1]{0,1:T(1,128)} %param.28) | copy-start | bytes 3076
  42.8 51.8 %copy-start.6 = (f32[3,4,128]{2,1,0:T(4,128)S(1)}, f32[3,4,128]{2,1,0:T(4,128)}, u32[]{:S(2)}) copy-start(f32[3,4,128]{2,1,0:T(4,128)} %taps_ref.3) | copy-start | bytes 18436
  42.8 17.0 %collective-permute-start.3 = (bf16[16,64,128]{2,1,0:T(8,128)(2,1)S(1)}, bf16[16,64,128]{2,1,0:T(8,128)(2,1)S(1)}, u32[]{:S(2)}, u32[]{:S(2)}) collective-permute-start(bf16[16,64,128]{2,1,0:T(8,128)(2,1)S(1)} %slice.13.w0_ref), channel_id=1, source_target_pairs={{0,24},{8,0},{16,8},{24,16},{1,25},{9,1},{17,9},{25,17},{2,26},{10... | collective-permute-start | bytes 786440 | tf_op jit(solution)/shard_map/ppermute | solution.py:93
  47.7 67.6 %collective-permute-start.6 = (bf16[16,160,128]{2,1,0:T(8,128)(2,1)S(1)}, bf16[16,160,128]{2,1,0:T(8,128)(2,1)S(1)}, u32[]{:S(2)}, u32[]{:S(2)}) collective-permute-start(bf16[16,160,128]{2,1,0:T(8,128)(2,1)S(1)} %slice.14.w0_ref), channel_id=1, source_target_pairs={{0,24},{8,0},{16,8},{24,16},{1,25},{9,1},{17,9},{25,17},{2,26},{10... | collective-permute-start | bytes 1966088 | tf_op jit(solution)/shard_map/ppermute | solution.py:93
  50.1 69.4 %collective-permute-start.5 = (bf16[16,160,128]{2,1,0:T(8,128)(2,1)S(1)}, bf16[16,160,128]{2,1,0:T(8,128)(2,1)S(1)}, u32[]{:S(2)}, u32[]{:S(2)}) collective-permute-start(bf16[16,160,128]{2,1,0:T(8,128)(2,1)S(1)} %slice.14.w0_ref), channel_id=1, source_target_pairs={{0,16},{8,24},{16,0},{24,8},{1,17},{9,25},{17,1},{25,9},{2,18},{10... | collective-permute-start | bytes 1966088 | tf_op jit(solution)/shard_map/ppermute | solution.py:93
  52.0 16.6 %collective-permute-start.2 = (bf16[16,64,128]{2,1,0:T(8,128)(2,1)S(1)}, bf16[16,64,128]{2,1,0:T(8,128)(2,1)}, u32[]{:S(2)}, u32[]{:S(2)}) collective-permute-start(bf16[16,64,128]{2,1,0:T(8,128)(2,1)S(1)} %slice.13.w0_ref), channel_id=1, source_target_pairs={{0,16},{8,24},{16,0},{24,8},{1,17},{9,25},{17,1},{25,9},{2,18},{10... | collective-permute-start | bytes 786440 | tf_op jit(solution)/shard_map/ppermute | solution.py:93
  56.9 68.4 %collective-permute-start.4 = (bf16[16,160,128]{2,1,0:T(8,128)(2,1)S(1)}, bf16[16,160,128]{2,1,0:T(8,128)(2,1)}, u32[]{:S(2)}, u32[]{:S(2)}) collective-permute-start(bf16[16,160,128]{2,1,0:T(8,128)(2,1)S(1)} %slice.14.w0_ref), channel_id=1, source_target_pairs={{0,8},{8,16},{16,24},{24,0},{1,9},{9,17},{17,25},{25,1},{2,10},{10... | collective-permute-start | bytes 1966088 | tf_op jit(solution)/shard_map/ppermute | solution.py:93
  60.5 34.1 %collective-permute-start.1 = (bf16[16,64,128]{2,1,0:T(8,128)(2,1)S(1)}, bf16[16,64,128]{2,1,0:T(8,128)(2,1)}, u32[]{:S(2)}, u32[]{:S(2)}) collective-permute-start(bf16[16,64,128]{2,1,0:T(8,128)(2,1)S(1)} %slice.13.w0_ref), channel_id=1, source_target_pairs={{0,8},{8,16},{16,24},{24,0},{1,9},{9,17},{17,25},{25,1},{2,10},{10... | collective-permute-start | bytes 786440 | tf_op jit(solution)/shard_map/ppermute | solution.py:93
  62.4 32.2 %copy-start.4 = (bf16[16,64,128]{2,1,0:T(8,128)(2,1)S(1)}, bf16[16,64,128]{2,1,0:T(8,128)(2,1)}, u32[]{:S(2)}) copy-start(bf16[16,64,128]{2,1,0:T(8,128)(2,1)} %copy-done.3) | copy-start | bytes 786436
  68.6 26.0 %collective-permute-start = (bf16[16,2048]{1,0:T(8,128)(2,1)S(1)}, bf16[16,2048]{1,0:T(8,128)(2,1)S(1)}, u32[]{:S(2)}, u32[]{:S(2)}) collective-permute-start(bf16[16,2048]{1,0:T(8,128)(2,1)S(1)} %slice.12), channel_id=1, source_target_pairs={{0,32},{32,64},{64,96},{96,128},{128,160},{160,192},{192,224},{224... | collective-permute-start | bytes 196616 | tf_op jit(solution)/shard_map/ppermute | solution.py:373
  94.6 31.6 %copy-start.5 = (bf16[1,128,128]{2,1,0:T(8,128)(2,1)S(1)}, bf16[1,128,128]{2,1,0:T(8,128)(2,1)}, u32[]{:S(2)}) copy-start(bf16[1,128,128]{2,1,0:T(8,128)(2,1)} %param.29) | copy-start | bytes 98308
  94.6 31.6 %copy-start.7 = (f32[128]{0:T(128)S(1)}, f32[128]{0:T(128)}, u32[]{:S(2)}) copy-start(f32[128]{0:T(128)} %param.30) | copy-start | bytes 1540
  94.6 31.6 %copy-start.8 = (f32[128]{0:T(128)S(1)}, f32[128]{0:T(128)}, u32[]{:S(2)}) copy-start(f32[128]{0:T(128)} %param.31) | copy-start | bytes 1540
  99.4 5.0 %collective-permute-start.7 = (bf16[128,256]{1,0:T(8,128)(2,1)S(1)}, bf16[128,256]{1,0:T(8,128)(2,1)S(1)}, u32[]{:S(2)}, u32[]{:S(2)}) collective-permute-start(bf16[128,256]{1,0:T(8,128)(2,1)S(1)} %get-tuple-element.30.own_ref), channel_id=1, source_target_pairs={{0,32},{32,0},{64,96},{96,64},{128,160},{160,128},{192,224},{224,1... | collective-permute-start | bytes 196616 | tf_op jit(solution)/shard_map/ppermute | solution.py:409
  104.6 6.6 %collective-permute-start.8 = (bf16[128,256]{1,0:T(8,128)(2,1)S(1)}, bf16[128,256]{1,0:T(8,128)(2,1)S(1)}, u32[]{:S(2)}, u32[]{:S(2)}) collective-permute-start(bf16[128,256]{1,0:T(8,128)(2,1)S(1)} %get-tuple-element.31.own_ref), channel_id=1, source_target_pairs={{0,64},{32,96},{64,0},{96,32},{128,192},{160,224},{192,128},{224,1... | collective-permute-start | bytes 196616 | tf_op jit(solution)/shard_map/ppermute | solution.py:409
  111.4 14.8 %collective-permute-start.9 = (bf16[128,256]{1,0:T(8,128)(2,1)S(1)}, bf16[128,256]{1,0:T(8,128)(2,1)S(1)}, u32[]{:S(2)}, u32[]{:S(2)}) collective-permute-start(bf16[128,256]{1,0:T(8,128)(2,1)S(1)} %get-tuple-element.33), channel_id=1, source_target_pairs={{0,128},{32,160},{64,192},{96,224},{128,256},{160,288},{192,320},{... | collective-permute-start | bytes 196616 | tf_op jit(solution)/shard_map/ppermute | solution.py:430
  114.6 10.6 %collective-permute-start.10 = (bf16[128,128]{1,0:T(8,128)(2,1)S(1)}, bf16[128,128]{1,0:T(8,128)(2,1)S(1)}, u32[]{:S(2)}, u32[]{:S(2)}) collective-permute-start(bf16[128,128]{1,0:T(8,128)(2,1)S(1)} %get-tuple-element.34), channel_id=1, source_target_pairs={{128,384},{160,416},{192,448},{224,480},{129,385},{161,417},{193,4... | collective-permute-start | bytes 98312 | tf_op jit(solution)/shard_map/ppermute | solution.py:430
  115.3 10.0 %collective-permute-start.12 = (bf16[128,128]{1,0:T(8,128)(2,1)S(1)}, bf16[128,128]{1,0:T(8,128)(2,1)S(1)}, u32[]{:S(2)}, u32[]{:S(2)}) collective-permute-start(bf16[128,128]{1,0:T(8,128)(2,1)S(1)} %get-tuple-element.35), channel_id=1, source_target_pairs={{0,384},{32,416},{64,448},{96,480},{1,385},{33,417},{65,449},{97,4... | collective-permute-start | bytes 98312 | tf_op jit(solution)/shard_map/ppermute | solution.py:430
  119.5 6.8 %collective-permute-start.11 = (bf16[128,128]{1,0:T(8,128)(2,1)S(1)}, bf16[128,128]{1,0:T(8,128)(2,1)S(1)}, u32[]{:S(2)}, u32[]{:S(2)}) collective-permute-start(bf16[128,128]{1,0:T(8,128)(2,1)S(1)} %get-tuple-element.35), channel_id=1, source_target_pairs={{0,256},{32,288},{64,320},{96,352},{128,384},{160,416},{192,448},{... | collective-permute-start | bytes 98312 | tf_op jit(solution)/shard_map/ppermute | solution.py:430
  129.6 7.7 %collective-permute-start.13 = (bf16[4,32,2048]{2,1,0:T(8,128)(2,1)S(1)}, bf16[4,32,2048]{2,1,0:T(8,128)(2,1)S(1)}, u32[]{:S(2)}, u32[]{:S(2)}) collective-permute-start(bf16[4,32,2048]{2,1,0:T(8,128)(2,1)S(1)} %get-tuple-element.38), channel_id=1, source_target_pairs={{0,1},{1,0},{2,3},{3,2},{4,5},{5,4},{6,7},{7,6},{8,9},{9,8},{10,11... | collective-permute-start | bytes 1572872 | tf_op jit(solution)/shard_map/ppermute | solution.py:452
  (1 other events, 0.7 us)

commit v8 on v7

--- a/solution.py
+++ b/solution.py
@@ -211,10 +211,8 @@
     ab_ref[:, width:] = made[:, :width].astype(BF16)
 
 
-def step_map(later, carry, width):
-    ch, cl = split(carry)
-    linear = later[:, :width]
-    moved = dot(linear, ch) + dot(linear, cl)
+def step_map(later, earlier, width):
+    moved = dot(later[:, :width], earlier)
     offset = later[:, width:].astype(F32)
     return jnp.concatenate([moved[:, :width], moved[:, width:] + offset], axis=1)
 
@@ -225,7 +223,7 @@
     own, other = own_ref[...], other_ref[...]
     earlier = jnp.where(odd, other, own)
     later = jnp.where(odd, own, other)
-    pair_ref[...] = step_map(later, earlier.astype(F32), width).astype(BF16)
+    pair_ref[...] = step_map(later, earlier, width).astype(BF16)
     r = lax.broadcasted_iota(jnp.int32, (width, 2 * width), 0)
     c = lax.broadcasted_iota(jnp.int32, (width, 2 * width), 1)
     before_ref[...] = jnp.where(odd, other, jnp.where(r == c, 1.0, 0.0).astype(BF16))
@@ -240,12 +238,12 @@
     own, other = own_ref[...], other_ref[...]
     earlier = jnp.where(upper, other, own)
     later = jnp.where(upper, own, other)
-    total = step_map(later, earlier.astype(F32), width).astype(BF16)
+    total = step_map(later, earlier, width).astype(BF16)
     total_ref[...] = total
     linear_ref[...] = total[:, :width]
     offset_ref[...] = total[:, width:]
     inner = inner_ref[...]
-    behind = step_map(inner, other.astype(F32), width)
+    behind = step_map(inner, other, width)
     before_ref[...] = jnp.where(upper, behind, inner.astype(F32))
 
 
@@ -262,7 +260,7 @@
 ):
     length, width = k_ref.shape
     pieces = (w0_ref, w1_ref, w2_ref, w3_ref)
-    state = apply(a8_ref[...], b12_ref[...].astype(F32)) + b8_ref[...].astype(F32)
+    state = dot(a8_ref[...], b12_ref[...]) + b8_ref[...].astype(F32)
     state = apply(t4_ref[:, :width], state) + t4_ref[:, width:].astype(F32)
     state = dot3(before_ref[:, :width], state) + before_ref[:, width:]
     gather_two(fs_ref[0], pieces, w_scr)

time: 152 us -> 151 us (level)
  no operation moved by 1% of the time
where the time goes in v8:
time: 151 us; the launch traced here: 150 us
  starting transfers between devices  55.6 us (37%)
  blocking collectives  41.9 us (28%)
  waiting for transfers between devices  37.9 us (25%)
  Pallas kernels  12.6 us (8%)
    all_gather x1, blocking collectives, layer(): quarters = lax.all_gather(part, 'sp', axis=0)  30.2 us
    ppermute x6, waiting for transfers between devices, turns(): lax.ppermute(x, axis, [(i, i - i % size + (i + d) % size) for i in range(...  28 us
    ppermute x6, starting transfers between devices, turns(): lax.ppermute(x, axis, [(i, i - i % size + (i + d) % size) for i in range(...  18.8 us
    ppermute x4, starting transfers between devices, from_behind(): lax.ppermute(x, 'sp', [(i, i + distance) for i in range(first, last)])  13.7 us
    pallas_call x8, Pallas kernels, call(): pl.pallas_call(kernel, out_shape=list(outs) if many else outs, in_specs=i...  12.6 us
    all_to_all x1, blocking collectives, exchange(): lax.all_to_all(copies, axis, split_axis=0, concat_axis=0, tiled=True, axi...  11.7 us
    all_to_all x1, starting transfers between devices, exchange(): lax.all_to_all(copies, axis, split_axis=0, concat_axis=0, tiled=True, axi...  10.4 us
    ppermute x2, waiting for transfers between devices, meet(): return lax.ppermute(x, 'sp', [(i, i ^ distance) for i in range(n_sp)])  7.39 us
  transfers between devices with their start and end apart: 15, of which 6 were waited for; matrix products, arithmetic and copies ran while one was open for 0% of the time, Pallas kernels for 4%

profile of v8, /device:TPU:1, one launch (start us, length us, event | category | flops | bytes accessed | tf_op | source)
XLA Modules:
  0.0 149.8 jit_solution(16113180057190808106)
XLA Ops:
  0.0 2.2 %shard_map.163 = (bf16[8,32,2048]{2,1,0:T(8,128)(2,1)}, bf16[224,128]{1,0:T(8,128)(2,1)}) custom-call(s32[1]{0:T(128)} %bitcast.sp_ref, s32[1]{0:T(128)} %bitcast.1.tp_ref, s32[1]{0:T(128)} %bitcast.2.fs_ref, bf16[32,2048]{1,0:T(8,128)(2,1)} %tok_ref.1, bf16[2048]{0:T(1024)(128)(2,1)} %gain_ref.1, bf16[128,128]{1,0:T(8,128)(2,1)} %k_ref.1, ...), custom_call_target="tpu_custom_call" | custom-call | tf_op jit(solution)/shard_map/pallas_call | solution.py:21
  2.2 10.4 %all-to-all-start = ((bf16[8,32,2048]{2,1,0:T(8,128)(2,1)}), bf16[8,32,2048]{2,1,0:T(8,128)(2,1)S(1)}, u32[]{:S(2)}, u32[]{:S(2)}) async-start(bf16[8,32,2048]{2,1,0:T(8,128)(2,1)} %get-tuple-element.22), calls=%async_computation | async-start | bytes 2097152 | tf_op jit(solution)/shard_map/all_to_all | solution.py:84
  12.6 30.2 %all-gather = bf16[3584,128]{1,0:T(8,128)(2,1)S(1)} all-gather(bf16[224,128]{1,0:T(8,128)(2,1)S(1)} %copy-done.9), channel_id=2, replica_groups=mesh['sp'=16,'fs'=4,'tp'=8] {'sp'}, dimensions={0}, use_global_device_ids=true | all-gather | bytes 974848 | tf_op jit(solution)/shard_map/all_gather | solution.py:374
  42.8 4.8 %collective-permute-start.3 = (bf16[16,64,128]{2,1,0:T(8,128)(2,1)S(1)}, bf16[16,64,128]{2,1,0:T(8,128)(2,1)S(1)}, u32[]{:S(2)}, u32[]{:S(2)}) collective-permute-start(bf16[16,64,128]{2,1,0:T(8,128)(2,1)S(1)} %slice.13.w0_ref), channel_id=1, source_target_pairs={{0,24},{8,0},{16,8},{24,16},{1,25},{9,1},{17,9},{25,17},{2,26},{10... | collective-permute-start | bytes 786440 | tf_op jit(solution)/shard_map/ppermute | solution.py:93
  47.7 2.4 %collective-permute-start.6 = (bf16[16,160,128]{2,1,0:T(8,128)(2,1)S(1)}, bf16[16,160,128]{2,1,0:T(8,128)(2,1)S(1)}, u32[]{:S(2)}, u32[]{:S(2)}) collective-permute-start(bf16[16,160,128]{2,1,0:T(8,128)(2,1)S(1)} %slice.14.w0_ref), channel_id=1, source_target_pairs={{0,24},{8,0},{16,8},{24,16},{1,25},{9,1},{17,9},{25,17},{2,26},{10... | collective-permute-start | bytes 1966088 | tf_op jit(solution)/shard_map/ppermute | solution.py:93
  50.1 1.9 %collective-permute-start.5 = (bf16[16,160,128]{2,1,0:T(8,128)(2,1)S(1)}, bf16[16,160,128]{2,1,0:T(8,128)(2,1)S(1)}, u32[]{:S(2)}, u32[]{:S(2)}) collective-permute-start(bf16[16,160,128]{2,1,0:T(8,128)(2,1)S(1)} %slice.14.w0_ref), channel_id=1, source_target_pairs={{0,16},{8,24},{16,0},{24,8},{1,17},{9,25},{17,1},{25,9},{2,18},{10... | collective-permute-start | bytes 1966088 | tf_op jit(solution)/shard_map/ppermute | solution.py:93
  52.0 4.9 %collective-permute-start.2 = (bf16[16,64,128]{2,1,0:T(8,128)(2,1)S(1)}, bf16[16,64,128]{2,1,0:T(8,128)(2,1)}, u32[]{:S(2)}, u32[]{:S(2)}) collective-permute-start(bf16[16,64,128]{2,1,0:T(8,128)(2,1)S(1)} %slice.13.w0_ref), channel_id=1, source_target_pairs={{0,16},{8,24},{16,0},{24,8},{1,17},{9,25},{17,1},{25,9},{2,18},{10... | collective-permute-start | bytes 786440 | tf_op jit(solution)/shard_map/ppermute | solution.py:93
  56.9 2.9 %collective-permute-start.4 = (bf16[16,160,128]{2,1,0:T(8,128)(2,1)S(1)}, bf16[16,160,128]{2,1,0:T(8,128)(2,1)}, u32[]{:S(2)}, u32[]{:S(2)}) collective-permute-start(bf16[16,160,128]{2,1,0:T(8,128)(2,1)S(1)} %slice.14.w0_ref), channel_id=1, source_target_pairs={{0,8},{8,16},{16,24},{24,0},{1,9},{9,17},{17,25},{25,1},{2,10},{10... | collective-permute-start | bytes 1966088 | tf_op jit(solution)/shard_map/ppermute | solution.py:93
  60.5 1.9 %collective-permute-start.1 = (bf16[16,64,128]{2,1,0:T(8,128)(2,1)S(1)}, bf16[16,64,128]{2,1,0:T(8,128)(2,1)}, u32[]{:S(2)}, u32[]{:S(2)}) collective-permute-start(bf16[16,64,128]{2,1,0:T(8,128)(2,1)S(1)} %slice.13.w0_ref), channel_id=1, source_target_pairs={{0,8},{8,16},{16,24},{24,0},{1,9},{9,17},{17,25},{25,1},{2,10},{10... | collective-permute-start | bytes 786440 | tf_op jit(solution)/shard_map/ppermute | solution.py:93
  62.5 6.1 %collective-permute-done.2.w2_ref = bf16[16,64,128]{2,1,0:T(8,128)(2,1)} collective-permute-done((bf16[16,64,128]{2,1,0:T(8,128)(2,1)S(1)}, bf16[16,64,128]{2,1,0:T(8,128)(2,1)}, u32[]{:S(2)}, u32[]{:S(2)}) %collective-permute-start.2) | collective-permute-done | bytes 262176 | tf_op jit(solution)/shard_map/ppermute | solution.py:93
  68.6 2.3 %collective-permute-start = (bf16[16,2048]{1,0:T(8,128)(2,1)S(1)}, bf16[16,2048]{1,0:T(8,128)(2,1)S(1)}, u32[]{:S(2)}, u32[]{:S(2)}) collective-permute-start(bf16[16,2048]{1,0:T(8,128)(2,1)S(1)} %slice.12), channel_id=1, source_target_pairs={{0,32},{32,64},{64,96},{96,128},{128,160},{160,192},{192,224},{224... | collective-permute-start | bytes 196616 | tf_op jit(solution)/shard_map/ppermute | solution.py:371
  72.8 21.8 %collective-permute-done.1.w1_ref = bf16[16,64,128]{2,1,0:T(8,128)(2,1)} collective-permute-done((bf16[16,64,128]{2,1,0:T(8,128)(2,1)S(1)}, bf16[16,64,128]{2,1,0:T(8,128)(2,1)}, u32[]{:S(2)}, u32[]{:S(2)}) %collective-permute-start.1) | collective-permute-done | bytes 262176 | tf_op jit(solution)/shard_map/ppermute | solution.py:93
  94.6 4.7 %shard_map.165 = (bf16[128,256]{1,0:T(8,128)(2,1)S(1)}, f32[256,128]{1,0:T(8,128)S(1)}, f32[256,256]{1,0:T(8,128)S(1)}, bf16[272,2048]{1,0:T(8,128)(2,1)S(1)}) custom-call(s32[1]{0:T(128)} %bitcast.sp_ref, s32[1]{0:T(128)} %bitcast.1.tp_ref, s32[1]{0:T(128)} %bitcast.2.fs_ref, bf16[256,2048]{1,0:T(8,128)(2,1)S(1)} %bitcast.13, ...), custom_call_target="tpu_custom_call" | custom-call | flops 1342177280 | tf_op jit(solution)/shard_map/pallas_call | solution.py:21
  99.4 2.3 %collective-permute-start.7 = (bf16[128,256]{1,0:T(8,128)(2,1)S(1)}, bf16[128,256]{1,0:T(8,128)(2,1)S(1)}, u32[]{:S(2)}, u32[]{:S(2)}) collective-permute-start(bf16[128,256]{1,0:T(8,128)(2,1)S(1)} %get-tuple-element.30.own_ref), channel_id=1, source_target_pairs={{0,32},{32,0},{64,96},{96,64},{128,160},{160,128},{192,224},{224,1... | collective-permute-start | bytes 196616 | tf_op jit(solution)/shard_map/ppermute | solution.py:407
  101.7 2.7 %collective-permute-done.7.other_ref = bf16[128,256]{1,0:T(8,128)(2,1)S(1)} collective-permute-done((bf16[128,256]{1,0:T(8,128)(2,1)S(1)}, bf16[128,256]{1,0:T(8,128)(2,1)S(1)}, u32[]{:S(2)}, u32[]{:S(2)}) %collective-permute-start.7) | collective-permute-done | bytes 65568 | tf_op jit(solution)/shard_map/ppermute | solution.py:407
  104.6 1.9 %collective-permute-start.8 = (bf16[128,256]{1,0:T(8,128)(2,1)S(1)}, bf16[128,256]{1,0:T(8,128)(2,1)S(1)}, u32[]{:S(2)}, u32[]{:S(2)}) collective-permute-start(bf16[128,256]{1,0:T(8,128)(2,1)S(1)} %get-tuple-element.31.own_ref), channel_id=1, source_target_pairs={{0,64},{32,96},{64,0},{96,32},{128,192},{160,224},{192,128},{224,1... | collective-permute-start | bytes 196616 | tf_op jit(solution)/shard_map/ppermute | solution.py:407
  106.5 4.7 %collective-permute-done.8.other_ref = bf16[128,256]{1,0:T(8,128)(2,1)S(1)} collective-permute-done((bf16[128,256]{1,0:T(8,128)(2,1)S(1)}, bf16[128,256]{1,0:T(8,128)(2,1)S(1)}, u32[]{:S(2)}, u32[]{:S(2)}) %collective-permute-start.8) | collective-permute-done | bytes 65568 | tf_op jit(solution)/shard_map/ppermute | solution.py:407
  111.4 3.2 %collective-permute-start.9 = (bf16[128,256]{1,0:T(8,128)(2,1)S(1)}, bf16[128,256]{1,0:T(8,128)(2,1)S(1)}, u32[]{:S(2)}, u32[]{:S(2)}) collective-permute-start(bf16[128,256]{1,0:T(8,128)(2,1)S(1)} %get-tuple-element.33), channel_id=1, source_target_pairs={{0,128},{32,160},{64,192},{96,224},{128,256},{160,288},{192,320},{... | collective-permute-start | bytes 196616 | tf_op jit(solution)/shard_map/ppermute | solution.py:428
  115.2 4.2 %collective-permute-start.12 = (bf16[128,128]{1,0:T(8,128)(2,1)S(1)}, bf16[128,128]{1,0:T(8,128)(2,1)S(1)}, u32[]{:S(2)}, u32[]{:S(2)}) collective-permute-start(bf16[128,128]{1,0:T(8,128)(2,1)S(1)} %get-tuple-element.35), channel_id=1, source_target_pairs={{0,384},{32,416},{64,448},{96,480},{1,385},{33,417},{65,449},{97,4... | collective-permute-start | bytes 98312 | tf_op jit(solution)/shard_map/ppermute | solution.py:428
  119.4 5.7 %collective-permute-start.11 = (bf16[128,128]{1,0:T(8,128)(2,1)S(1)}, bf16[128,128]{1,0:T(8,128)(2,1)S(1)}, u32[]{:S(2)}, u32[]{:S(2)}) collective-permute-start(bf16[128,128]{1,0:T(8,128)(2,1)S(1)} %get-tuple-element.35), channel_id=1, source_target_pairs={{0,256},{32,288},{64,320},{96,352},{128,384},{160,416},{192,448},{... | collective-permute-start | bytes 98312 | tf_op jit(solution)/shard_map/ppermute | solution.py:428
  126.2 3.4 %shard_map.168 = (bf16[4,32,2048]{2,1,0:T(8,128)(2,1)S(1)}, bf16[4,32,2048]{2,1,0:T(8,128)(2,1)S(1)}) custom-call(s32[1]{0:T(128)} %bitcast.sp_ref, s32[1]{0:T(128)} %bitcast.1.tp_ref, s32[1]{0:T(128)} %bitcast.2.fs_ref, bf16[272,2048]{1,0:T(8,128)(2,1)S(1)} %get-tuple-element.27.xn_ref, bf16[16,160,128]{2,1,0:T(8,128)(2,1)S(1)} %slice.14.w0_ref, ...), custom_call_target="tpu_custom_call" | custom-call | flops 1342177280 | tf_op jit(solution)/shard_map/pallas_call | solution.py:21
  129.5 6.1 %collective-permute-start.13 = (bf16[4,32,2048]{2,1,0:T(8,128)(2,1)S(1)}, bf16[4,32,2048]{2,1,0:T(8,128)(2,1)S(1)}, u32[]{:S(2)}, u32[]{:S(2)}) collective-permute-start(bf16[4,32,2048]{2,1,0:T(8,128)(2,1)S(1)} %get-tuple-element.38), channel_id=1, source_target_pairs={{0,1},{1,0},{2,3},{3,2},{4,5},{5,4},{6,7},{7,6},{8,9},{9,8},{10,11... | collective-permute-start | bytes 1572872 | tf_op jit(solution)/shard_map/ppermute | solution.py:450
  135.7 1.5 %collective-permute-done.13.theirs_ref = bf16[4,32,2048]{2,1,0:T(8,128)(2,1)S(1)} collective-permute-done((bf16[4,32,2048]{2,1,0:T(8,128)(2,1)S(1)}, bf16[4,32,2048]{2,1,0:T(8,128)(2,1)S(1)}, u32[]{:S(2)}, u32[]{:S(2)}) %collective-permute-start.13) | collective-permute-done | bytes 524320 | tf_op jit(solution)/shard_map/ppermute | solution.py:450
  137.3 11.7 %all_to_all.10.in_ref = bf16[4,32,2048]{2,1,0:T(8,128)(2,1)S(1)} all-to-all(bf16[4,32,2048]{2,1,0:T(8,128)(2,1)S(1)} %shard_map.169), channel_id=1, replica_groups={{0,2,4,6},{1,3,5,7},{8,10,12,14},{9,11,13,15},{16,18,20,22},{17,19,21,2..., dimensions={0} | all-to-all | bytes 1048576 | tf_op jit(solution)/shard_map/all_to_all | solution.py:84
  (39 shorter events, 4.8 us)
Async XLA Ops:
  2.2 10.4 %copy-start.9 = (bf16[224,128]{1,0:T(8,128)(2,1)S(1)}, bf16[224,128]{1,0:T(8,128)(2,1)}, u32[]{:S(2)}) copy-start(bf16[224,128]{1,0:T(8,128)(2,1)} %get-tuple-element.23) | copy-start | bytes 172036
  2.2 60.3 %all-to-all-start = ((bf16[8,32,2048]{2,1,0:T(8,128)(2,1)}), bf16[8,32,2048]{2,1,0:T(8,128)(2,1)S(1)}, u32[]{:S(2)}, u32[]{:S(2)}) async-start(bf16[8,32,2048]{2,1,0:T(8,128)(2,1)} %get-tuple-element.22), calls=%async_computation | async-start | bytes 2097152 | tf_op jit(solution)/shard_map/all_to_all | solution.py:84
  42.7 28.8 %copy-start = (bf16[2048,8]{0,1:T(8,128)(2,1)S(1)}, bf16[2048,8]{0,1:T(8,128)(2,1)}, u32[]{:S(2)}) copy-start(bf16[2048,8]{0,1:T(8,128)(2,1)} %param.24) | copy-start | bytes 98308
  42.7 28.8 %copy-start.1 = (bf16[2048,8]{0,1:T(8,128)(2,1)S(1)}, bf16[2048,8]{0,1:T(8,128)(2,1)}, u32[]{:S(2)}) copy-start(bf16[2048,8]{0,1:T(8,128)(2,1)} %param.25) | copy-start | bytes 98308
  42.8 28.8 %copy-start.2 = (f32[256,1]{0,1:T(1,128)S(1)}, f32[256,1]{0,1:T(1,128)}, u32[]{:S(2)}) copy-start(f32[256,1]{0,1:T(1,128)} %param.28) | copy-start | bytes 3076
  42.8 51.8 %copy-start.6 = (f32[3,4,128]{2,1,0:T(4,128)S(1)}, f32[3,4,128]{2,1,0:T(4,128)}, u32[]{:S(2)}) copy-start(f32[3,4,128]{2,1,0:T(4,128)} %taps_ref.3) | copy-start | bytes 18436
  42.8 17.0 %collective-permute-start.3 = (bf16[16,64,128]{2,1,0:T(8,128)(2,1)S(1)}, bf16[16,64,128]{2,1,0:T(8,128)(2,1)S(1)}, u32[]{:S(2)}, u32[]{:S(2)}) collective-permute-start(bf16[16,64,128]{2,1,0:T(8,128)(2,1)S(1)} %slice.13.w0_ref), channel_id=1, source_target_pairs={{0,24},{8,0},{16,8},{24,16},{1,25},{9,1},{17,9},{25,17},{2,26},{10... | collective-permute-start | bytes 786440 | tf_op jit(solution)/shard_map/ppermute | solution.py:93
  47.7 67.5 %collective-permute-start.6 = (bf16[16,160,128]{2,1,0:T(8,128)(2,1)S(1)}, bf16[16,160,128]{2,1,0:T(8,128)(2,1)S(1)}, u32[]{:S(2)}, u32[]{:S(2)}) collective-permute-start(bf16[16,160,128]{2,1,0:T(8,128)(2,1)S(1)} %slice.14.w0_ref), channel_id=1, source_target_pairs={{0,24},{8,0},{16,8},{24,16},{1,25},{9,1},{17,9},{25,17},{2,26},{10... | collective-permute-start | bytes 1966088 | tf_op jit(solution)/shard_map/ppermute | solution.py:93
  50.1 69.3 %collective-permute-start.5 = (bf16[16,160,128]{2,1,0:T(8,128)(2,1)S(1)}, bf16[16,160,128]{2,1,0:T(8,128)(2,1)S(1)}, u32[]{:S(2)}, u32[]{:S(2)}) collective-permute-start(bf16[16,160,128]{2,1,0:T(8,128)(2,1)S(1)} %slice.14.w0_ref), channel_id=1, source_target_pairs={{0,16},{8,24},{16,0},{24,8},{1,17},{9,25},{17,1},{25,9},{2,18},{10... | collective-permute-start | bytes 1966088 | tf_op jit(solution)/shard_map/ppermute | solution.py:93
  52.0 16.6 %collective-permute-start.2 = (bf16[16,64,128]{2,1,0:T(8,128)(2,1)S(1)}, bf16[16,64,128]{2,1,0:T(8,128)(2,1)}, u32[]{:S(2)}, u32[]{:S(2)}) collective-permute-start(bf16[16,64,128]{2,1,0:T(8,128)(2,1)S(1)} %slice.13.w0_ref), channel_id=1, source_target_pairs={{0,16},{8,24},{16,0},{24,8},{1,17},{9,25},{17,1},{25,9},{2,18},{10... | collective-permute-start | bytes 786440 | tf_op jit(solution)/shard_map/ppermute | solution.py:93
  56.9 68.3 %collective-permute-start.4 = (bf16[16,160,128]{2,1,0:T(8,128)(2,1)S(1)}, bf16[16,160,128]{2,1,0:T(8,128)(2,1)}, u32[]{:S(2)}, u32[]{:S(2)}) collective-permute-start(bf16[16,160,128]{2,1,0:T(8,128)(2,1)S(1)} %slice.14.w0_ref), channel_id=1, source_target_pairs={{0,8},{8,16},{16,24},{24,0},{1,9},{9,17},{17,25},{25,1},{2,10},{10... | collective-permute-start | bytes 1966088 | tf_op jit(solution)/shard_map/ppermute | solution.py:93
  60.5 34.1 %collective-permute-start.1 = (bf16[16,64,128]{2,1,0:T(8,128)(2,1)S(1)}, bf16[16,64,128]{2,1,0:T(8,128)(2,1)}, u32[]{:S(2)}, u32[]{:S(2)}) collective-permute-start(bf16[16,64,128]{2,1,0:T(8,128)(2,1)S(1)} %slice.13.w0_ref), channel_id=1, source_target_pairs={{0,8},{8,16},{16,24},{24,0},{1,9},{9,17},{17,25},{25,1},{2,10},{10... | collective-permute-start | bytes 786440 | tf_op jit(solution)/shard_map/ppermute | solution.py:93
  62.4 32.2 %copy-start.4 = (bf16[16,64,128]{2,1,0:T(8,128)(2,1)S(1)}, bf16[16,64,128]{2,1,0:T(8,128)(2,1)}, u32[]{:S(2)}) copy-start(bf16[16,64,128]{2,1,0:T(8,128)(2,1)} %copy-done.3) | copy-start | bytes 786436
  68.6 26.0 %collective-permute-start = (bf16[16,2048]{1,0:T(8,128)(2,1)S(1)}, bf16[16,2048]{1,0:T(8,128)(2,1)S(1)}, u32[]{:S(2)}, u32[]{:S(2)}) collective-permute-start(bf16[16,2048]{1,0:T(8,128)(2,1)S(1)} %slice.12), channel_id=1, source_target_pairs={{0,32},{32,64},{64,96},{96,128},{128,160},{160,192},{192,224},{224... | collective-permute-start | bytes 196616 | tf_op jit(solution)/shard_map/ppermute | solution.py:371
  94.6 31.6 %copy-start.5 = (bf16[1,128,128]{2,1,0:T(8,128)(2,1)S(1)}, bf16[1,128,128]{2,1,0:T(8,128)(2,1)}, u32[]{:S(2)}) copy-start(bf16[1,128,128]{2,1,0:T(8,128)(2,1)} %param.29) | copy-start | bytes 98308
  94.6 31.6 %copy-start.7 = (f32[128]{0:T(128)S(1)}, f32[128]{0:T(128)}, u32[]{:S(2)}) copy-start(f32[128]{0:T(128)} %param.30) | copy-start | bytes 1540
  94.6 31.5 %copy-start.8 = (f32[128]{0:T(128)S(1)}, f32[128]{0:T(128)}, u32[]{:S(2)}) copy-start(f32[128]{0:T(128)} %param.31) | copy-start | bytes 1540
  99.4 5.0 %collective-permute-start.7 = (bf16[128,256]{1,0:T(8,128)(2,1)S(1)}, bf16[128,256]{1,0:T(8,128)(2,1)S(1)}, u32[]{:S(2)}, u32[]{:S(2)}) collective-permute-start(bf16[128,256]{1,0:T(8,128)(2,1)S(1)} %get-tuple-element.30.own_ref), channel_id=1, source_target_pairs={{0,32},{32,0},{64,96},{96,64},{128,160},{160,128},{192,224},{224,1... | collective-permute-start | bytes 196616 | tf_op jit(solution)/shard_map/ppermute | solution.py:407
  104.6 6.6 %collective-permute-start.8 = (bf16[128,256]{1,0:T(8,128)(2,1)S(1)}, bf16[128,256]{1,0:T(8,128)(2,1)S(1)}, u32[]{:S(2)}, u32[]{:S(2)}) collective-permute-start(bf16[128,256]{1,0:T(8,128)(2,1)S(1)} %get-tuple-element.31.own_ref), channel_id=1, source_target_pairs={{0,64},{32,96},{64,0},{96,32},{128,192},{160,224},{192,128},{224,1... | collective-permute-start | bytes 196616 | tf_op jit(solution)/shard_map/ppermute | solution.py:407
  111.4 14.8 %collective-permute-start.9 = (bf16[128,256]{1,0:T(8,128)(2,1)S(1)}, bf16[128,256]{1,0:T(8,128)(2,1)S(1)}, u32[]{:S(2)}, u32[]{:S(2)}) collective-permute-start(bf16[128,256]{1,0:T(8,128)(2,1)S(1)} %get-tuple-element.33), channel_id=1, source_target_pairs={{0,128},{32,160},{64,192},{96,224},{128,256},{160,288},{192,320},{... | collective-permute-start | bytes 196616 | tf_op jit(solution)/shard_map/ppermute | solution.py:428
  114.5 10.6 %collective-permute-start.10 = (bf16[128,128]{1,0:T(8,128)(2,1)S(1)}, bf16[128,128]{1,0:T(8,128)(2,1)S(1)}, u32[]{:S(2)}, u32[]{:S(2)}) collective-permute-start(bf16[128,128]{1,0:T(8,128)(2,1)S(1)} %get-tuple-element.34), channel_id=1, source_target_pairs={{128,384},{160,416},{192,448},{224,480},{129,385},{161,417},{193,4... | collective-permute-start | bytes 98312 | tf_op jit(solution)/shard_map/ppermute | solution.py:428
  115.2 10.0 %collective-permute-start.12 = (bf16[128,128]{1,0:T(8,128)(2,1)S(1)}, bf16[128,128]{1,0:T(8,128)(2,1)S(1)}, u32[]{:S(2)}, u32[]{:S(2)}) collective-permute-start(bf16[128,128]{1,0:T(8,128)(2,1)S(1)} %get-tuple-element.35), channel_id=1, source_target_pairs={{0,384},{32,416},{64,448},{96,480},{1,385},{33,417},{65,449},{97,4... | collective-permute-start | bytes 98312 | tf_op jit(solution)/shard_map/ppermute | solution.py:428
  119.4 6.8 %collective-permute-start.11 = (bf16[128,128]{1,0:T(8,128)(2,1)S(1)}, bf16[128,128]{1,0:T(8,128)(2,1)S(1)}, u32[]{:S(2)}, u32[]{:S(2)}) collective-permute-start(bf16[128,128]{1,0:T(8,128)(2,1)S(1)} %get-tuple-element.35), channel_id=1, source_target_pairs={{0,256},{32,288},{64,320},{96,352},{128,384},{160,416},{192,448},{... | collective-permute-start | bytes 98312 | tf_op jit(solution)/shard_map/ppermute | solution.py:428
  129.5 7.7 %collective-permute-start.13 = (bf16[4,32,2048]{2,1,0:T(8,128)(2,1)S(1)}, bf16[4,32,2048]{2,1,0:T(8,128)(2,1)S(1)}, u32[]{:S(2)}, u32[]{:S(2)}) collective-permute-start(bf16[4,32,2048]{2,1,0:T(8,128)(2,1)S(1)} %get-tuple-element.38), channel_id=1, source_target_pairs={{0,1},{1,0},{2,3},{3,2},{4,5},{5,4},{6,7},{7,6},{8,9},{9,8},{10,11... | collective-permute-start | bytes 1572872 | tf_op jit(solution)/shard_map/ppermute | solution.py:450
  (1 other events, 0.7 us)
